TPU v7x, 256 devices: a whole 4x4x8 slice. The times are simulated.
256 devices in a mesh: ep: 64 (over z, y, core), tp: 4 (over x).
Axes of the slice: x: 4, y: 4, z: 8, core: 2. Of those that a mesh axis runs over, the one named last changes fastest.
Arguments:
- tokens: bfloat16 [1024, 4096], P(None, 'ep'), may hold values from -80 to 80
- mix_gain: bfloat16 [4096], P('ep'), may hold values from 0.099609375 to 1.8984375
- w_query: bfloat16 [4096, 1024], P('ep', 'tp'), may hold values from -0.09375 to 0.09375
- w_key: bfloat16 [4096, 1024], P('ep', 'tp'), may hold values from -0.09375 to 0.09375
- w_value: bfloat16 [4096, 2048], P('ep', 'tp'), may hold values from -0.09375 to 0.09375
- w_outgate: bfloat16 [4096, 2048], P('ep', 'tp'), may hold values from -0.09375 to 0.09375
- w_igate: bfloat16 [4096, 16], P('ep', 'tp'), may hold values from -0.09375 to 0.09375
- w_fgate: bfloat16 [4096, 16], P('ep', 'tp'), may hold values from -0.09375 to 0.09375
- igate_bias: float32 [16], P('tp'), may hold values from -3 to 3
- fgate_bias: float32 [16], P('tp'), may hold values from -1 to 3
- head_gain: bfloat16 [2048], P('tp'), may hold values from 0.099609375 to 1.8984375
- w_mixout: bfloat16 [2048, 4096], P('tp', 'ep'), may hold values from -0.125 to 0.125
- state_matrix: float32 [1024, 16, 64, 128], P('ep', 'tp'), may hold values from -3 to 3
- state_norm: float32 [1024, 16, 64], P('ep', 'tp'), may hold values from -3 to 3
- state_max: float32 [1024, 16], P('ep', 'tp'), may hold values from -3 to 3
- ffn_gain: bfloat16 [4096], P('ep'), may hold values from 0.099609375 to 1.8984375
- dense_mix: bfloat16 [4096], P('ep'), may hold values from -0.09375 to 0.09375
- w_dense_gate: bfloat16 [4096, 1024], P('ep', 'tp'), may hold values from -0.09375 to 0.09375
- w_dense_up: bfloat16 [4096, 1024], P('ep', 'tp'), may hold values from -0.09375 to 0.09375
- w_dense_down: bfloat16 [1024, 4096], P('tp', 'ep'), may hold values from -0.1875 to 0.1875
- routes: int32 [1024, 4], replicated, may hold values from 0 to 63, all different within a row; in each aligned block of 16 rows (0 to 15, 16 to 31, ...) at most 2 rows name the same one
- route_weights: float32 [1024, 4], replicated, may hold values from 0.2 to 1.5
- w_exp_gate: bfloat16 [64, 4096, 1024], P('ep', None, 'tp'), may hold values from -0.09375 to 0.09375
- w_exp_up: bfloat16 [64, 4096, 1024], P('ep', None, 'tp'), may hold values from -0.09375 to 0.09375
- w_exp_down: bfloat16 [64, 1024, 4096], P('ep', 'tp'), may hold values from -0.1875 to 0.1875
Outputs:
- layer_out: bfloat16 [1024, 4096], P(None, 'ep')
- new_matrix: float32 [1024, 16, 64, 128], P('ep', 'tp')
- new_norm: float32 [1024, 16, 64], P('ep', 'tp')
- new_max: float32 [1024, 16], P('ep', 'tp')
Inputs may be any that keep to these rules, and one draw needn't show every extreme that they name: `routes`: each row names 4 different experts. In the rows of one device (aligned blocks of 16 rows) no expert is named by more than 2 rows, a bound that some block reaches.
All inputs are finite; a program needn't handle non-finite values.
Results may differ from a plain program's by a relative error of at most 0.012.
Values may be sent and summed in bfloat16 or wider, within the bound.
No kernel may reach another device: no remote copies, remote signals or barrier semaphores. Data moves between devices by JAX's collectives and lax.ppermute only.
A program may use at most 128 MiB of HBM per device.

v0:
```python
import jax
import jax.numpy as jnp
from jax import lax
from jax.sharding import PartitionSpec as P

D = 4096


EPSILON = 1e-06
SOFT_CAP = 15.0


def in_one_piece(arrays, axis, dim, along):
    ends, at = ([], 0)
    for a in arrays[:-1]:
        at += a.shape[along]
        ends.append(at)
    both = jnp.concatenate(arrays, axis=along)
    return tuple(jnp.split(lax.all_gather(both, axis, axis=dim, tiled=True), ends, axis=along))


def in_order(blocks, dim):
    blocks = jnp.moveaxis(blocks, 0, dim)
    lengths = blocks.shape
    return blocks.reshape(*lengths[:dim], lengths[dim] * lengths[dim + 1], *lengths[dim + 2 :])


def sent_to_all(x, axis):
    copies = jnp.broadcast_to(x, (lax.axis_size(axis), *x.shape))
    return lax.all_to_all(copies, axis, split_axis=0, concat_axis=0, tiled=True)


def gather_directly(x, axis, dim):
    return in_order(sent_to_all(x, axis), dim)


def taken_together(x, axis):
    everything = sent_to_all(x, axis)
    return jnp.sum(everything, axis=0)


def over_copies(x, axis):
    return sent_to_all(x, axis).astype(jnp.float32).sum(axis=0)


def together(arrays, axis):
    ravelled, at, finished = (jnp.concatenate([a.reshape(-1) for a in arrays]), 0, [])
    so_far = taken_together(ravelled, axis)
    for a in arrays:
        finished.append(so_far[at : at + a.size].reshape(a.shape))
        at += a.size
    return tuple(finished)


def cut_along(x, dim, size):
    lengths = x.shape
    blocks = x.reshape(*lengths[:dim], size, lengths[dim] // size, *lengths[dim + 1 :])
    return jnp.moveaxis(blocks, dim, 0)


def sent_and_summed(x, axis, dim):
    blocks = cut_along(x, dim, lax.axis_size(axis))
    arrived = lax.all_to_all(blocks, axis, split_axis=0, concat_axis=0, tiled=True)
    return arrived.astype(jnp.float32).sum(axis=0)


def gate_logs(in_pre, forget_pre, igate_bias, fgate_bias):
    in_log = SOFT_CAP * jnp.tanh((in_pre + igate_bias) / SOFT_CAP)
    forget_log = jax.nn.log_sigmoid(SOFT_CAP * jnp.tanh((forget_pre + fgate_bias) / SOFT_CAP))
    return (in_log, forget_log)


def recurrent_read(
    queries, keys_in, values_in, in_log, forget_log, state_matrix, state_norm, state_max
):
    scaled_query = queries.astype(jnp.float32) * queries.shape[-1] ** (-0.5)
    key_float = keys_in.astype(jnp.float32)
    value_float = values_in.astype(jnp.float32)
    new_max = jnp.maximum(forget_log + state_max, in_log)
    carried = jnp.exp(forget_log + state_max - new_max)
    fresh_weight = jnp.exp(in_log - new_max)
    new_matrix = (
        carried[..., None, None] * state_matrix
        + fresh_weight[..., None, None] * key_float[..., :, None] * value_float[..., None, :]
    )
    new_norm = carried[..., None] * state_norm + fresh_weight[..., None] * key_float
    numerator = jnp.sum(new_matrix * scaled_query[..., :, None], axis=-2)
    denominator = jnp.sum(new_norm * scaled_query, axis=-1)
    floor_value = jnp.maximum(jnp.abs(denominator), jnp.exp(-new_max))
    readout = numerator / floor_value[..., None]
    return (readout, new_matrix, new_norm, new_max)


def head_output(readout, outgates, head_gain):
    scaled = readout * lax.rsqrt(jnp.mean(readout * readout, axis=-1, keepdims=True) + EPSILON)
    rows_count, heads_count, head_width = readout.shape
    gated_rows = (
        scaled.reshape(rows_count, heads_count * head_width)
        * head_gain.astype(jnp.float32)[None, :]
    )
    gated_rows = gated_rows * jax.nn.sigmoid(outgates.astype(jnp.float32))
    return gated_rows.astype(jnp.bfloat16)


def expert_slots(routes, groups, capacity, experts_all):
    row_total = routes.shape[0]
    chosen = (routes[:, :, None] == jnp.arange(experts_all, dtype=jnp.int32)[None, None, :]).astype(
        jnp.int32
    )
    per_row = jnp.sum(chosen, axis=1)
    grouped = per_row.reshape(groups, row_total // groups, experts_all)
    earlier = (jnp.cumsum(grouped, axis=1) - grouped).reshape(row_total, experts_all)
    rank_in = jnp.sum(chosen * earlier[:, None, :], axis=2)
    group_of = jnp.arange(row_total, dtype=jnp.int32) // (row_total // groups)
    return routes * (groups * capacity) + group_of[:, None] * capacity + rank_in


def mixer_half(
    normed,
    weights,
    igate_bias,
    fgate_bias,
    head_gain,
    w_mixout,
    state_matrix,
    state_norm,
    state_max,
):
    seq_rows = state_matrix.shape[0]
    heads_here = state_matrix.shape[1]
    w_query, w_key, w_value, w_outgate, w_igate, w_fgate = weights
    own_rows = lax.all_to_all(normed, "ep", split_axis=0, concat_axis=1, tiled=True)
    pieces = in_one_piece((w_query, w_key, w_value, w_outgate, w_igate, w_fgate), "ep", 0, 1)
    pieces_out = tuple(
        (
            jnp.dot(own_rows, shard_piece, preferred_element_type=jnp.float32)
            for shard_piece in pieces
        )
    )
    queries = pieces_out[0].astype(jnp.bfloat16).reshape(seq_rows, heads_here, -1)
    keys_in = pieces_out[1].astype(jnp.bfloat16).reshape(seq_rows, heads_here, -1)
    values_in = pieces_out[2].astype(jnp.bfloat16).reshape(seq_rows, heads_here, -1)
    outgates = pieces_out[3].astype(jnp.bfloat16)
    in_log, forget_log = gate_logs(pieces_out[4], pieces_out[5], igate_bias, fgate_bias)
    readout, new_matrix, new_norm, new_max = recurrent_read(
        queries, keys_in, values_in, in_log, forget_log, state_matrix, state_norm, state_max
    )
    heads_out = head_output(readout, outgates, head_gain)
    partial_rows = jnp.dot(
        gather_directly(heads_out, "ep", 0), w_mixout, preferred_element_type=jnp.float32
    )
    return (partial_rows, new_matrix, new_norm, new_max)


def on_device(
    tokens,
    mix_gain,
    w_query,
    w_key,
    w_value,
    w_outgate,
    w_igate,
    w_fgate,
    igate_bias,
    fgate_bias,
    head_gain,
    w_mixout,
    state_matrix,
    state_norm,
    state_max,
    ffn_gain,
    dense_mix,
    w_dense_gate,
    w_dense_up,
    w_dense_down,
    routes,
    route_weights,
    w_exp_gate,
    w_exp_up,
    w_exp_down,
):
    groups = lax.axis_size("ep")
    seq_rows = state_matrix.shape[0]
    feature_cols = tokens.shape[1]
    token_float = tokens.astype(jnp.float32)
    square_sum = taken_together(jnp.sum(token_float * token_float, axis=1), "ep")
    inverse = lax.rsqrt(square_sum / D + EPSILON)
    normed = (token_float * inverse[:, None] * mix_gain.astype(jnp.float32)[None, :]).astype(
        jnp.bfloat16
    )
    weights = (w_query, w_key, w_value, w_outgate, w_igate, w_fgate)
    partial_rows, new_matrix, new_norm, new_max = mixer_half(
        normed,
        weights,
        igate_bias,
        fgate_bias,
        head_gain,
        w_mixout,
        state_matrix,
        state_norm,
        state_max,
    )
    mixer_total = over_copies(partial_rows.astype(jnp.bfloat16), "tp").astype(jnp.float32)
    mixer = lax.optimization_barrier(mixer_total.astype(jnp.bfloat16))
    hidden_state = lax.optimization_barrier(
        (token_float + mixer.astype(jnp.float32)).astype(jnp.bfloat16)
    )
    hidden_float = hidden_state.astype(jnp.float32)
    gain_float = ffn_gain.astype(jnp.float32)
    square_two, gate_dot = together(
        (
            jnp.sum(hidden_float * hidden_float, axis=1),
            jnp.sum(
                hidden_float * gain_float[None, :] * dense_mix.astype(jnp.float32)[None, :], axis=1
            ),
        ),
        "ep",
    )
    inverse_two = lax.rsqrt(square_two / D + EPSILON)
    dense_gate = inverse_two * gate_dot
    normed_two = (hidden_float * inverse_two[:, None] * gain_float[None, :]).astype(jnp.bfloat16)
    dense_sum = sent_and_summed(
        jnp.concatenate(
            [
                jnp.dot(normed_two, w_dense_gate, preferred_element_type=jnp.float32),
                jnp.dot(normed_two, w_dense_up, preferred_element_type=jnp.float32),
            ],
            axis=1,
        ).astype(jnp.bfloat16),
        "ep",
        0,
    )
    unit_count = w_dense_gate.shape[1]
    dense_hidden = (jax.nn.silu(dense_sum[:, :unit_count]) * dense_sum[:, unit_count:]).astype(
        jnp.bfloat16
    )
    dense_rows = jnp.dot(
        gather_directly(dense_hidden, "ep", 0), w_dense_down, preferred_element_type=jnp.float32
    )
    experts_all = w_exp_gate.shape[0] * groups
    pick_count = routes.shape[1]
    capacity = max(2, 2 * seq_rows * pick_count // experts_all)
    slot_count = groups * capacity
    flat_index = expert_slots(routes, groups, capacity, experts_all).reshape(-1)
    sources = jnp.repeat(normed_two, pick_count, axis=0)
    send_rows = (
        jnp.zeros((experts_all * slot_count, feature_cols), jnp.bfloat16)
        .at[flat_index]
        .set(sources)
    )
    send_rows = send_rows.reshape(experts_all, slot_count, feature_cols)
    arrived = lax.all_to_all(send_rows, "ep", split_axis=0, concat_axis=2, tiled=True)
    gate_part = jnp.einsum("esd,edf->esf", arrived, w_exp_gate, preferred_element_type=jnp.float32)
    upper_part = jnp.einsum("esd,edf->esf", arrived, w_exp_up, preferred_element_type=jnp.float32)
    expert_hidden = (jax.nn.silu(gate_part) * upper_part).astype(jnp.bfloat16)
    down_part = jnp.einsum(
        "esf,efd->esd", expert_hidden, w_exp_down, preferred_element_type=jnp.float32
    ).astype(jnp.bfloat16)
    returned = lax.all_to_all(down_part, "ep", split_axis=2, concat_axis=0, tiled=True)
    picked = returned.reshape(experts_all * slot_count, feature_cols)[flat_index].astype(
        jnp.float32
    )
    picked = picked.reshape(routes.shape[0], pick_count, feature_cols)
    routed = jnp.sum(picked * route_weights[:, :, None], axis=1)
    branch_total = over_copies(
        (routed + jax.nn.sigmoid(dense_gate)[:, None] * dense_rows).astype(jnp.bfloat16), "tp"
    ).astype(jnp.float32)
    layer_out = (hidden_float + branch_total).astype(jnp.bfloat16)
    return (layer_out, new_matrix, new_norm, new_max)


def solution(mesh):
    return jax.shard_map(
        on_device,
        mesh=mesh,
        in_specs=(
            P(None, "ep"),
            P("ep"),
            P("ep", "tp"),
            P("ep", "tp"),
            P("ep", "tp"),
            P("ep", "tp"),
            P("ep", "tp"),
            P("ep", "tp"),
            P("tp"),
            P("tp"),
            P("tp"),
            P("tp", "ep"),
            P("ep", "tp", None, None),
            P("ep", "tp", None),
            P("ep", "tp"),
            P("ep"),
            P("ep"),
            P("ep", "tp"),
            P("ep", "tp"),
            P("tp", "ep"),
            P(),
            P(),
            P("ep", None, "tp"),
            P("ep", None, "tp"),
            P("ep", "tp", None),
        ),
        out_specs=(P(None, "ep"), P("ep", "tp", None, None), P("ep", "tp", None), P("ep", "tp")),
        check_vma=False,
    )
```

profile of v0, /device:TPU:8, one launch (start us, length us, event | category | flops | bytes accessed | tf_op | source)
XLA Modules:
  0.0 394.6 jit_solution(14655723986366283353)
XLA Ops:
  12.4 12.1 %all-to-all-start = ((f32[64,1,1024]{2,1,0:T(1,128)}), f32[64,1,1024]{2,1,0:T(1,128)S(1)}, u32[]{:S(2)}, u32[]{:S(2)}) async-start(f32[64,1,1024]{2,1,0:T(1,128)} %broadcast_in_dim.16), calls=%async_computation | async-start | bytes 524288 | tf_op jit(solution)/shard_map/all_to_all | solution.py:30
  25.2 12.9 %all-to-all-done = f32[64,1,1024]{2,1,0:T(1,128)S(1)} async-done(((f32[64,1,1024]{2,1,0:T(1,128)}), f32[64,1,1024]{2,1,0:T(1,128)S(1)}, u32[]{:S(2)}, u32[]{:S(2)}) %all-to-all-start) | async-done | bytes 262176 | tf_op jit(solution)/shard_map/all_to_all | solution.py:30
  40.4 5.6 %all-to-all-start.1 = ((bf16[64,2,512]{2,1,0:T(2,128)(2,1)}), bf16[64,2,512]{2,1,0:T(2,128)(2,1)S(1)}, u32[]{:S(2)}, u32[]{:S(2)}) async-start(bf16[64,2,512]{2,1,0:T(2,128)(2,1)} %reshape.224), calls=%async_computation.1 | async-start | bytes 262144 | tf_op jit(solution)/shard_map/all_to_all | solution.py:132
  46.0 10.0 %all-to-all-done.1 = bf16[64,2,512]{2,1,0:T(2,128)(2,1)S(1)} async-done(((bf16[64,2,512]{2,1,0:T(2,128)(2,1)}), bf16[64,2,512]{2,1,0:T(2,128)(2,1)S(1)}, u32[]{:S(2)}, u32[]{:S(2)}) %all-to-all-start.1) | async-done | bytes 131104 | tf_op jit(solution)/shard_map/all_to_all | solution.py:132
  56.6 49.1 %all-gather.2.cloned.1.call-done = bf16[4096,1544]{1,0:T(8,128)(2,1)} async-done(((bf16[64,1544]{1,0:T(8,128)(2,1)}), bf16[4096,1544]{1,0:T(8,128)(2,1)}) %all-gather.2.cloned.1.call-update) | async-done | bytes 12648464 | tf_op jit(solution)/shard_map/all_gather | solution.py:19
  125.8 7.5 %all-to-all-start.2 = ((bf16[64,16,512]{2,1,0:T(8,128)(2,1)}), bf16[64,16,512]{2,1,0:T(8,128)(2,1)S(1)}, u32[]{:S(2)}, u32[]{:S(2)}) async-start(bf16[64,16,512]{2,1,0:T(8,128)(2,1)} %broadcast_in_dim.17), calls=%async_computation.2 | async-start | bytes 2097152 | tf_op jit(solution)/shard_map/all_to_all | solution.py:30
  135.6 26.6 %all-to-all-done.2 = bf16[64,16,512]{2,1,0:T(8,128)(2,1)S(1)} async-done(((bf16[64,16,512]{2,1,0:T(8,128)(2,1)}), bf16[64,16,512]{2,1,0:T(8,128)(2,1)S(1)}, u32[]{:S(2)}, u32[]{:S(2)}) %all-to-all-start.2) | async-done | bytes 1048608 | tf_op jit(solution)/shard_map/all_to_all | solution.py:30
  163.4 4.2 %all-to-all-start.3 = ((bf16[4,1024,64]{1,2,0:T(8,128)(2,1)}), bf16[4,1024,64]{1,2,0:T(8,128)(2,1)S(1)}, u32[]{:S(2)}, u32[]{:S(2)}) async-start(bf16[4,1024,64]{1,2,0:T(8,128)(2,1)} %broadcast_in_dim.18), calls=%async_computation.3 | async-start | bytes 1048576 | tf_op jit(solution)/shard_map/all_to_all | solution.py:30
  171.6 4.6 %all-to-all-done.3 = bf16[4,1024,64]{1,2,0:T(8,128)(2,1)S(1)} async-done(((bf16[4,1024,64]{1,2,0:T(8,128)(2,1)}), bf16[4,1024,64]{1,2,0:T(8,128)(2,1)S(1)}, u32[]{:S(2)}, u32[]{:S(2)}) %all-to-all-start.3) | async-done | bytes 524320 | tf_op jit(solution)/shard_map/all_to_all | solution.py:30
  178.1 6.4 %all-to-all-start.4 = ((f32[64,1,2048]{2,1,0:T(1,128)}), f32[64,1,2048]{2,1,0:T(1,128)S(1)}, u32[]{:S(2)}, u32[]{:S(2)}) async-start(f32[64,1,2048]{2,1,0:T(1,128)} %broadcast_in_dim.20), calls=%async_computation.4 | async-start | bytes 1048576 | tf_op jit(solution)/shard_map/all_to_all | solution.py:30
  185.2 16.9 %all-to-all-done.4 = f32[64,1,2048]{2,1,0:T(1,128)S(1)} async-done(((f32[64,1,2048]{2,1,0:T(1,128)}), f32[64,1,2048]{2,1,0:T(1,128)S(1)}, u32[]{:S(2)}, u32[]{:S(2)}) %all-to-all-start.4) | async-done | bytes 524320 | tf_op jit(solution)/shard_map/all_to_all | solution.py:30
  205.2 12.5 %scatter_custom_fusion = bf16[8192,64]{1,0:T(8,128)(2,1)} fusion(s32[4096]{0:T(1024)S(1)} %bitcast.78, bf16[4096,64]{1,0:T(8,128)(2,1)S(1)} %bitcast.75, bf16[]{:T(256)} %constant.53.clone.1), kind=kCustom, calls=%fused_computation.61 | custom fusion | bytes 1048578 | tf_op jit(solution)/shard_map/scatter | solution.py:249
  220.4 6.0 %all-to-all-start.5 = ((bf16[64,128,64]{1,2,0:T(8,128)(2,1)}), bf16[64,128,64]{1,2,0:T(8,128)(2,1)S(1)}, u32[]{:S(2)}, u32[]{:S(2)}) async-start(bf16[64,128,64]{1,2,0:T(8,128)(2,1)} %copy.178), calls=%async_computation.5 | async-start | bytes 2097152 | tf_op jit(solution)/shard_map/all_to_all | solution.py:252
  228.2 27.0 %all-to-all-done.5 = bf16[64,128,64]{1,2,0:T(8,128)(2,1)S(1)} async-done(((bf16[64,128,64]{1,2,0:T(8,128)(2,1)}), bf16[64,128,64]{1,2,0:T(8,128)(2,1)S(1)}, u32[]{:S(2)}, u32[]{:S(2)}) %all-to-all-start.5) | async-done | bytes 1048608 | tf_op jit(solution)/shard_map/all_to_all | solution.py:252
  255.2 5.9 %all-to-all-start.7 = ((bf16[64,16,512]{2,1,0:T(8,128)(2,1)}), bf16[64,16,512]{2,1,0:T(8,128)(2,1)}, u32[]{:S(2)}, u32[]{:S(2)}) async-start(bf16[64,16,512]{2,1,0:T(8,128)(2,1)} %pad_maximum_fusion), calls=%async_computation.7 | async-start | bytes 2097152 | tf_op jit(solution)/shard_map/all_to_all | solution.py:63
  263.2 3.9 fusion
  267.1 5.5 %copy.179 = bf16[1,128,4096]{1,0,2:T(2,128)(2,1)} copy(bf16[1,128,4096]{2,1,0:T(8,128)(2,1)} %fusion) | data formatting | bytes 2097152 | tf_op jit(solution)/shard_map/convert_element_type | solution.py:258
  273.1 23.4 %reduce.3 = bf16[4096,128]{1,0:T(8,128)(2,1)S(1)} reduce(bf16[4096,1,128]{2,1,0:T(2,128)(2,1)} %bitcast.67, bf16[]{:T(256)} %broadcast.168), dimensions={1}, to_apply=%bitcast.44.reduce_sub_computation | reduce | bytes 2097154
  297.7 10.4 %all-to-all-start.6 = ((bf16[64,2,4096]{2,1,0:T(2,128)(2,1)}), bf16[64,2,4096]{2,1,0:T(2,128)(2,1)S(1)}, u32[]{:S(2)}, u32[]{:S(2)}) async-start(bf16[64,2,4096]{2,1,0:T(2,128)(2,1)} %reshape.226), calls=%async_computation.6 | async-start | bytes 2097152 | tf_op jit(solution)/shard_map/all_to_all | solution.py:259
  309.5 27.3 %all-to-all-done.6 = bf16[64,2,4096]{2,1,0:T(2,128)(2,1)S(1)} async-done(((bf16[64,2,4096]{2,1,0:T(2,128)(2,1)}), bf16[64,2,4096]{2,1,0:T(2,128)(2,1)S(1)}, u32[]{:S(2)}, u32[]{:S(2)}) %all-to-all-start.6) | async-done | bytes 1048608 | tf_op jit(solution)/shard_map/all_to_all | solution.py:259
  337.7 5.9 %all-to-all-start.8 = ((bf16[64,16,256]{2,1,0:T(8,128)(2,1)}), bf16[64,16,256]{2,1,0:T(8,128)(2,1)}, u32[]{:S(2)}, u32[]{:S(2)}) async-start(bf16[64,16,256]{2,1,0:T(8,128)(2,1)} %broadcast_in_dim.22), calls=%async_computation.8 | async-start | bytes 1048576 | tf_op jit(solution)/shard_map/all_to_all | solution.py:30
  351.7 12.9 %gather_fusion = bf16[4096,64]{1,0:T(8,128)(2,1)S(1)} fusion(bf16[8192,64]{1,0:T(8,128)(2,1)} %bitcast.62, s32[4096]{0:T(1024)S(1)} %broadcast_clamp_fusion), kind=kCustom, calls=%fused_computation | custom fusion | bytes 1064960 | tf_op jit(solution)/shard_map/gather | solution.py:260
  364.6 7.4 %fusion.9 = f32[1024,64]{1,0:T(8,128)} fusion(bf16[1024,4,64]{2,1,0:T(4,128)(2,1)S(1)} %bitcast.69, f32[1024,4]{1,0:T(8,128)} %copy.181), kind=kLoop, calls=%fused_computation.13 | loop fusion | flops 720896 | bytes 802816 | tf_op jit(solution)/shard_map/reduce_sum | solution.py:264
  374.6 12.4 %all_to_all.86 = bf16[4,1024,64]{1,2,0:T(8,128)(2,1)S(1)} all-to-all(bf16[4,1024,64]{1,2,0:T(8,128)(2,1)S(1)} %broadcast_in_dim.23), channel_id=1, replica_groups=mesh['ep'=64,'tp'=4] {'tp'}, dimensions={0} | all-to-all | bytes 1048576 | tf_op jit(solution)/shard_map/all_to_all | solution.py:30
  (118 shorter events, 63.5 us)
Async XLA Ops:
  7.2 256.0 %copy-start = (bf16[1,256,4096]{2,1,0:T(8,128)(2,1)S(1)}, bf16[1,256,4096]{2,1,0:T(8,128)(2,1)}, u32[]{:S(2)}) copy-start(bf16[1,256,4096]{2,1,0:T(8,128)(2,1)} %param.49) | copy-start | bytes 6291460
  7.2 38.8 %copy-start.11 = (bf16[512]{0:T(512)(128)(2,1)S(1)}, bf16[512]{0:T(512)(128)(2,1)}, u32[]{:S(2)}) copy-start(bf16[512]{0:T(512)(128)(2,1)} %param.35) | copy-start | bytes 3076
  7.2 98.6 %all-gather.2.cloned.1.call-start = ((), (), s32[]{:S(2)}) async-start(), calls=%async_computation.10 | async-start | bytes 13844480 | tf_op jit(solution)/shard_map/all_gather | solution.py:19
  10.6 95.1 %copy-start.12 = (f32[4]{0:T(128)S(1)}, f32[4]{0:T(128)}, u32[]{:S(2)}) copy-start(f32[4]{0:T(128)} %param.33) | copy-start | bytes 52
  12.4 25.7 %all-to-all-start = ((f32[64,1,1024]{2,1,0:T(1,128)}), f32[64,1,1024]{2,1,0:T(1,128)S(1)}, u32[]{:S(2)}, u32[]{:S(2)}) async-start(f32[64,1,1024]{2,1,0:T(1,128)} %broadcast_in_dim.16), calls=%async_computation | async-start | bytes 524288 | tf_op jit(solution)/shard_map/all_to_all | solution.py:30
  24.5 82.8 %copy-start.10 = (f32[16,4]{0,1:T(4,128)S(1)}, f32[16,4]{0,1:T(4,128)}, u32[]{:S(2)}) copy-start(f32[16,4]{0,1:T(4,128)} %param.39) | copy-start | bytes 772
  24.5 82.9 %copy-start.13 = (f32[4]{0:T(128)S(1)}, f32[4]{0:T(128)}, u32[]{:S(2)}) copy-start(f32[4]{0:T(128)} %param.34) | copy-start | bytes 52
  40.4 15.7 %all-to-all-start.1 = ((bf16[64,2,512]{2,1,0:T(2,128)(2,1)}), bf16[64,2,512]{2,1,0:T(2,128)(2,1)S(1)}, u32[]{:S(2)}, u32[]{:S(2)}) async-start(bf16[64,2,512]{2,1,0:T(2,128)(2,1)} %reshape.224), calls=%async_computation.1 | async-start | bytes 262144 | tf_op jit(solution)/shard_map/all_to_all | solution.py:132
  109.6 8.0 %copy-start.8 = (f32[16,4]{0,1:T(4,128)}, f32[16,4]{0,1:T(4,128)S(1)}, u32[]{:S(2)}) copy-start(f32[16,4]{0,1:T(4,128)S(1)} %get-tuple-element.28) | copy-start | bytes 772
  124.6 8.7 %copy-start.14 = (bf16[64]{0:T(256)(128)(2,1)S(1)}, bf16[64]{0:T(256)(128)(2,1)}, u32[]{:S(2)}) copy-start(bf16[64]{0:T(256)(128)(2,1)} %param.40) | copy-start | bytes 388
  124.6 9.3 %copy-start.15 = (bf16[64]{0:T(256)(128)(2,1)S(1)}, bf16[64]{0:T(256)(128)(2,1)}, u32[]{:S(2)}) copy-start(bf16[64]{0:T(256)(128)(2,1)} %param.41) | copy-start | bytes 388
  124.6 9.8 %copy-start.2 = (s32[1024,4]{0,1:T(4,128)S(1)}, s32[1024,4]{0,1:T(4,128)}, u32[]{:S(2)}) copy-start(s32[1024,4]{0,1:T(4,128)} %param.45) | copy-start | bytes 49156
  124.7 37.5 %copy-start.3 = (bf16[512,64]{0,1:T(8,128)(2,1)S(1)}, bf16[512,64]{0,1:T(8,128)(2,1)}, u32[]{:S(2)}) copy-start(bf16[512,64]{0,1:T(8,128)(2,1)} %param.36) | copy-start | bytes 196612
  125.8 36.3 %all-to-all-start.2 = ((bf16[64,16,512]{2,1,0:T(8,128)(2,1)}), bf16[64,16,512]{2,1,0:T(8,128)(2,1)S(1)}, u32[]{:S(2)}, u32[]{:S(2)}) async-start(bf16[64,16,512]{2,1,0:T(8,128)(2,1)} %broadcast_in_dim.17), calls=%async_computation.2 | async-start | bytes 2097152 | tf_op jit(solution)/shard_map/all_to_all | solution.py:30
  163.4 12.8 %all-to-all-start.3 = ((bf16[4,1024,64]{1,2,0:T(8,128)(2,1)}), bf16[4,1024,64]{1,2,0:T(8,128)(2,1)S(1)}, u32[]{:S(2)}, u32[]{:S(2)}) async-start(bf16[4,1024,64]{1,2,0:T(8,128)(2,1)} %broadcast_in_dim.18), calls=%async_computation.3 | async-start | bytes 1048576 | tf_op jit(solution)/shard_map/all_to_all | solution.py:30
  167.7 8.6 %copy-start.1 = (bf16[1024,64]{0,1:T(8,128)(2,1)S(1)}, bf16[1024,64]{0,1:T(8,128)(2,1)}, u32[]{:S(2)}) copy-start(bf16[1024,64]{0,1:T(8,128)(2,1)} %param.25) | copy-start | bytes 393220
  178.1 24.0 %all-to-all-start.4 = ((f32[64,1,2048]{2,1,0:T(1,128)}), f32[64,1,2048]{2,1,0:T(1,128)S(1)}, u32[]{:S(2)}, u32[]{:S(2)}) async-start(f32[64,1,2048]{2,1,0:T(1,128)} %broadcast_in_dim.20), calls=%async_computation.4 | async-start | bytes 1048576 | tf_op jit(solution)/shard_map/all_to_all | solution.py:30
  217.7 8.7 %copy-start.5 = (bf16[64,256]{1,0:T(8,128)(2,1)S(1)}, bf16[64,256]{1,0:T(8,128)(2,1)}, u32[]{:S(2)}) copy-start(bf16[64,256]{1,0:T(8,128)(2,1)} %param.42) | copy-start | bytes 98308
  220.4 34.8 %all-to-all-start.5 = ((bf16[64,128,64]{1,2,0:T(8,128)(2,1)}), bf16[64,128,64]{1,2,0:T(8,128)(2,1)S(1)}, u32[]{:S(2)}, u32[]{:S(2)}) async-start(bf16[64,128,64]{1,2,0:T(8,128)(2,1)} %copy.178), calls=%async_computation.5 | async-start | bytes 2097152 | tf_op jit(solution)/shard_map/all_to_all | solution.py:252
  255.2 42.5 %all-to-all-start.7 = ((bf16[64,16,512]{2,1,0:T(8,128)(2,1)}), bf16[64,16,512]{2,1,0:T(8,128)(2,1)}, u32[]{:S(2)}, u32[]{:S(2)}) async-start(bf16[64,16,512]{2,1,0:T(8,128)(2,1)} %pad_maximum_fusion), calls=%async_computation.7 | async-start | bytes 2097152 | tf_op jit(solution)/shard_map/all_to_all | solution.py:63
  297.7 45.9 %copy-start.9 = (f32[1024,4]{0,1:T(4,128)S(1)}, f32[1024,4]{0,1:T(4,128)}, u32[]{:S(2)}) copy-start(f32[1024,4]{0,1:T(4,128)} %param.46) | copy-start | bytes 49156
  297.7 39.2 %all-to-all-start.6 = ((bf16[64,2,4096]{2,1,0:T(2,128)(2,1)}), bf16[64,2,4096]{2,1,0:T(2,128)(2,1)S(1)}, u32[]{:S(2)}, u32[]{:S(2)}) async-start(bf16[64,2,4096]{2,1,0:T(2,128)(2,1)} %reshape.226), calls=%async_computation.6 | async-start | bytes 2097152 | tf_op jit(solution)/shard_map/all_to_all | solution.py:259
  337.7 35.4 %all-to-all-start.8 = ((bf16[64,16,256]{2,1,0:T(8,128)(2,1)}), bf16[64,16,256]{2,1,0:T(8,128)(2,1)}, u32[]{:S(2)}, u32[]{:S(2)}) async-start(bf16[64,16,256]{2,1,0:T(8,128)(2,1)} %broadcast_in_dim.22), calls=%async_computation.8 | async-start | bytes 1048576 | tf_op jit(solution)/shard_map/all_to_all | solution.py:30
  364.6 8.6 %copy-start.7 = (bf16[256,64]{0,1:T(8,128)(2,1)S(1)}, bf16[256,64]{0,1:T(8,128)(2,1)}, u32[]{:S(2)}) copy-start(bf16[256,64]{0,1:T(8,128)(2,1)} %param.44) | copy-start | bytes 98308
  (2 other events, 9.2 us)
Sparse Core Ops, SparseCore 0:
  10.8 94.9 all-gather.1
where the time goes:
time: 397 us; the launch traced here: 395 us
  waiting for transfers between devices  174 us (44%)
  starting transfers between devices  64.1 us (16%)
  local copies, waits for them, and re-layouts  60.8 us (15%)
  other arithmetic  46.4 us (12%)
  matrix products  21.9 us (6%)
  between operations  14.5 us (4%)
  blocking collectives  12.4 us (3%)
    all_to_all x5, waiting for transfers between devices, sent_to_all(): return lax.all_to_all(copies, axis, split_axis=0, concat_axis=0, tiled=True)  61 us
    all_gather x1, waiting for transfers between devices, in_one_piece(): lax.all_gather(both, axis, axis=dim, tiled=True)  49.1 us
    all_to_all x5, starting transfers between devices, sent_to_all(): return lax.all_to_all(copies, axis, split_axis=0, concat_axis=0, tiled=True)  36.2 us
    all_to_all x1, waiting for transfers between devices, on_device(): lax.all_to_all(down_part, 'ep', split_axis=2, concat_axis=0, tiled=True)  27.3 us
    all_to_all x1, waiting for transfers between devices, on_device(): lax.all_to_all(send_rows, 'ep', split_axis=0, concat_axis=2, tiled=True)  27 us
    unnamed x1, other arithmetic  23.4 us
    dot_general x6, matrix products, mixer_half(): jnp.dot(own_rows, shard_piece, preferred_element_type=jnp.float32)  13.5 us
    gather x1, local copies, waits for them, and re-layouts, on_device(): returned.reshape(experts_all * slot_count, feature_cols)[flat_index]  12.9 us
  transfers between devices with their start and end apart: 10, of which 8 were waited for; matrix products, arithmetic and copies ran while one was open for 21% of the time, Pallas kernels for 0%

commit v1 on v0

v1 whole, which is shorter than its diff:
```python
import functools

import jax
import jax.numpy as jnp
from jax import lax
from jax.experimental import pallas as pl
from jax.experimental.pallas import tpu as pltpu
from jax.sharding import Mesh
from jax.sharding import PartitionSpec as P


D = 4096


EPSILON = 1e-06
SOFT_CAP = 15.0
NZ, NY, NC, NX = 8, 4, 2, 4
EP = ("z", "y", "c")
F32, BF16 = jnp.float32, jnp.bfloat16


def exchanged(x, axis):
    return lax.all_to_all(x, axis, split_axis=0, concat_axis=0, tiled=True)


def to_all(x, axis):
    return exchanged(jnp.broadcast_to(x, (lax.axis_size(axis), *x.shape)), axis)


def other_core(x):
    return lax.ppermute(x, "c", [(0, 1), (1, 0)])


def stacked_kernel(*refs):
    for i in range(NZ):
        refs[-1][i] = refs[i][...]


def gathered_z(x):
    pieces = [x] + [
        lax.ppermute(x, "z", [(i, (i + s) % NZ) for i in range(NZ)]) for s in range(1, NZ)
    ]
    zs = pl.pallas_call(
        stacked_kernel,
        out_shape=jax.ShapeDtypeStruct((NZ, *x.shape), x.dtype),
        in_specs=[VMEM] * NZ,
        out_specs=VMEM,
        cost_estimate=pl.CostEstimate(flops=1 << 20, bytes_accessed=2 << 20, transcendentals=0),
        name="stacked",
    )(*pieces)
    return zs, other_core(zs)


def over_x(x):
    return to_all(x, "x").astype(F32).sum(axis=0)


def packed(x):
    h = x.shape[0] // 2
    return jnp.concatenate([x[:h], x[h:]], axis=1)


def unpacked(x):
    return jnp.concatenate([x[:, :64], x[:, 64:]], axis=0)


def turned_z(place_ref, z):
    az = lax.rem(place_ref[2] + (NZ - z), NZ)
    return pl.ds(pl.multiple_of(az * 128, 128), 128)


def mix_kernel(c_ref, h_ref, mine_ref, away_ref, out_ref):
    c = c_ref[0]
    both = jnp.concatenate(
        [h_ref[y, :16, :256] for y in range(NY)] + [h_ref[y, :16, 256:] for y in range(NY)], axis=0
    )
    lane = lax.broadcasted_iota(jnp.int32, (64, 128), 1)
    for z in range(NZ):
        res = []
        for w in (mine_ref, away_ref):
            r = jnp.dot(both, w[z, :256, :], preferred_element_type=F32)
            top, low = r[:64], r[64:]
            res.append((top + pltpu.roll(low, 64, 1), pltpu.roll(top, 64, 1) + low))
        first = jnp.where(c == 0, res[0][0], res[1][0])
        second = jnp.where(c == 0, res[1][1], res[0][1])
        tile = jnp.where(lane < 64, first, second).astype(BF16)
        for y in range(NY):
            out_ref[y, :, turned_z(c_ref, z)] = tile[y * 16 : (y + 1) * 16]


VMEM = pl.BlockSpec(memory_space=pltpu.VMEM)
SMEM = pl.BlockSpec(memory_space=pltpu.SMEM)


def mix(c, heads, mine, away):
    return pl.pallas_call(
        mix_kernel,
        out_shape=jax.ShapeDtypeStruct((NY, 16, 1024), BF16),
        in_specs=[SMEM, VMEM, VMEM, VMEM],
        out_specs=VMEM,
        cost_estimate=pl.CostEstimate(
            flops=2 * 128 * 256 * 128 * 16, bytes_accessed=2 << 20, transcendentals=0
        ),
        name="mix",
    )(c, heads, mine, away)


def settle_kernel(
    c_ref, got_ref, tok_ref, gain_ref, mix_ref, spread_ref,
    hid_ref, gate_ref, send_ref, n0_ref, n1_ref, n2_ref, n3_ref, norm_ref,
):
    square = jnp.zeros((16, 1), F32)
    dot = jnp.zeros((16, 1), F32)
    for y in range(NY):
        total = got_ref[y, 0].astype(F32)
        for x in range(1, NX):
            total += got_ref[y, x].astype(F32)
        total = total.astype(BF16).astype(F32)
        for z in range(NZ):
            at = (z * NY + y) * 128
            cols = slice(at, at + 128)
            hid = (tok_ref[:, cols].astype(F32) + total[:, z * 128 : (z + 1) * 128]).astype(BF16)
            hid_ref[:, cols] = hid
            wide = hid.astype(F32)
            square += jnp.sum(wide * wide, axis=1, keepdims=True)
            dot += jnp.sum(wide * gain_ref[:, cols] * mix_ref[:, cols], axis=1, keepdims=True)
    inverse = lax.rsqrt(square / D + EPSILON)
    gate_ref[...] = jnp.broadcast_to(1.0 / (1.0 + jnp.exp(-(inverse * dot))), (16, 128))
    spread = spread_ref[...]
    for at in range(0, D, 512):
        cols = slice(at, at + 512)
        norm = (hid_ref[:, cols].astype(F32) * inverse * gain_ref[:, cols]).astype(BF16)
        norm_ref[:, cols] = norm
        send_ref[:, cols] = jnp.dot(spread, norm, preferred_element_type=F32).astype(BF16)
    for s, out in enumerate((n0_ref, n1_ref, n2_ref, n3_ref)):
        to = lax.rem(c_ref[1] + s, NY)
        for z in range(NZ):
            at = pl.multiple_of((z * NY + to) * 128, 128)
            out[:, z * 128 : (z + 1) * 128] = norm_ref[:, pl.ds(at, 128)]


def settle(c, got, tok, gain, mix_row, spread):
    part = jax.ShapeDtypeStruct((16, 1024), BF16)
    return pl.pallas_call(
        settle_kernel,
        out_shape=(
            jax.ShapeDtypeStruct((16, D), BF16),
            jax.ShapeDtypeStruct((16, 128), F32),
            jax.ShapeDtypeStruct((128, D), BF16),
            part, part, part, part,
        ),
        in_specs=[SMEM] + [VMEM] * 5,
        out_specs=(VMEM,) * 7,
        scratch_shapes=[pltpu.VMEM((16, D), BF16)],
        cost_estimate=pl.CostEstimate(
            flops=2 * 128 * 128 * 4096, bytes_accessed=3 << 20, transcendentals=0
        ),
        name="settle",
    )(c, got, tok, gain, mix_row, spread)


def dense_kernel(c_ref, x0, x1, x2, x3, mine_ref, away_ref, o0, o1, o2, o3):
    c = c_ref[0]
    acc = [jnp.zeros((64, 128), F32) for _ in range(4)]
    for z in range(NZ):
        cols = turned_z(c_ref, z)
        x = jnp.concatenate([r[:, cols] for r in (x0, x1, x2, x3)], axis=0)
        own = jnp.where(c == 0, x[:, :64], x[:, 64:])
        off = jnp.where(c == 0, x[:, 64:], x[:, :64])
        for j in range(4):
            rows = slice(272 + j * 64, 336 + j * 64)
            acc[j] += jnp.dot(own, mine_ref[z, rows, :], preferred_element_type=F32)
            acc[j] += jnp.dot(off, away_ref[z, rows, :], preferred_element_type=F32)
    for s, out in enumerate((o0, o1, o2, o3)):
        for j in range(4):
            out[:, j * 128 : (j + 1) * 128] = acc[j][s * 16 : (s + 1) * 16].astype(BF16)


def dense_products(c, xs, mine, away):
    part = jax.ShapeDtypeStruct((16, 512), BF16)
    return pl.pallas_call(
        dense_kernel,
        out_shape=(part,) * 4,
        in_specs=[SMEM] + [VMEM] * 6,
        out_specs=(VMEM,) * 4,
        cost_estimate=pl.CostEstimate(
            flops=2 * 64 * 1024 * 512, bytes_accessed=2 << 20, transcendentals=0
        ),
        name="dense_products",
    )(c, *xs, mine, away)


def dense_down_kernel(c_ref, x0, x1, x2, x3, mine_ref, away_ref, o0, o1, o2, o3):
    c = c_ref[0]
    xs = (x0, x1, x2, x3)
    both = jnp.concatenate([r[:, :128] for r in xs] + [r[:, 128:] for r in xs], axis=0)
    lane = lax.broadcasted_iota(jnp.int32, (64, 128), 1)
    for z in range(NZ):
        res = []
        for w in (mine_ref, away_ref):
            r = jnp.dot(both, w[z, 528:656, :], preferred_element_type=F32)
            top, low = r[:64], r[64:]
            res.append((top + pltpu.roll(low, 64, 1), pltpu.roll(top, 64, 1) + low))
        first = jnp.where(c == 0, res[0][0], res[1][0])
        second = jnp.where(c == 0, res[1][1], res[0][1])
        tile = jnp.where(lane < 64, first, second).astype(BF16)
        for s, out in enumerate((o0, o1, o2, o3)):
            out[:, turned_z(c_ref, z)] = tile[s * 16 : (s + 1) * 16]


def dense_down(c, xs, mine, away):
    part = jax.ShapeDtypeStruct((16, 1024), BF16)
    return pl.pallas_call(
        dense_down_kernel,
        out_shape=(part,) * 4,
        in_specs=[SMEM] + [VMEM] * 6,
        out_specs=(VMEM,) * 4,
        cost_estimate=pl.CostEstimate(
            flops=2 * 64 * 1024 * 512, bytes_accessed=1 << 20, transcendentals=0
        ),
        name="dense_down",
    )(c, *xs, mine, away)


def half_rows(tile):
    lane = lax.broadcasted_iota(jnp.int32, (8, 128), 1)
    wide = tile.astype(F32)
    turn = pltpu.roll(wide, 64, 1)
    return (
        jnp.where(lane < 64, wide[:8], turn[8:]),
        jnp.where(lane < 64, turn[:8], wide[8:]),
    )


def down_kernel(c_ref, h_ref, w_ref, hid_ref, d0, d1, d2, d3, out_ref):
    res = jnp.dot(h_ref[...], w_ref[...], preferred_element_type=F32)
    lane = lax.broadcasted_iota(jnp.int32, (64, 128), 1)
    for p in range(8):
        cols = slice(p * 128, (p + 1) * 128)
        top, low = res[:64, cols], res[64:, cols]
        out_ref[2 * p, :64] = jnp.where(lane < 64, top, pltpu.roll(low, 64, 1)).astype(BF16)
        out_ref[2 * p + 1, :64] = jnp.where(lane < 64, pltpu.roll(top, 64, 1), low).astype(BF16)
    for zl in range(2):
        for s, d in enumerate((d0, d1, d2, d3)):
            at = zl * NY + lax.rem(c_ref[1] + s, NY)
            hid = half_rows(hid_ref[:, pl.ds(pl.multiple_of(at * 128, 128), 128)])
            den = half_rows(d[:, zl * 128 : (zl + 1) * 128])
            for k in range(2):
                out_ref[2 * at + k, 64:] = jnp.concatenate([hid[k], den[k]], axis=0).astype(BF16)


def down_for_all(c, expert_hidden, w, hidden, downs):
    return pl.pallas_call(
        down_kernel,
        grid=(4,),
        out_shape=jax.ShapeDtypeStruct((64, 80, 128), BF16),
        in_specs=[
            SMEM,
            pl.BlockSpec((128, 256), lambda i: (0, 0)),
            pl.BlockSpec((256, 1024), lambda i: (0, i)),
            pl.BlockSpec((16, 1024), lambda i: (0, i)),
        ]
        + [pl.BlockSpec((16, 256), lambda i: (0, i))] * 4,
        out_specs=pl.BlockSpec((16, 80, 128), lambda i: (i, 0, 0)),
        cost_estimate=pl.CostEstimate(
            flops=2 * 128 * 256 * 4096, bytes_accessed=4 << 20, transcendentals=0
        ),
        name="down",
    )(c, expert_hidden, w, hidden, *downs)


def project_kernel(kept, c_ref, tok_ref, gain_ref, q_ref, k_ref, v_ref, o_ref, i_ref, f_ref, out, all_ref, x_ref):
    core = c_ref[0] if kept else 1 - c_ref[0]
    gain = gain_ref[...].astype(F32)
    lane = lax.broadcasted_iota(jnp.int32, (128, 128), 1)
    all_ref[...] = jnp.transpose(tok_ref[...])
    gate_rows = jnp.concatenate(
        [jnp.zeros((64, 64), BF16), i_ref[...], f_ref[...], jnp.zeros((56, 64), BF16)], axis=0
    )
    for y in range(NY):
        for z in range(NZ):
            at = pl.multiple_of(((z * NY + y) * NC + core) * 16, 16)
            x_ref[z * 16 : (z + 1) * 16, :] = all_ref[pl.ds(at, 16), :]
        wide = x_ref[...].astype(F32)
        scaled = (wide * gain).astype(BF16)
        rows = slice(y * 128, (y + 1) * 128)
        at = 0
        for w in (q_ref, k_ref, v_ref, o_ref):
            n = w.shape[1]
            res = jnp.dot(scaled, w[...], preferred_element_type=F32)
            out[rows, at : at + n] = res.astype(out.dtype)
            at += n
        gates = lax.dot_general(
            scaled, gate_rows, (((1,), (1,)), ((), ())), preferred_element_type=F32
        )
        square = jnp.sum(wide * wide, axis=1, keepdims=True)
        both = jnp.concatenate([wide, jnp.zeros((128, 64), F32)], axis=1)
        last = jnp.where(lane < 64, both, jnp.where(lane == 72, square, gates))
        out[rows, 1536:1664] = last.astype(out.dtype)


def project(kept, *args):
    return pl.pallas_call(
        functools.partial(project_kernel, kept),
        out_shape=jax.ShapeDtypeStruct((512, 1664), F32 if kept else BF16),
        in_specs=[SMEM] + [VMEM] * 8,
        out_specs=VMEM,
        scratch_shapes=[pltpu.VMEM((1024, 64), BF16), pltpu.VMEM((128, 64), BF16)],
        cost_estimate=pl.CostEstimate(
            flops=2 * 512 * 256 * 1664, bytes_accessed=3 << 20, transcendentals=0
        ),
        name="project_kept" if kept else "project_away",
    )(*args)


def fold_core_kernel(c_ref, kept_ref, got_ref, out_ref):
    c = c_ref[0]
    lane = lax.broadcasted_iota(jnp.int32, (128, 128), 1)
    for y in range(NY):
        rows = slice(y * 128, (y + 1) * 128)
        kept, got = kept_ref[rows, :], got_ref[rows, :].astype(F32)
        out_ref[y, :, :1664] = (kept + got).astype(BF16)
        a, b = kept[:, 1536:], got[:, 1536:]
        first = jnp.where(c == 0, a, b)
        second = jnp.where(c == 0, b, a)
        out_ref[y, :, 1664:] = jnp.where(lane < 64, first, pltpu.roll(second, 64, 1)).astype(BF16)


def fold_core(c, kept, got):
    return pl.pallas_call(
        fold_core_kernel,
        out_shape=jax.ShapeDtypeStruct((NY, 128, 1792), BF16),
        in_specs=[SMEM, VMEM, VMEM],
        out_specs=VMEM,
        cost_estimate=pl.CostEstimate(
            flops=1 << 20, bytes_accessed=6 << 20, transcendentals=0
        ),
        name="fold_core",
    )(c, kept, got)


def fold_y_kernel(in_ref, out_ref):
    for z in range(NZ):
        rows = slice(z * 16, (z + 1) * 16)
        total = in_ref[0, rows, :1664].astype(F32)
        for y in range(1, NY):
            total += in_ref[y, rows, :1664].astype(F32)
        out_ref[z, :, :1664] = total.astype(BF16)
        for y in range(NY):
            at = 1664 + y * 128
            out_ref[z, :, at : at + 128] = in_ref[y, rows, 1664:]


def fold_y(x):
    return pl.pallas_call(
        fold_y_kernel,
        out_shape=jax.ShapeDtypeStruct((NZ, 16, 2176), BF16),
        in_specs=[VMEM],
        out_specs=VMEM,
        cost_estimate=pl.CostEstimate(
            flops=1 << 20, bytes_accessed=3 << 20, transcendentals=0
        ),
        name="fold_y",
    )(x)


def recur_kernel(
    in_ref, ib_ref, fb_ref, hg_ref, sm_ref, sn_ref, mx_ref,
    heads_ref, tok_ref, nm_ref, nn_ref, nx_ref,
    kt_ref, qt_ref, car_ref, flo_ref, val_ref, out_ref, num_ref,
):
    g = pl.program_id(0)

    @pl.when(g == 0)
    def _():
        total = in_ref[0, :, :1664].astype(F32)
        for z in range(1, NZ):
            total += in_ref[z, :, :1664].astype(F32)
        for z in range(NZ):
            for y in range(NY):
                at, src = (z * NY + y) * 128, 1664 + y * 128
                tok_ref[:, at : at + 128] = in_ref[z, :, src : src + 128]
        inverse = lax.rsqrt(total[:, 1608:1609] / D + EPSILON)
        total = total * inverse
        q = total[:, :256].astype(BF16).astype(F32) * 0.125
        k = total[:, 256:512].astype(BF16).astype(F32)
        for h in range(4):
            cols = slice(512 + h * 128, 640 + h * 128)
            val_ref[h] = total[:, cols].astype(BF16).astype(F32)
        out_ref[...] = total[:, 1024:1536].astype(BF16).astype(F32)
        in_log = SOFT_CAP * jnp.tanh((total[:, 1600:1604] + ib_ref[...]) / SOFT_CAP)
        f = SOFT_CAP * jnp.tanh((total[:, 1604:1608] + fb_ref[...]) / SOFT_CAP)
        forget_log = jnp.minimum(f, 0.0) - jnp.log1p(jnp.exp(-jnp.abs(f)))
        kept = forget_log + mx_ref[...]
        top = jnp.maximum(kept, in_log)
        nx_ref[...] = top
        carried = jnp.exp(kept - top)
        fresh = jnp.exp(in_log - top)
        least = jnp.exp(-top)
        scaled = []
        for h in range(4):
            cols = slice(h * 64, (h + 1) * 64)
            fk = fresh[:, h : h + 1] * k[:, cols]
            scaled.append(fk)
            norm = carried[:, h : h + 1] * sn_ref[:, h, :] + fk
            nn_ref[:, h, :] = norm
            den = jnp.abs(jnp.sum(norm * q[:, cols], axis=1, keepdims=True))
            flo_ref[h] = jnp.broadcast_to(jnp.maximum(den, least[:, h : h + 1]), (16, 128))
            car_ref[h] = jnp.broadcast_to(carried[:, h : h + 1], (16, 128))
        kt = jnp.transpose(jnp.concatenate(scaled, axis=1))
        qt = jnp.transpose(q)
        for i in range(4):
            kt_ref[i] = kt[:, i * 4 : (i + 1) * 4]
            qt_ref[i] = qt[:, i * 4 : (i + 1) * 4]

    for i in range(4):
        b = g * 4 + i
        for h in range(4):
            rows = slice(h * 64, (h + 1) * 64)
            new = (
                car_ref[h, pl.ds(b, 1), :] * sm_ref[i, h]
                + kt_ref[g, rows, i : i + 1] * val_ref[h, pl.ds(b, 1), :]
            )
            nm_ref[i, h] = new
            num_ref[h, pl.ds(b, 1), :] = jnp.sum(
                new * qt_ref[g, rows, i : i + 1], axis=0, keepdims=True
            )

    @pl.when(g == 3)
    def _():
        for h in range(4):
            cols = slice(h * 128, (h + 1) * 128)
            read = num_ref[h] / flo_ref[h]
            mean = jnp.mean(read * read, axis=1, keepdims=True)
            gate = 1.0 / (1.0 + jnp.exp(-out_ref[:, cols]))
            scaled = read * lax.rsqrt(mean + EPSILON) * hg_ref[:, cols].astype(F32)
            heads_ref[:, cols] = (scaled * gate).astype(BF16)


def recur(x, igate_bias, fgate_bias, head_gain, state_matrix, state_norm, state_max):
    whole = lambda *shape: pl.BlockSpec(shape, lambda g: (0,) * len(shape))
    block = pl.BlockSpec((4, 4, 64, 128), lambda g: (g, 0, 0, 0))
    return pl.pallas_call(
        recur_kernel,
        grid=(4,),
        out_shape=(
            jax.ShapeDtypeStruct((16, 512), BF16),
            jax.ShapeDtypeStruct((16, D), BF16),
            jax.ShapeDtypeStruct((16, 4, 64, 128), F32),
            jax.ShapeDtypeStruct((16, 4, 64), F32),
            jax.ShapeDtypeStruct((16, 4), F32),
        ),
        in_specs=[
            whole(NZ, 16, 2176), whole(1, 4), whole(1, 4), whole(1, 512),
            block, whole(16, 4, 64), whole(16, 4),
        ],
        out_specs=(whole(16, 512), whole(16, D), block, whole(16, 4, 64), whole(16, 4)),
        scratch_shapes=[
            pltpu.VMEM((4, 256, 4), F32),
            pltpu.VMEM((4, 256, 4), F32),
            pltpu.VMEM((4, 16, 128), F32),
            pltpu.VMEM((4, 16, 128), F32),
            pltpu.VMEM((4, 16, 128), F32),
            pltpu.VMEM((16, 512), F32),
            pltpu.VMEM((4, 16, 128), F32),
        ],
        cost_estimate=pl.CostEstimate(
            flops=8 << 20, bytes_accessed=5 << 20, transcendentals=1 << 14
        ),
        name="recur",
    )(x, igate_bias[None], fgate_bias[None], head_gain[None], state_matrix, state_norm, state_max)


def slot_ranks(routes):
    chosen = (routes[:, :, None] == jnp.arange(64, dtype=jnp.int32)[None, None, :]).astype(F32)
    per_row = jnp.sum(chosen, axis=1).reshape(64, 16, 64)
    lower = jnp.tril(jnp.ones((16, 16), F32), -1)
    earlier = jnp.einsum("rs,gse->gre", lower, per_row).reshape(1024, 64)
    return jnp.sum(chosen * earlier[:, None, :], axis=2).astype(jnp.int32)


def layer(
    tokens,
    mix_gain,
    w_query,
    w_key,
    w_value,
    w_outgate,
    w_igate,
    w_fgate,
    igate_bias,
    fgate_bias,
    head_gain,
    w_mixout,
    state_matrix,
    state_norm,
    state_max,
    ffn_gain,
    dense_mix,
    w_dense_gate,
    w_dense_up,
    w_dense_down,
    routes,
    route_weights,
    w_exp_gate,
    w_exp_up,
    w_exp_down,
):
    me = lax.axis_index(EP)
    c = lax.axis_index("c")
    y, z = lax.axis_index("y"), lax.axis_index("z")
    c_ref = jnp.stack([c, y, z]).astype(jnp.int32)
    piece = jnp.concatenate(
        [
            packed(w_mixout),
            jnp.stack([jnp.pad(ffn_gain, (0, 64)), jnp.pad(dense_mix, (0, 64))]),
            jnp.zeros((14, 128), BF16),
            w_dense_gate[:, :128],
            w_dense_gate[:, 128:],
            w_dense_up[:, :128],
            w_dense_up[:, 128:],
            packed(w_dense_down),
        ],
        axis=0,
    )
    operands = (
        c_ref, tokens.T, mix_gain[None], w_query, w_key, w_value, w_outgate, w_igate.T, w_fgate.T
    )
    away = project(False, *operands)
    got = other_core(away)
    kept = project(True, *operands)
    folded = fold_core(c_ref, kept, got)
    folded = exchanged(folded, "y")
    folded = fold_y(folded)
    folded = exchanged(folded, "z")
    heads_out, tok, new_matrix, new_norm, new_max = recur(
        folded, igate_bias, fgate_bias, head_gain, state_matrix, state_norm, state_max
    )
    mine, away = gathered_z(piece)
    extra = jnp.stack([mine[:, 256:258, :64], away[:, 256:258, :64]])
    extra = jnp.where(c == 0, extra, extra[::-1])[:, (z - jnp.arange(NZ)) % NZ]
    extra = extra.transpose(2, 1, 0, 3).reshape(4, 512)
    heads = jnp.concatenate([heads_out, extra, jnp.zeros((4, 512), BF16)], axis=0)
    heads = to_all(heads, "y")
    vectors = heads[:, 16:20].reshape(NY, 2, NZ, 128).transpose(1, 2, 0, 3).reshape(2, 1, D)
    vectors = vectors.astype(F32)
    partial = mix(c_ref, heads, mine, away)
    copies = jnp.broadcast_to(partial[:, None], (NY, NX, 16, 1024)).reshape(16, 16, 1024)
    got = exchanged(copies, ("y", "x")).reshape(NY, NX, 16, 1024)
    ranks = slot_ranks(routes)
    target = routes * 2 + ranks
    own_target = lax.dynamic_slice(target, (me * 16, 0), (16, 4))
    slots = jnp.arange(128)
    spread = jnp.any(own_target[:, :, None] == slots[None, None, :], axis=1).T.astype(BF16)
    hidden, dense_gate, send, *sides = settle(c_ref, got, tok, vectors[0], vectors[1], spread)
    arrived = exchanged(send.reshape(64, 2, D), EP).reshape(128, D)
    xs = [sides[0]] + [
        lax.ppermute(sides[s], "y", [(i, (i + s) % NY) for i in range(NY)]) for s in (1, 2, 3)
    ]
    sums = dense_products(c_ref, xs, mine, away)
    parts = [sums[0]] + [
        lax.ppermute(sums[s], "y", [(i, (i - s) % NY) for i in range(NY)]) for s in (1, 2, 3)
    ]
    dense_sum = sum(p.astype(F32) for p in parts)
    dense_hidden = (
        jax.nn.silu(dense_sum[:, :256]) * dense_sum[:, 256:] * dense_gate[:, :1]
    ).astype(BF16)
    units = [dense_hidden] + [
        lax.ppermute(dense_hidden, "y", [(i, (i + s) % NY) for i in range(NY)])
        for s in (1, 2, 3)
    ]
    downs = dense_down(c_ref, units, mine, away)
    downs = [downs[0]] + [
        lax.ppermute(downs[s], "y", [(i, (i - s) % NY) for i in range(NY)]) for s in (1, 2, 3)
    ]
    named = routes == me
    slot_of = jnp.sum(jnp.where(named, (jnp.arange(1024) // 16)[:, None] * 2 + ranks, 0), axis=1)
    slot_weight = jnp.sum(jnp.where(named, route_weights, 0.0), axis=1)
    slot_hit = (slot_of[:, None] == slots[None, :]) & jnp.any(named, axis=1)[:, None]
    weight = jnp.sum(jnp.where(slot_hit, slot_weight[:, None], 0.0), axis=0)
    gate_part = jnp.dot(arrived, w_exp_gate[0], preferred_element_type=F32)
    up_part = jnp.dot(arrived, w_exp_up[0], preferred_element_type=F32)
    expert_hidden = (jax.nn.silu(gate_part) * up_part * weight[:, None]).astype(BF16)
    returned = down_for_all(c_ref, expert_hidden, w_exp_down[0], hidden, downs)
    returned = exchanged(returned, EP)
    rows = returned[:, 64:].reshape(64, 2, 8, 2, 64).transpose(1, 0, 3, 2, 4).reshape(2, 1024, 64)
    hidden_cols, dense_rows = rows[0], rows[1]
    returned = returned[:, :64]
    local = routes * 16 + 2 * ((jnp.arange(1024) // 16)[:, None] % 8) + ranks
    pick = jnp.any(local[:, :, None] == jnp.arange(1024)[None, None, :], axis=1).astype(BF16)
    pick = pick.reshape(2, 4, 128, 1024)
    source = returned.reshape(64, 4, 16, 128).transpose(1, 0, 2, 3).reshape(4, 1024, 128)
    halves = jnp.einsum("hgmk,gkn->hgmn", pick, source, preferred_element_type=F32)
    routed = jnp.concatenate(
        [halves[0, :, :, :64].reshape(512, 64), halves[1, :, :, 64:].reshape(512, 64)], axis=0
    )
    branch = packed((routed + dense_rows.astype(F32)).astype(BF16))
    branch = unpacked(over_x(branch))
    layer_out = (hidden_cols.astype(F32) + branch).astype(BF16)
    return (layer_out, new_matrix, new_norm, new_max)


def solution(mesh):
    return jax.shard_map(
        layer,
        mesh=Mesh(mesh.devices.reshape(NZ, NY, NC, NX), ("z", "y", "c", "x")),
        in_specs=(
            P(None, EP),
            P(EP),
            P(EP, "x"),
            P(EP, "x"),
            P(EP, "x"),
            P(EP, "x"),
            P(EP, "x"),
            P(EP, "x"),
            P("x"),
            P("x"),
            P("x"),
            P("x", EP),
            P(EP, "x", None, None),
            P(EP, "x", None),
            P(EP, "x"),
            P(EP),
            P(EP),
            P(EP, "x"),
            P(EP, "x"),
            P("x", EP),
            P(),
            P(),
            P(EP, None, "x"),
            P(EP, None, "x"),
            P(EP, "x", None),
        ),
        out_specs=(P(None, EP), P(EP, "x", None, None), P(EP, "x", None), P(EP, "x")),
        check_vma=False,
    )
```

time: 397 us -> 264 us (0.66)
  waiting for transfers between devices: 174 us -> 93.1 us
  Pallas kernels: 0 us -> 37.7 us
  other arithmetic: 46.4 us -> 13 us
  local copies, waits for them, and re-layouts: 60.8 us -> 32 us
  matrix products: 21.9 us -> 4.42 us
  starting transfers between devices: 64.1 us -> 80.2 us
  between operations: 14.5 us -> 1.31 us
  blocking collectives: 12.4 us -> 0 us
    all_to_all x9 -> x7, waiting for transfers between devices: 125 us -> 63.8 us  [exchanged(): return lax.all_to_all(x, axis, split_axis=0, concat_axis=0, tiled=True)]
    all_gather x1 -> x0, waiting for transfers between devices: 49.1 us -> none  [in_one_piece(): lax.all_gather(both, axis, axis=dim, tiled=True)]
    pallas_call x0 -> x11, Pallas kernels: none -> 37.7 us  [the longest x2 6.38 us: project(): pl.pallas_call(functools.partial(project_kernel, kept), out_shape=jax.Sha...]
    ppermute x0 -> x21, starting transfers between devices: none -> 36.9 us  [the longest x7 18.7 us: gathered_z(): lax.ppermute(x, 'z', [(i, (i + s) % NZ) for i in range(NZ)])]
    ppermute x0 -> x21, waiting for transfers between devices: none -> 29.3 us  [the longest x7 20.2 us: gathered_z(): lax.ppermute(x, 'z', [(i, (i + s) % NZ) for i in range(NZ)])]
    unnamed x1 -> x0, other arithmetic: 23.4 us -> none
    all_to_all x9 -> x7, starting transfers between devices: 64.1 us -> 43.3 us  [exchanged(): return lax.all_to_all(x, axis, split_axis=0, concat_axis=0, tiled=True)]
    dot_general x12 -> x4, matrix products: 21.9 us -> 4.42 us  [the longest x1 2.02 us: slot_ranks(): earlier = jnp.einsum('rs,gse->gre', lower, per_row).reshape(1024, 64)]
  transfers between devices with their start and end apart: 10 -> 28, of which waited for: 8 -> 15; matrix products, arithmetic and copies ran while one was open for 21% -> 12% of each run, Pallas kernels for 0% -> 6%
where the time goes in v1:
time: 264 us; the launch traced here: 262 us
  waiting for transfers between devices  93.1 us (35%)
  starting transfers between devices  80.2 us (30%)
  Pallas kernels  37.7 us (14%)
  local copies, waits for them, and re-layouts  32 us (12%)
  other arithmetic  13 us (5%)
  matrix products  4.42 us (2%)
    all_to_all x7, waiting for transfers between devices, exchanged(): return lax.all_to_all(x, axis, split_axis=0, concat_axis=0, tiled=True)  63.8 us
    all_to_all x7, starting transfers between devices, exchanged(): return lax.all_to_all(x, axis, split_axis=0, concat_axis=0, tiled=True)  43.3 us
    ppermute x7, waiting for transfers between devices, gathered_z(): lax.ppermute(x, 'z', [(i, (i + s) % NZ) for i in range(NZ)])  20.2 us
    ppermute x7, starting transfers between devices, gathered_z(): lax.ppermute(x, 'z', [(i, (i + s) % NZ) for i in range(NZ)])  18.7 us
    unnamed x91, local copies, waits for them, and re-layouts  9.34 us
    pallas_call x2, Pallas kernels, project(): pl.pallas_call(functools.partial(project_kernel, kept), out_shape=jax.Sha...  6.38 us
    pallas_call x1, Pallas kernels, recur(): pl.pallas_call(recur_kernel, grid=(4,), out_shape=(jax.ShapeDtypeStruct((...  5.57 us
  transfers between devices with their start and end apart: 28, of which 15 were waited for; matrix products, arithmetic and copies ran while one was open for 12% of the time, Pallas kernels for 6%

profile of v1, /device:TPU:8, one launch (start us, length us, event | category | flops | bytes accessed | tf_op | source)
XLA Modules:
  0.0 261.8 jit_solution(2761828266942233959)
XLA Ops:
  5.3 3.4 %project_kept.1.kept_ref = f32[512,1664]{1,0:T(8,128)} custom-call(s32[3]{0:T(128)} %pad_add_fusion.c_ref, bf16[64,1024]{1,0:T(8,128)(2,1)} %bitcast.95, bf16[1,64]{1,0:T(2,128)(2,1)} %bitcast.110, bf16[64,256]{1,0:T(8,128)(2,1)} %q_ref.3, bf16[64,256]{1,0:T(8,128)(2,1)} %k_ref.3, bf16[64,512]{1,0:T(8,128)(2,1)} %v_ref.3, bf16[64,512]{1,0:T(8,128)(2,1)} %o_ref.3, ...), custom_call_target="tpu_custom_call" | custom-call | flops 436207616 | bytes 3145728 | tf_op jit(solution)/shard_map/project_kept/pallas_call | solution.py:303
  8.9 4.3 %fold_core.1 = bf16[4,128,1792]{2,1,0:T(8,128)(2,1)} custom-call(s32[3]{0:T(128)} %pad_add_fusion.c_ref, f32[512,1664]{1,0:T(8,128)} %project_kept.1.kept_ref, bf16[512,1664]{1,0:T(8,128)(2,1)} %collective-permute-done.got_ref), custom_call_target="tpu_custom_call" | custom-call | flops 1048576 | bytes 6291456 | tf_op jit(solution)/shard_map/fold_core/pallas_call | solution.py:330
  13.2 6.7 %all-to-all-start = ((bf16[4,128,1792]{2,1,0:T(8,128)(2,1)}), bf16[4,128,1792]{2,1,0:T(8,128)(2,1)}, u32[]{:S(2)}, u32[]{:S(2)}) async-start(bf16[4,128,1792]{2,1,0:T(8,128)(2,1)} %fold_core.1), calls=%async_computation | async-start | bytes 3670016 | tf_op jit(solution)/shard_map/all_to_all | solution.py:23
  20.9 3.3 %collective-permute-start.2 = (bf16[656,128]{1,0:T(8,128)(2,1)S(1)}, bf16[656,128]{1,0:T(8,128)(2,1)S(1)}, u32[]{:S(2)}, u32[]{:S(2)}) collective-permute-start(bf16[656,128]{1,0:T(8,128)(2,1)S(1)} %concatenate.23.refs_0_), channel_id=1, source_target_pairs={{0,64},{32,96},{64,128},{96,160},{128,192},{160,224},{192,0},{224,... | collective-permute-start | bytes 503816 | tf_op jit(solution)/shard_map/ppermute | solution.py:41
  24.2 4.0 %collective-permute-start.3 = (bf16[656,128]{1,0:T(8,128)(2,1)S(1)}, bf16[656,128]{1,0:T(8,128)(2,1)S(1)}, u32[]{:S(2)}, u32[]{:S(2)}) collective-permute-start(bf16[656,128]{1,0:T(8,128)(2,1)S(1)} %concatenate.23.refs_0_), channel_id=1, source_target_pairs={{0,96},{32,128},{64,160},{96,192},{128,224},{160,0},{192,32},{224,... | collective-permute-start | bytes 503816 | tf_op jit(solution)/shard_map/ppermute | solution.py:41
  28.7 5.0 %collective-permute-start.5 = (bf16[656,128]{1,0:T(8,128)(2,1)S(1)}, bf16[656,128]{1,0:T(8,128)(2,1)S(1)}, u32[]{:S(2)}, u32[]{:S(2)}) collective-permute-start(bf16[656,128]{1,0:T(8,128)(2,1)S(1)} %concatenate.23.refs_0_), channel_id=1, source_target_pairs={{0,160},{32,192},{64,224},{96,0},{128,32},{160,64},{192,96},{224,1... | collective-permute-start | bytes 503816 | tf_op jit(solution)/shard_map/ppermute | solution.py:41
  36.3 3.4 %collective-permute-done.2.refs_2_ = bf16[656,128]{1,0:T(8,128)(2,1)S(1)} collective-permute-done((bf16[656,128]{1,0:T(8,128)(2,1)S(1)}, bf16[656,128]{1,0:T(8,128)(2,1)S(1)}, u32[]{:S(2)}, u32[]{:S(2)}) %collective-permute-start.2) | collective-permute-done | bytes 167968 | tf_op jit(solution)/shard_map/ppermute | solution.py:41
  42.6 8.5 %collective-permute-done.3.refs_3_ = bf16[656,128]{1,0:T(8,128)(2,1)S(1)} collective-permute-done((bf16[656,128]{1,0:T(8,128)(2,1)S(1)}, bf16[656,128]{1,0:T(8,128)(2,1)S(1)}, u32[]{:S(2)}, u32[]{:S(2)}) %collective-permute-start.3) | collective-permute-done | bytes 167968 | tf_op jit(solution)/shard_map/ppermute | solution.py:41
  53.2 5.0 %collective-permute-done.6.refs_6_ = bf16[656,128]{1,0:T(8,128)(2,1)S(1)} collective-permute-done((bf16[656,128]{1,0:T(8,128)(2,1)S(1)}, bf16[656,128]{1,0:T(8,128)(2,1)S(1)}, u32[]{:S(2)}, u32[]{:S(2)}) %collective-permute-start.6) | collective-permute-done | bytes 167968 | tf_op jit(solution)/shard_map/ppermute | solution.py:41
  78.9 5.4 %all-to-all-start.1 = ((bf16[8,16,2176]{2,1,0:T(8,128)(2,1)}), bf16[8,16,2176]{2,1,0:T(8,128)(2,1)}, u32[]{:S(2)}, u32[]{:S(2)}) async-start(bf16[8,16,2176]{2,1,0:T(8,128)(2,1)} %fold_y.1), calls=%async_computation.1 | async-start | bytes 1114112 | tf_op jit(solution)/shard_map/all_to_all | solution.py:23
  85.8 17.5 %all-to-all-done.1.in_ref = bf16[8,16,2176]{2,1,0:T(8,128)(2,1)} async-done(((bf16[8,16,2176]{2,1,0:T(8,128)(2,1)}), bf16[8,16,2176]{2,1,0:T(8,128)(2,1)}, u32[]{:S(2)}, u32[]{:S(2)}) %all-to-all-start.1) | async-done | bytes 557088 | tf_op jit(solution)/shard_map/all_to_all | solution.py:23
  103.3 5.6 %recur.1 = (bf16[16,512]{1,0:T(8,128)(2,1)}, bf16[16,4096]{1,0:T(8,128)(2,1)}, f32[16,4,64,128]{3,2,1,0:T(8,128)}, f32[16,4,64]{2,1,0:T(4,128)}, f32[16,4]{1,0:T(8,128)}) custom-call(bf16[8,16,2176]{2,1,0:T(8,128)(2,1)} %all-to-all-done.1.in_ref, f32[1,4]{1,0:T(1,128)} %bitcast.111, f32[1,4]{1,0:T(1,128)} %bitcast.112, ...), custom_call_target="tpu_custom_call" | custom-call | flops 8388608 | bytes 5242880 | tf_op jit(solution)/shard_map/recur/pallas_call | solution.py:443
  110.3 4.8 %all-to-all-start.2 = ((bf16[4,24,512]{2,1,0:T(8,128)(2,1)}), bf16[4,24,512]{2,1,0:T(8,128)(2,1)S(1)}, u32[]{:S(2)}, u32[]{:S(2)}) async-start(bf16[4,24,512]{2,1,0:T(8,128)(2,1)} %broadcast_in_dim.77), calls=%async_computation.2 | async-start | bytes 196608 | tf_op jit(solution)/shard_map/all_to_all | solution.py:23
  124.8 6.4 %all-to-all-start.3 = ((bf16[16,16,1024]{2,1,0:T(8,128)(2,1)}), bf16[16,16,1024]{2,1,0:T(8,128)(2,1)S(1)}, u32[]{:S(2)}, u32[]{:S(2)}) async-start(bf16[16,16,1024]{2,1,0:T(8,128)(2,1)} %bitcast.15), calls=%async_computation.3 | async-start | bytes 1048576 | tf_op jit(solution)/shard_map/all_to_all | solution.py:23
  134.1 5.4 %all-to-all-done.3 = bf16[16,16,1024]{2,1,0:T(8,128)(2,1)S(1)} async-done(((bf16[16,16,1024]{2,1,0:T(8,128)(2,1)}), bf16[16,16,1024]{2,1,0:T(8,128)(2,1)S(1)}, u32[]{:S(2)}, u32[]{:S(2)}) %all-to-all-start.3) | async-done | bytes 524320 | tf_op jit(solution)/shard_map/all_to_all | solution.py:23
  145.7 7.2 %all-to-all-start.4 = ((bf16[64,2,4096]{2,1,0:T(2,128)(2,1)}), bf16[64,2,4096]{2,1,0:T(2,128)(2,1)}, u32[]{:S(2)}, u32[]{:S(2)}) async-start(bf16[64,2,4096]{2,1,0:T(2,128)(2,1)} %reshape.166), calls=%async_computation.4 | async-start | bytes 2097152 | tf_op jit(solution)/shard_map/all_to_all | solution.py:23
  169.0 3.7 %collective-permute-done.13 = bf16[16,512]{1,0:T(8,128)(2,1)S(1)} collective-permute-done((bf16[16,512]{1,0:T(8,128)(2,1)}, bf16[16,512]{1,0:T(8,128)(2,1)S(1)}, u32[]{:S(2)}, u32[]{:S(2)}) %collective-permute-start.13) | collective-permute-done | bytes 16416 | tf_op jit(solution)/shard_map/ppermute | solution.py:562
  173.8 3.6 %collective-permute-start.16 = (bf16[16,256]{1,0:T(8,128)(2,1)S(1)}, bf16[16,256]{1,0:T(8,128)(2,1)S(1)}, u32[]{:S(2)}, u32[]{:S(2)}) collective-permute-start(bf16[16,256]{1,0:T(8,128)(2,1)S(1)} %fusion.24.x0), channel_id=1, source_target_pairs={{0,16},{8,24},{16,0},{24,8},{1,17},{9,25},{17,1},{25,9},{2,18},{10... | collective-permute-start | bytes 24584 | tf_op jit(solution)/shard_map/ppermute | solution.py:569
  194.2 4.5 %down.1 = bf16[64,80,128]{2,1,0:T(8,128)(2,1)} custom-call(s32[3]{0:T(128)} %pad_add_fusion.c_ref, bf16[128,256]{1,0:T(8,128)(2,1)} %fusion.16.h_ref, bf16[256,4096]{1,0:T(8,128)(2,1)} %bitcast.87, bf16[16,4096]{1,0:T(8,128)(2,1)} %get-tuple-element.27.hid_ref, bf16[16,1024]{1,0:T(8,128)(2,1)} %get-tuple-element.37.d0, bf16[16,1024]{1,0:T(8,128)(2,1)} %copy-done.18, ...), custom_call_target="tpu_custom_call" | custom-call | flops 268435456 | bytes 4194304 | tf_op jit(solution)/shard_map/down/pallas_call | solution.py:253
  198.7 9.3 %all-to-all-start.5 = ((bf16[64,80,128]{2,1,0:T(8,128)(2,1)}), bf16[64,80,128]{2,1,0:T(8,128)(2,1)S(1)}, u32[]{:S(2)}, u32[]{:S(2)}) async-start(bf16[64,80,128]{2,1,0:T(8,128)(2,1)} %down.1), calls=%async_computation.5 | async-start | bytes 2621440 | tf_op jit(solution)/shard_map/all_to_all | solution.py:23
  208.0 4.1 %fusion = pred[1024,1024]{1,0:T(8,128)(4,1)} fusion(s32[1024,4]{0,1:T(4,128)S(1)} %get-tuple-element.84), kind=kLoop, calls=%fused_computation.2 | loop fusion | flops 7340032 | bytes 1064960 | tf_op jit(solution)/shard_map/reduce_or | solution.py:590
  212.2 30.2 %all-to-all-done.5 = bf16[64,80,128]{2,1,0:T(8,128)(2,1)S(1)} async-done(((bf16[64,80,128]{2,1,0:T(8,128)(2,1)}), bf16[64,80,128]{2,1,0:T(8,128)(2,1)S(1)}, u32[]{:S(2)}, u32[]{:S(2)}) %all-to-all-start.5) | async-done | bytes 1310752 | tf_op jit(solution)/shard_map/all_to_all | solution.py:23
  248.9 3.5 %all-to-all-start.6 = ((bf16[4,512,128]{2,1,0:T(8,128)(2,1)}), bf16[4,512,128]{2,1,0:T(8,128)(2,1)S(1)}, u32[]{:S(2)}, u32[]{:S(2)}) async-start(bf16[4,512,128]{2,1,0:T(8,128)(2,1)} %broadcast_in_dim.85), calls=%async_computation.6 | async-start | bytes 1048576 | tf_op jit(solution)/shard_map/all_to_all | solution.py:23
  253.0 7.7 %all-to-all-done.6 = bf16[4,512,128]{2,1,0:T(8,128)(2,1)S(1)} async-done(((bf16[4,512,128]{2,1,0:T(8,128)(2,1)}), bf16[4,512,128]{2,1,0:T(8,128)(2,1)S(1)}, u32[]{:S(2)}, u32[]{:S(2)}) %all-to-all-start.6) | async-done | bytes 524320 | tf_op jit(solution)/shard_map/all_to_all | solution.py:23
  (208 shorter events, 97.9 us)
Async XLA Ops:
  4.2 4.7 %collective-permute-start = (bf16[512,1664]{1,0:T(8,128)(2,1)}, bf16[512,1664]{1,0:T(8,128)(2,1)}, u32[]{:S(2)}, u32[]{:S(2)}) collective-permute-start(bf16[512,1664]{1,0:T(8,128)(2,1)} %project_away.1), channel_id=1, source_target_pairs={{0,4},{4,0},{1,5},{5,1},{2,6},{6,2},{3,7},{7,3},{8,12},{12,8},{9,1... | collective-permute-start | bytes 5111816 | tf_op jit(solution)/shard_map/ppermute | solution.py:31
  13.2 63.1 %all-to-all-start = ((bf16[4,128,1792]{2,1,0:T(8,128)(2,1)}), bf16[4,128,1792]{2,1,0:T(8,128)(2,1)}, u32[]{:S(2)}, u32[]{:S(2)}) async-start(bf16[4,128,1792]{2,1,0:T(8,128)(2,1)} %fold_core.1), calls=%async_computation | async-start | bytes 3670016 | tf_op jit(solution)/shard_map/all_to_all | solution.py:23
  20.5 13.2 %collective-permute-start.1 = (bf16[656,128]{1,0:T(8,128)(2,1)S(1)}, bf16[656,128]{1,0:T(8,128)(2,1)S(1)}, u32[]{:S(2)}, u32[]{:S(2)}) collective-permute-start(bf16[656,128]{1,0:T(8,128)(2,1)S(1)} %concatenate.23.refs_0_), channel_id=1, source_target_pairs={{0,32},{32,64},{64,96},{96,128},{128,160},{160,192},{192,224},{224... | collective-permute-start | bytes 503816 | tf_op jit(solution)/shard_map/ppermute | solution.py:41
  20.9 18.9 %collective-permute-start.2 = (bf16[656,128]{1,0:T(8,128)(2,1)S(1)}, bf16[656,128]{1,0:T(8,128)(2,1)S(1)}, u32[]{:S(2)}, u32[]{:S(2)}) collective-permute-start(bf16[656,128]{1,0:T(8,128)(2,1)S(1)} %concatenate.23.refs_0_), channel_id=1, source_target_pairs={{0,64},{32,96},{64,128},{96,160},{128,192},{160,224},{192,0},{224,... | collective-permute-start | bytes 503816 | tf_op jit(solution)/shard_map/ppermute | solution.py:41
  24.2 27.0 %collective-permute-start.3 = (bf16[656,128]{1,0:T(8,128)(2,1)S(1)}, bf16[656,128]{1,0:T(8,128)(2,1)S(1)}, u32[]{:S(2)}, u32[]{:S(2)}) collective-permute-start(bf16[656,128]{1,0:T(8,128)(2,1)S(1)} %concatenate.23.refs_0_), channel_id=1, source_target_pairs={{0,96},{32,128},{64,160},{96,192},{128,224},{160,0},{192,32},{224,... | collective-permute-start | bytes 503816 | tf_op jit(solution)/shard_map/ppermute | solution.py:41
  28.2 23.0 %collective-permute-start.4 = (bf16[656,128]{1,0:T(8,128)(2,1)S(1)}, bf16[656,128]{1,0:T(8,128)(2,1)S(1)}, u32[]{:S(2)}, u32[]{:S(2)}) collective-permute-start(bf16[656,128]{1,0:T(8,128)(2,1)S(1)} %concatenate.23.refs_0_), channel_id=1, source_target_pairs={{0,128},{32,160},{64,192},{96,224},{128,0},{160,32},{192,64},{224,... | collective-permute-start | bytes 503816 | tf_op jit(solution)/shard_map/ppermute | solution.py:41
  28.7 24.5 %collective-permute-start.5 = (bf16[656,128]{1,0:T(8,128)(2,1)S(1)}, bf16[656,128]{1,0:T(8,128)(2,1)S(1)}, u32[]{:S(2)}, u32[]{:S(2)}) collective-permute-start(bf16[656,128]{1,0:T(8,128)(2,1)S(1)} %concatenate.23.refs_0_), channel_id=1, source_target_pairs={{0,160},{32,192},{64,224},{96,0},{128,32},{160,64},{192,96},{224,1... | collective-permute-start | bytes 503816 | tf_op jit(solution)/shard_map/ppermute | solution.py:41
  33.7 24.5 %collective-permute-start.6 = (bf16[656,128]{1,0:T(8,128)(2,1)S(1)}, bf16[656,128]{1,0:T(8,128)(2,1)S(1)}, u32[]{:S(2)}, u32[]{:S(2)}) collective-permute-start(bf16[656,128]{1,0:T(8,128)(2,1)S(1)} %concatenate.23.refs_0_), channel_id=1, source_target_pairs={{0,192},{32,224},{64,0},{96,32},{128,64},{160,96},{192,128},{224,1... | collective-permute-start | bytes 503816 | tf_op jit(solution)/shard_map/ppermute | solution.py:41
  39.8 19.6 %collective-permute-start.7 = (bf16[656,128]{1,0:T(8,128)(2,1)S(1)}, bf16[656,128]{1,0:T(8,128)(2,1)S(1)}, u32[]{:S(2)}, u32[]{:S(2)}) collective-permute-start(bf16[656,128]{1,0:T(8,128)(2,1)S(1)} %concatenate.23.refs_0_), channel_id=1, source_target_pairs={{0,224},{32,0},{64,32},{96,64},{128,96},{160,128},{192,160},{224,1... | collective-permute-start | bytes 503816 | tf_op jit(solution)/shard_map/ppermute | solution.py:41
  62.7 22.4 %collective-permute-start.8 = (bf16[8,656,128]{2,1,0:T(8,128)(2,1)}, bf16[8,656,128]{2,1,0:T(8,128)(2,1)S(1)}, u32[]{:S(2)}, u32[]{:S(2)}) collective-permute-start(bf16[8,656,128]{2,1,0:T(8,128)(2,1)} %stacked.1.mine_ref), channel_id=1, source_target_pairs={{0,4},{4,0},{1,5},{5,1},{2,6},{6,2},{3,7},{7,3},{8,12},{12,8},{9,1... | collective-permute-start | bytes 4030472 | tf_op jit(solution)/shard_map/ppermute | solution.py:31
  78.9 24.5 %all-to-all-start.1 = ((bf16[8,16,2176]{2,1,0:T(8,128)(2,1)}), bf16[8,16,2176]{2,1,0:T(8,128)(2,1)}, u32[]{:S(2)}, u32[]{:S(2)}) async-start(bf16[8,16,2176]{2,1,0:T(8,128)(2,1)} %fold_y.1), calls=%async_computation.1 | async-start | bytes 1114112 | tf_op jit(solution)/shard_map/all_to_all | solution.py:23
  110.3 9.2 %all-to-all-start.2 = ((bf16[4,24,512]{2,1,0:T(8,128)(2,1)}), bf16[4,24,512]{2,1,0:T(8,128)(2,1)S(1)}, u32[]{:S(2)}, u32[]{:S(2)}) async-start(bf16[4,24,512]{2,1,0:T(8,128)(2,1)} %broadcast_in_dim.77), calls=%async_computation.2 | async-start | bytes 196608 | tf_op jit(solution)/shard_map/all_to_all | solution.py:23
  124.8 14.6 %all-to-all-start.3 = ((bf16[16,16,1024]{2,1,0:T(8,128)(2,1)}), bf16[16,16,1024]{2,1,0:T(8,128)(2,1)S(1)}, u32[]{:S(2)}, u32[]{:S(2)}) async-start(bf16[16,16,1024]{2,1,0:T(8,128)(2,1)} %bitcast.15), calls=%async_computation.3 | async-start | bytes 1048576 | tf_op jit(solution)/shard_map/all_to_all | solution.py:23
  145.7 43.7 %all-to-all-start.4 = ((bf16[64,2,4096]{2,1,0:T(2,128)(2,1)}), bf16[64,2,4096]{2,1,0:T(2,128)(2,1)}, u32[]{:S(2)}, u32[]{:S(2)}) async-start(bf16[64,2,4096]{2,1,0:T(2,128)(2,1)} %reshape.166), calls=%async_computation.4 | async-start | bytes 2097152 | tf_op jit(solution)/shard_map/all_to_all | solution.py:23
  153.0 6.1 %collective-permute-start.10 = (bf16[16,1024]{1,0:T(8,128)(2,1)S(1)}, bf16[16,1024]{1,0:T(8,128)(2,1)S(1)}, u32[]{:S(2)}, u32[]{:S(2)}) collective-permute-start(bf16[16,1024]{1,0:T(8,128)(2,1)S(1)} %copy-done.40), channel_id=1, source_target_pairs={{0,16},{8,24},{16,0},{24,8},{1,17},{9,25},{17,1},{25,9},{2,18},{10... | collective-permute-start | bytes 98312 | tf_op jit(solution)/shard_map/ppermute | solution.py:558
  167.2 5.5 %collective-permute-start.13 = (bf16[16,512]{1,0:T(8,128)(2,1)}, bf16[16,512]{1,0:T(8,128)(2,1)S(1)}, u32[]{:S(2)}, u32[]{:S(2)}) collective-permute-start(bf16[16,512]{1,0:T(8,128)(2,1)} %get-tuple-element.34), channel_id=1, source_target_pairs={{0,16},{8,24},{16,0},{24,8},{1,17},{9,25},{17,1},{25,9},{2,18},{10... | collective-permute-start | bytes 49160 | tf_op jit(solution)/shard_map/ppermute | solution.py:562
  167.2 5.5 %collective-permute-start.14 = (bf16[16,512]{1,0:T(8,128)(2,1)}, bf16[16,512]{1,0:T(8,128)(2,1)S(1)}, u32[]{:S(2)}, u32[]{:S(2)}) collective-permute-start(bf16[16,512]{1,0:T(8,128)(2,1)} %get-tuple-element.35), channel_id=1, source_target_pairs={{0,8},{8,16},{16,24},{24,0},{1,9},{9,17},{17,25},{25,1},{2,10},{10... | collective-permute-start | bytes 49160 | tf_op jit(solution)/shard_map/ppermute | solution.py:562
  173.5 5.5 %collective-permute-start.15 = (bf16[16,256]{1,0:T(8,128)(2,1)S(1)}, bf16[16,256]{1,0:T(8,128)(2,1)S(1)}, u32[]{:S(2)}, u32[]{:S(2)}) collective-permute-start(bf16[16,256]{1,0:T(8,128)(2,1)S(1)} %fusion.24.x0), channel_id=1, source_target_pairs={{0,8},{8,16},{16,24},{24,0},{1,9},{9,17},{17,25},{25,1},{2,10},{10... | collective-permute-start | bytes 24584 | tf_op jit(solution)/shard_map/ppermute | solution.py:569
  173.8 5.3 %collective-permute-start.16 = (bf16[16,256]{1,0:T(8,128)(2,1)S(1)}, bf16[16,256]{1,0:T(8,128)(2,1)S(1)}, u32[]{:S(2)}, u32[]{:S(2)}) collective-permute-start(bf16[16,256]{1,0:T(8,128)(2,1)S(1)} %fusion.24.x0), channel_id=1, source_target_pairs={{0,16},{8,24},{16,0},{24,8},{1,17},{9,25},{17,1},{25,9},{2,18},{10... | collective-permute-start | bytes 24584 | tf_op jit(solution)/shard_map/ppermute | solution.py:569
  184.6 8.9 %collective-permute-start.18 = (bf16[16,1024]{1,0:T(8,128)(2,1)}, bf16[16,1024]{1,0:T(8,128)(2,1)S(1)}, u32[]{:S(2)}, u32[]{:S(2)}) collective-permute-start(bf16[16,1024]{1,0:T(8,128)(2,1)} %get-tuple-element.38), channel_id=1, source_target_pairs={{0,24},{8,0},{16,8},{24,16},{1,25},{9,1},{17,9},{25,17},{2,26},{10... | collective-permute-start | bytes 98312 | tf_op jit(solution)/shard_map/ppermute | solution.py:574
  185.5 8.1 %collective-permute-start.19 = (bf16[16,1024]{1,0:T(8,128)(2,1)}, bf16[16,1024]{1,0:T(8,128)(2,1)S(1)}, u32[]{:S(2)}, u32[]{:S(2)}) collective-permute-start(bf16[16,1024]{1,0:T(8,128)(2,1)} %get-tuple-element.39), channel_id=1, source_target_pairs={{0,16},{8,24},{16,0},{24,8},{1,17},{9,25},{17,1},{25,9},{2,18},{10... | collective-permute-start | bytes 98312 | tf_op jit(solution)/shard_map/ppermute | solution.py:574
  186.9 6.6 %collective-permute-start.20 = (bf16[16,1024]{1,0:T(8,128)(2,1)}, bf16[16,1024]{1,0:T(8,128)(2,1)S(1)}, u32[]{:S(2)}, u32[]{:S(2)}) collective-permute-start(bf16[16,1024]{1,0:T(8,128)(2,1)} %get-tuple-element.40), channel_id=1, source_target_pairs={{0,8},{8,16},{16,24},{24,0},{1,9},{9,17},{17,25},{25,1},{2,10},{10... | collective-permute-start | bytes 98312 | tf_op jit(solution)/shard_map/ppermute | solution.py:574
  198.7 43.7 %all-to-all-start.5 = ((bf16[64,80,128]{2,1,0:T(8,128)(2,1)}), bf16[64,80,128]{2,1,0:T(8,128)(2,1)S(1)}, u32[]{:S(2)}, u32[]{:S(2)}) async-start(bf16[64,80,128]{2,1,0:T(8,128)(2,1)} %down.1), calls=%async_computation.5 | async-start | bytes 2621440 | tf_op jit(solution)/shard_map/all_to_all | solution.py:23
  248.9 11.8 %all-to-all-start.6 = ((bf16[4,512,128]{2,1,0:T(8,128)(2,1)}), bf16[4,512,128]{2,1,0:T(8,128)(2,1)S(1)}, u32[]{:S(2)}, u32[]{:S(2)}) async-start(bf16[4,512,128]{2,1,0:T(8,128)(2,1)} %broadcast_in_dim.85), calls=%async_computation.6 | async-start | bytes 1048576 | tf_op jit(solution)/shard_map/all_to_all | solution.py:23
  (45 other events, 651.7 us)

commit v2 on v1

--- a/solution.py
+++ b/solution.py
@@ -17,14 +17,11 @@
 NZ, NY, NC, NX = 8, 4, 2, 4
 EP = ("z", "y", "c")
 F32, BF16 = jnp.float32, jnp.bfloat16
+LIMIT = 16 << 20
 
 
 def exchanged(x, axis):
     return lax.all_to_all(x, axis, split_axis=0, concat_axis=0, tiled=True)
-
-
-def to_all(x, axis):
-    return exchanged(jnp.broadcast_to(x, (lax.axis_size(axis), *x.shape)), axis)
 
 
 def other_core(x):
@@ -37,9 +34,14 @@
 
 
 def gathered_z(x):
-    pieces = [x] + [
-        lax.ppermute(x, "z", [(i, (i + s) % NZ) for i in range(NZ)]) for s in range(1, NZ)
-    ]
+    pieces = [x] + [None] * (NZ - 1)
+    up, down = x, x
+    for s in range(1, NZ // 2 + 1):
+        up = lax.ppermute(up, "z", [(i, (i + 1) % NZ) for i in range(NZ)])
+        pieces[s] = up
+        if s < NZ // 2:
+            down = lax.ppermute(down, "z", [(i, (i - 1) % NZ) for i in range(NZ)])
+            pieces[NZ - s] = down
     zs = pl.pallas_call(
         stacked_kernel,
         out_shape=jax.ShapeDtypeStruct((NZ, *x.shape), x.dtype),
@@ -51,41 +53,37 @@
     return zs, other_core(zs)
 
 
-def over_x(x):
-    return to_all(x, "x").astype(F32).sum(axis=0)
-
-
 def packed(x):
     h = x.shape[0] // 2
     return jnp.concatenate([x[:h], x[h:]], axis=1)
 
 
-def unpacked(x):
-    return jnp.concatenate([x[:, :64], x[:, 64:]], axis=0)
-
-
 def turned_z(place_ref, z):
     az = lax.rem(place_ref[2] + (NZ - z), NZ)
     return pl.ds(pl.multiple_of(az * 128, 128), 128)
 
 
-def mix_kernel(c_ref, h_ref, mine_ref, away_ref, out_ref):
+def both_kinds(c, r, n):
+    lane = lax.broadcasted_iota(jnp.int32, (n, 128), 1)
+    res = []
+    for k in range(2):
+        top, low = r[:n, k * 128 : (k + 1) * 128], r[n:, k * 128 : (k + 1) * 128]
+        res.append((top + pltpu.roll(low, 64, 1), pltpu.roll(top, 64, 1) + low))
+    first = jnp.where(c == 0, res[0][0], res[1][0])
+    second = jnp.where(c == 0, res[1][1], res[0][1])
+    return jnp.where(lane < 64, first, second).astype(BF16)
+
+
+def mix_kernel(c_ref, x0, x1, x2, x3, mine_ref, away_ref, out_ref):
     c = c_ref[0]
-    both = jnp.concatenate(
-        [h_ref[y, :16, :256] for y in range(NY)] + [h_ref[y, :16, 256:] for y in range(NY)], axis=0
-    )
-    lane = lax.broadcasted_iota(jnp.int32, (64, 128), 1)
+    xs = (x0, x1, x2, x3)
+    both = jnp.concatenate([r[:16, :256] for r in xs] + [r[:16, 256:] for r in xs], axis=0)
     for z in range(NZ):
-        res = []
-        for w in (mine_ref, away_ref):
-            r = jnp.dot(both, w[z, :256, :], preferred_element_type=F32)
-            top, low = r[:64], r[64:]
-            res.append((top + pltpu.roll(low, 64, 1), pltpu.roll(top, 64, 1) + low))
-        first = jnp.where(c == 0, res[0][0], res[1][0])
-        second = jnp.where(c == 0, res[1][1], res[0][1])
-        tile = jnp.where(lane < 64, first, second).astype(BF16)
-        for y in range(NY):
-            out_ref[y, :, turned_z(c_ref, z)] = tile[y * 16 : (y + 1) * 16]
+        w = jnp.concatenate([mine_ref[z, :256, :], away_ref[z, :256, :]], axis=1)
+        tile = both_kinds(c, jnp.dot(both, w, preferred_element_type=F32), 64)
+        for s in range(NY):
+            to = lax.rem(c_ref[1] + (NY - s), NY)
+            out_ref[to, :, turned_z(c_ref, z)] = tile[s * 16 : (s + 1) * 16]
 
 
 VMEM = pl.BlockSpec(memory_space=pltpu.VMEM)
@@ -96,13 +94,14 @@
     return pl.pallas_call(
         mix_kernel,
         out_shape=jax.ShapeDtypeStruct((NY, 16, 1024), BF16),
-        in_specs=[SMEM, VMEM, VMEM, VMEM],
+        in_specs=[SMEM] + [VMEM] * 6,
         out_specs=VMEM,
+        compiler_params=pltpu.CompilerParams(vmem_limit_bytes=LIMIT),
         cost_estimate=pl.CostEstimate(
             flops=2 * 128 * 256 * 128 * 16, bytes_accessed=2 << 20, transcendentals=0
         ),
         name="mix",
-    )(c, heads, mine, away)
+    )(c, *heads, mine, away)
 
 
 def settle_kernel(
@@ -131,7 +130,8 @@
         cols = slice(at, at + 512)
         norm = (hid_ref[:, cols].astype(F32) * inverse * gain_ref[:, cols]).astype(BF16)
         norm_ref[:, cols] = norm
-        send_ref[:, cols] = jnp.dot(spread, norm, preferred_element_type=F32).astype(BF16)
+        rows = jnp.dot(spread, norm, preferred_element_type=F32)
+        send_ref[:, :, cols] = rows.reshape(64, 2, 512).astype(BF16)
     for s, out in enumerate((n0_ref, n1_ref, n2_ref, n3_ref)):
         to = lax.rem(c_ref[1] + s, NY)
         for z in range(NZ):
@@ -146,7 +146,7 @@
         out_shape=(
             jax.ShapeDtypeStruct((16, D), BF16),
             jax.ShapeDtypeStruct((16, 128), F32),
-            jax.ShapeDtypeStruct((128, D), BF16),
+            jax.ShapeDtypeStruct((64, 2, D), BF16),
             part, part, part, part,
         ),
         in_specs=[SMEM] + [VMEM] * 5,
@@ -161,19 +161,19 @@
 
 def dense_kernel(c_ref, x0, x1, x2, x3, mine_ref, away_ref, o0, o1, o2, o3):
     c = c_ref[0]
-    acc = [jnp.zeros((64, 128), F32) for _ in range(4)]
+    acc = jnp.zeros((64, 512), F32)
     for z in range(NZ):
         cols = turned_z(c_ref, z)
         x = jnp.concatenate([r[:, cols] for r in (x0, x1, x2, x3)], axis=0)
         own = jnp.where(c == 0, x[:, :64], x[:, 64:])
         off = jnp.where(c == 0, x[:, 64:], x[:, :64])
-        for j in range(4):
-            rows = slice(272 + j * 64, 336 + j * 64)
-            acc[j] += jnp.dot(own, mine_ref[z, rows, :], preferred_element_type=F32)
-            acc[j] += jnp.dot(off, away_ref[z, rows, :], preferred_element_type=F32)
+        for part, ref in ((own, mine_ref), (off, away_ref)):
+            w = jnp.concatenate(
+                [ref[z, 272 + j * 64 : 336 + j * 64, :] for j in range(4)], axis=1
+            )
+            acc += jnp.dot(part, w, preferred_element_type=F32)
     for s, out in enumerate((o0, o1, o2, o3)):
-        for j in range(4):
-            out[:, j * 128 : (j + 1) * 128] = acc[j][s * 16 : (s + 1) * 16].astype(BF16)
+        out[...] = acc[s * 16 : (s + 1) * 16].astype(BF16)
 
 
 def dense_products(c, xs, mine, away):
@@ -183,6 +183,7 @@
         out_shape=(part,) * 4,
         in_specs=[SMEM] + [VMEM] * 6,
         out_specs=(VMEM,) * 4,
+        compiler_params=pltpu.CompilerParams(vmem_limit_bytes=LIMIT),
         cost_estimate=pl.CostEstimate(
             flops=2 * 64 * 1024 * 512, bytes_accessed=2 << 20, transcendentals=0
         ),
@@ -194,16 +195,9 @@
     c = c_ref[0]
     xs = (x0, x1, x2, x3)
     both = jnp.concatenate([r[:, :128] for r in xs] + [r[:, 128:] for r in xs], axis=0)
-    lane = lax.broadcasted_iota(jnp.int32, (64, 128), 1)
     for z in range(NZ):
-        res = []
-        for w in (mine_ref, away_ref):
-            r = jnp.dot(both, w[z, 528:656, :], preferred_element_type=F32)
-            top, low = r[:64], r[64:]
-            res.append((top + pltpu.roll(low, 64, 1), pltpu.roll(top, 64, 1) + low))
-        first = jnp.where(c == 0, res[0][0], res[1][0])
-        second = jnp.where(c == 0, res[1][1], res[0][1])
-        tile = jnp.where(lane < 64, first, second).astype(BF16)
+        w = jnp.concatenate([mine_ref[z, 528:656, :], away_ref[z, 528:656, :]], axis=1)
+        tile = both_kinds(c, jnp.dot(both, w, preferred_element_type=F32), 64)
         for s, out in enumerate((o0, o1, o2, o3)):
             out[:, turned_z(c_ref, z)] = tile[s * 16 : (s + 1) * 16]
 
@@ -215,6 +209,7 @@
         out_shape=(part,) * 4,
         in_specs=[SMEM] + [VMEM] * 6,
         out_specs=(VMEM,) * 4,
+        compiler_params=pltpu.CompilerParams(vmem_limit_bytes=LIMIT),
         cost_estimate=pl.CostEstimate(
             flops=2 * 64 * 1024 * 512, bytes_accessed=1 << 20, transcendentals=0
         ),
@@ -222,9 +217,8 @@
     )(c, *xs, mine, away)
 
 
-def half_rows(tile):
+def half_rows(wide):
     lane = lax.broadcasted_iota(jnp.int32, (8, 128), 1)
-    wide = tile.astype(F32)
     turn = pltpu.roll(wide, 64, 1)
     return (
         jnp.where(lane < 64, wide[:8], turn[8:]),
@@ -240,20 +234,21 @@
         top, low = res[:64, cols], res[64:, cols]
         out_ref[2 * p, :64] = jnp.where(lane < 64, top, pltpu.roll(low, 64, 1)).astype(BF16)
         out_ref[2 * p + 1, :64] = jnp.where(lane < 64, pltpu.roll(top, 64, 1), low).astype(BF16)
+    quarter = lax.broadcasted_iota(jnp.int32, (16, 128), 0) // 4 == c_ref[3]
     for zl in range(2):
         for s, d in enumerate((d0, d1, d2, d3)):
             at = zl * NY + lax.rem(c_ref[1] + s, NY)
-            hid = half_rows(hid_ref[:, pl.ds(pl.multiple_of(at * 128, 128), 128)])
-            den = half_rows(d[:, zl * 128 : (zl + 1) * 128])
-            for k in range(2):
-                out_ref[2 * at + k, 64:] = jnp.concatenate([hid[k], den[k]], axis=0).astype(BF16)
+            hid = hid_ref[:, pl.ds(pl.multiple_of(at * 128, 128), 128)].astype(F32)
+            wide = d[:, zl * 128 : (zl + 1) * 128].astype(F32) + jnp.where(quarter, hid, 0.0)
+            for k, half in enumerate(half_rows(wide)):
+                out_ref[2 * at + k, 64:] = half.astype(BF16)
 
 
 def down_for_all(c, expert_hidden, w, hidden, downs):
     return pl.pallas_call(
         down_kernel,
         grid=(4,),
-        out_shape=jax.ShapeDtypeStruct((64, 80, 128), BF16),
+        out_shape=jax.ShapeDtypeStruct((64, 72, 128), BF16),
         in_specs=[
             SMEM,
             pl.BlockSpec((128, 256), lambda i: (0, 0)),
@@ -261,7 +256,8 @@
             pl.BlockSpec((16, 1024), lambda i: (0, i)),
         ]
         + [pl.BlockSpec((16, 256), lambda i: (0, i))] * 4,
-        out_specs=pl.BlockSpec((16, 80, 128), lambda i: (i, 0, 0)),
+        out_specs=pl.BlockSpec((16, 72, 128), lambda i: (i, 0, 0)),
+        compiler_params=pltpu.CompilerParams(vmem_limit_bytes=LIMIT),
         cost_estimate=pl.CostEstimate(
             flops=2 * 128 * 256 * 4096, bytes_accessed=4 << 20, transcendentals=0
         ),
@@ -269,74 +265,67 @@
     )(c, expert_hidden, w, hidden, *downs)
 
 
-def project_kernel(kept, c_ref, tok_ref, gain_ref, q_ref, k_ref, v_ref, o_ref, i_ref, f_ref, out, all_ref, x_ref):
-    core = c_ref[0] if kept else 1 - c_ref[0]
-    gain = gain_ref[...].astype(F32)
-    lane = lax.broadcasted_iota(jnp.int32, (128, 128), 1)
-    all_ref[...] = jnp.transpose(tok_ref[...])
+def project_kernel(kept, c_ref, tok_ref, gain_ref, q_ref, k_ref, v_ref, o_ref, i_ref, f_ref, *refs):
+    got_ref, out, all_ref, x_ref = refs if kept else (None, *refs)
+    c = c_ref[0]
+    core = c if kept else 1 - c
+    y = pl.program_id(0)
+
+    @pl.when(y == 0)
+    def _():
+        all_ref[...] = jnp.transpose(tok_ref[...])
+
     gate_rows = jnp.concatenate(
         [jnp.zeros((64, 64), BF16), i_ref[...], f_ref[...], jnp.zeros((56, 64), BF16)], axis=0
     )
-    for y in range(NY):
-        for z in range(NZ):
-            at = pl.multiple_of(((z * NY + y) * NC + core) * 16, 16)
-            x_ref[z * 16 : (z + 1) * 16, :] = all_ref[pl.ds(at, 16), :]
-        wide = x_ref[...].astype(F32)
-        scaled = (wide * gain).astype(BF16)
-        rows = slice(y * 128, (y + 1) * 128)
-        at = 0
-        for w in (q_ref, k_ref, v_ref, o_ref):
-            n = w.shape[1]
-            res = jnp.dot(scaled, w[...], preferred_element_type=F32)
-            out[rows, at : at + n] = res.astype(out.dtype)
-            at += n
-        gates = lax.dot_general(
-            scaled, gate_rows, (((1,), (1,)), ((), ())), preferred_element_type=F32
-        )
-        square = jnp.sum(wide * wide, axis=1, keepdims=True)
-        both = jnp.concatenate([wide, jnp.zeros((128, 64), F32)], axis=1)
-        last = jnp.where(lane < 64, both, jnp.where(lane == 72, square, gates))
-        out[rows, 1536:1664] = last.astype(out.dtype)
+    for z in range(NZ):
+        at = pl.multiple_of(((z * NY + y) * NC + core) * 16, 16)
+        x_ref[z * 16 : (z + 1) * 16, :] = all_ref[pl.ds(at, 16), :]
+    wide = x_ref[...].astype(F32)
+    scaled = (wide * gain_ref[...].astype(F32)).astype(BF16)
+    at = 0
+    for w in (q_ref, k_ref, v_ref, o_ref):
+        for half in range(0, w.shape[1], 256):
+            res = jnp.dot(scaled, w[:, half : half + 256], preferred_element_type=F32)
+            cols = slice(at, at + 256)
+            if kept:
+                res += got_ref[:, cols].astype(F32)
+            out[0, :, cols] = res.astype(BF16)
+            at += 256
+    lane = lax.broadcasted_iota(jnp.int32, (128, 128), 1)
+    gates = lax.dot_general(
+        scaled, gate_rows, (((1,), (1,)), ((), ())), preferred_element_type=F32
+    )
+    square = jnp.sum(wide * wide, axis=1, keepdims=True)
+    both = jnp.concatenate([wide, jnp.zeros((128, 64), F32)], axis=1)
+    last = jnp.where(lane < 64, both, jnp.where(lane == 72, square, gates))
+    if not kept:
+        out[0, :, 1536:] = last.astype(BF16)
+    else:
+        other = got_ref[:, 1536:].astype(F32)
+        out[0, :, 1536:1664] = (last + other).astype(BF16)
+        first = jnp.where(c == 0, last, other)
+        second = jnp.where(c == 0, other, last)
+        out[0, :, 1664:] = jnp.where(lane < 64, first, pltpu.roll(second, 64, 1)).astype(BF16)
 
 
 def project(kept, *args):
+    whole = lambda *shape: pl.BlockSpec(shape, lambda g: (0,) * len(shape))
+    wide = 1792 if kept else 1664
     return pl.pallas_call(
         functools.partial(project_kernel, kept),
-        out_shape=jax.ShapeDtypeStruct((512, 1664), F32 if kept else BF16),
-        in_specs=[SMEM] + [VMEM] * 8,
-        out_specs=VMEM,
+        grid=(NY,),
+        out_shape=jax.ShapeDtypeStruct((NY, 128, wide), BF16),
+        in_specs=[SMEM]
+        + [whole(*a.shape) for a in args[1:9]]
+        + [pl.BlockSpec((None, 128, 1664), lambda g: (g, 0, 0))] * kept,
+        out_specs=pl.BlockSpec((1, 128, wide), lambda g: (g, 0, 0)),
         scratch_shapes=[pltpu.VMEM((1024, 64), BF16), pltpu.VMEM((128, 64), BF16)],
         cost_estimate=pl.CostEstimate(
             flops=2 * 512 * 256 * 1664, bytes_accessed=3 << 20, transcendentals=0
         ),
         name="project_kept" if kept else "project_away",
     )(*args)
-
-
-def fold_core_kernel(c_ref, kept_ref, got_ref, out_ref):
-    c = c_ref[0]
-    lane = lax.broadcasted_iota(jnp.int32, (128, 128), 1)
-    for y in range(NY):
-        rows = slice(y * 128, (y + 1) * 128)
-        kept, got = kept_ref[rows, :], got_ref[rows, :].astype(F32)
-        out_ref[y, :, :1664] = (kept + got).astype(BF16)
-        a, b = kept[:, 1536:], got[:, 1536:]
-        first = jnp.where(c == 0, a, b)
-        second = jnp.where(c == 0, b, a)
-        out_ref[y, :, 1664:] = jnp.where(lane < 64, first, pltpu.roll(second, 64, 1)).astype(BF16)
-
-
-def fold_core(c, kept, got):
-    return pl.pallas_call(
-        fold_core_kernel,
-        out_shape=jax.ShapeDtypeStruct((NY, 128, 1792), BF16),
-        in_specs=[SMEM, VMEM, VMEM],
-        out_specs=VMEM,
-        cost_estimate=pl.CostEstimate(
-            flops=1 << 20, bytes_accessed=6 << 20, transcendentals=0
-        ),
-        name="fold_core",
-    )(c, kept, got)
 
 
 def fold_y_kernel(in_ref, out_ref):
@@ -471,12 +460,105 @@
     )(x, igate_bias[None], fgate_bias[None], head_gain[None], state_matrix, state_norm, state_max)
 
 
-def slot_ranks(routes):
-    chosen = (routes[:, :, None] == jnp.arange(64, dtype=jnp.int32)[None, None, :]).astype(F32)
-    per_row = jnp.sum(chosen, axis=1).reshape(64, 16, 64)
-    lower = jnp.tril(jnp.ones((16, 16), F32), -1)
-    earlier = jnp.einsum("rs,gse->gre", lower, per_row).reshape(1024, 64)
-    return jnp.sum(chosen * earlier[:, None, :], axis=2).astype(jnp.int32)
+def rank_kernel(me_ref, routes_ref, weights_ref, target_ref, spread_ref, weight_ref):
+    me = me_ref[0]
+    expert = lax.broadcasted_iota(jnp.int32, (64, 128), 0)
+    a = lax.broadcasted_iota(jnp.int32, (128, 128), 0)
+    b = lax.broadcasted_iota(jnp.int32, (128, 128), 1)
+    before = jnp.where((a < b) & (a // 16 == b // 16), 1.0, 0.0).astype(BF16)
+    weight = jnp.zeros((128, 128), F32)
+    for t in range(8):
+        cols = slice(t * 128, (t + 1) * 128)
+        hits = [expert == routes_ref[j : j + 1, cols] for j in range(4)]
+        count = sum(jnp.where(h, 1.0, 0.0) for h in hits)
+        earlier = jnp.dot(count.astype(BF16), before, preferred_element_type=F32)
+        for j in range(4):
+            rank = jnp.sum(jnp.where(hits[j], earlier, 0.0), axis=0, keepdims=True)
+            target = routes_ref[j : j + 1, cols] * 2 + rank.astype(jnp.int32)
+            target_ref[j : j + 1, cols] = target
+            mine = (target == me * 2 + a % 2) & (b // 16 + t * 8 == a // 2)
+            weight += jnp.where(mine, weights_ref[j : j + 1, cols], 0.0)
+    weight_ref[...] = jnp.broadcast_to(jnp.sum(weight, axis=1, keepdims=True), (128, 128))
+    cols = pl.ds(pl.multiple_of((me // 8) * 128, 128), 128)
+    named = a == target_ref[0:1, cols]
+    for j in range(1, 4):
+        named = named | (a == target_ref[j : j + 1, cols])
+    lane = lax.broadcasted_iota(jnp.int32, (128, 16), 0)
+    row = lax.broadcasted_iota(jnp.int32, (128, 16), 1)
+    own = jnp.where(lane == lax.rem(me, 8) * 16 + row, 1.0, 0.0).astype(BF16)
+    spread_ref[...] = jnp.dot(
+        jnp.where(named, 1.0, 0.0).astype(BF16), own, preferred_element_type=F32
+    ).astype(BF16)
+
+
+def rank_rows(me, routes, weights):
+    return pl.pallas_call(
+        rank_kernel,
+        out_shape=(
+            jax.ShapeDtypeStruct((4, 1024), jnp.int32),
+            jax.ShapeDtypeStruct((128, 16), BF16),
+            jax.ShapeDtypeStruct((128, 128), F32),
+        ),
+        in_specs=[SMEM, VMEM, VMEM],
+        out_specs=(VMEM,) * 3,
+        cost_estimate=pl.CostEstimate(flops=1 << 24, bytes_accessed=1 << 20, transcendentals=0),
+        name="rank_rows",
+    )(me, routes, weights)
+
+
+def pick_kernel(target_ref, out_ref):
+    at = lax.broadcasted_iota(jnp.int32, (128, 128), 0)
+    row = lax.broadcasted_iota(jnp.int32, (1, 128), 1)
+    for t in range(8):
+        cols = slice(t * 128, (t + 1) * 128)
+        local = []
+        for j in range(4):
+            target = target_ref[j : j + 1, cols]
+            local.append((target // 2) * 16 + 2 * (row // 16) + target % 2)
+        for k in range(8):
+            hit = at + k * 128 == local[0]
+            for j in range(1, 4):
+                hit = hit | (at + k * 128 == local[j])
+            out_ref[t, k * 128 : (k + 1) * 128, :] = jnp.where(hit, 1.0, 0.0).astype(BF16)
+
+
+def picks(target):
+    return pl.pallas_call(
+        pick_kernel,
+        out_shape=jax.ShapeDtypeStruct((8, 1024, 128), BF16),
+        in_specs=[VMEM],
+        out_specs=VMEM,
+        compiler_params=pltpu.CompilerParams(vmem_limit_bytes=LIMIT),
+        cost_estimate=pl.CostEstimate(flops=1 << 24, bytes_accessed=2 << 20, transcendentals=0),
+        name="picks",
+    )(target)
+
+
+def finish_kernel(c_ref, b0, b1, b2, b3, out_ref):
+    x = c_ref[3]
+    parts = [r[...].astype(F32) for r in (b0, b1, b2, b3)]
+    total = None
+    for a in range(NX):
+        s = lax.rem(x + (NX - a), NX)
+        part = jnp.where(
+            s == 0, parts[0], jnp.where(s == 1, parts[1], jnp.where(s == 2, parts[2], parts[3]))
+        )
+        total = part if total is None else total + part
+    turned = jnp.transpose(total)
+    out_ref[:, :512] = turned[:64].astype(BF16)
+    out_ref[:, 512:] = turned[64:].astype(BF16)
+
+
+def finish(c, parts):
+    return pl.pallas_call(
+        finish_kernel,
+        out_shape=jax.ShapeDtypeStruct((64, 1024), BF16),
+        in_specs=[SMEM] + [VMEM] * 4,
+        out_specs=VMEM,
+        compiler_params=pltpu.CompilerParams(vmem_limit_bytes=LIMIT),
+        cost_estimate=pl.CostEstimate(flops=1 << 20, bytes_accessed=1 << 20, transcendentals=0),
+        name="finish",
+    )(c, *parts)
 
 
 def layer(
@@ -509,7 +591,7 @@
     me = lax.axis_index(EP)
     c = lax.axis_index("c")
     y, z = lax.axis_index("y"), lax.axis_index("z")
-    c_ref = jnp.stack([c, y, z]).astype(jnp.int32)
+    c_ref = jnp.stack([c, y, z, lax.axis_index("x")]).astype(jnp.int32)
     piece = jnp.concatenate(
         [
             packed(w_mixout),
@@ -528,8 +610,7 @@
     )
     away = project(False, *operands)
     got = other_core(away)
-    kept = project(True, *operands)
-    folded = fold_core(c_ref, kept, got)
+    folded = project(True, *operands, got)
     folded = exchanged(folded, "y")
     folded = fold_y(folded)
     folded = exchanged(folded, "z")
@@ -541,19 +622,20 @@
     extra = jnp.where(c == 0, extra, extra[::-1])[:, (z - jnp.arange(NZ)) % NZ]
     extra = extra.transpose(2, 1, 0, 3).reshape(4, 512)
     heads = jnp.concatenate([heads_out, extra, jnp.zeros((4, 512), BF16)], axis=0)
-    heads = to_all(heads, "y")
-    vectors = heads[:, 16:20].reshape(NY, 2, NZ, 128).transpose(1, 2, 0, 3).reshape(2, 1, D)
+    heads = [heads] + [
+        lax.ppermute(heads, "y", [(i, (i + s) % NY) for i in range(NY)]) for s in (1, 2, 3)
+    ]
+    vectors = jnp.stack([h[16:20] for h in heads])[(y - jnp.arange(NY)) % NY]
+    vectors = vectors.reshape(NY, 2, NZ, 128).transpose(1, 2, 0, 3).reshape(2, 1, D)
     vectors = vectors.astype(F32)
     partial = mix(c_ref, heads, mine, away)
     copies = jnp.broadcast_to(partial[:, None], (NY, NX, 16, 1024)).reshape(16, 16, 1024)
     got = exchanged(copies, ("y", "x")).reshape(NY, NX, 16, 1024)
-    ranks = slot_ranks(routes)
-    target = routes * 2 + ranks
-    own_target = lax.dynamic_slice(target, (me * 16, 0), (16, 4))
-    slots = jnp.arange(128)
-    spread = jnp.any(own_target[:, :, None] == slots[None, None, :], axis=1).T.astype(BF16)
+    target, spread, weight = rank_rows(
+        jnp.full((1,), me, jnp.int32), routes.T, route_weights.T
+    )
     hidden, dense_gate, send, *sides = settle(c_ref, got, tok, vectors[0], vectors[1], spread)
-    arrived = exchanged(send.reshape(64, 2, D), EP).reshape(128, D)
+    arrived = exchanged(send, EP).reshape(128, D)
     xs = [sides[0]] + [
         lax.ppermute(sides[s], "y", [(i, (i + s) % NY) for i in range(NY)]) for s in (1, 2, 3)
     ]
@@ -573,30 +655,24 @@
     downs = [downs[0]] + [
         lax.ppermute(downs[s], "y", [(i, (i - s) % NY) for i in range(NY)]) for s in (1, 2, 3)
     ]
-    named = routes == me
-    slot_of = jnp.sum(jnp.where(named, (jnp.arange(1024) // 16)[:, None] * 2 + ranks, 0), axis=1)
-    slot_weight = jnp.sum(jnp.where(named, route_weights, 0.0), axis=1)
-    slot_hit = (slot_of[:, None] == slots[None, :]) & jnp.any(named, axis=1)[:, None]
-    weight = jnp.sum(jnp.where(slot_hit, slot_weight[:, None], 0.0), axis=0)
     gate_part = jnp.dot(arrived, w_exp_gate[0], preferred_element_type=F32)
     up_part = jnp.dot(arrived, w_exp_up[0], preferred_element_type=F32)
-    expert_hidden = (jax.nn.silu(gate_part) * up_part * weight[:, None]).astype(BF16)
+    expert_hidden = (jax.nn.silu(gate_part) * up_part * weight[:, :1]).astype(BF16)
     returned = down_for_all(c_ref, expert_hidden, w_exp_down[0], hidden, downs)
     returned = exchanged(returned, EP)
-    rows = returned[:, 64:].reshape(64, 2, 8, 2, 64).transpose(1, 0, 3, 2, 4).reshape(2, 1024, 64)
-    hidden_cols, dense_rows = rows[0], rows[1]
+    dense_rows = returned[:, 64:].reshape(64, 8, 2, 64).transpose(0, 2, 1, 3).reshape(1024, 64)
     returned = returned[:, :64]
-    local = routes * 16 + 2 * ((jnp.arange(1024) // 16)[:, None] % 8) + ranks
-    pick = jnp.any(local[:, :, None] == jnp.arange(1024)[None, None, :], axis=1).astype(BF16)
-    pick = pick.reshape(2, 4, 128, 1024)
     source = returned.reshape(64, 4, 16, 128).transpose(1, 0, 2, 3).reshape(4, 1024, 128)
-    halves = jnp.einsum("hgmk,gkn->hgmn", pick, source, preferred_element_type=F32)
+    pick = picks(target).reshape(2, 4, 1024, 128)
+    halves = jnp.einsum("hgkm,gkn->hgmn", pick, source, preferred_element_type=F32)
     routed = jnp.concatenate(
         [halves[0, :, :, :64].reshape(512, 64), halves[1, :, :, 64:].reshape(512, 64)], axis=0
     )
     branch = packed((routed + dense_rows.astype(F32)).astype(BF16))
-    branch = unpacked(over_x(branch))
-    layer_out = (hidden_cols.astype(F32) + branch).astype(BF16)
+    branches = [branch] + [
+        lax.ppermute(branch, "x", [(i, (i + s) % NX) for i in range(NX)]) for s in (1, 2, 3)
+    ]
+    layer_out = finish(c_ref, branches).T
     return (layer_out, new_matrix, new_norm, new_max)
 
 

time: 264 us -> 215 us (0.81)
  local copies, waits for them, and re-layouts: 32 us -> 14.9 us
  waiting for transfers between devices: 93.1 us -> 80 us
  other arithmetic: 13 us -> 3.41 us
  starting transfers between devices: 80.2 us -> 76 us
  matrix products: 4.42 us -> 1.47 us
    all_to_all x7 -> x5, waiting for transfers between devices: 63.8 us -> 52.9 us  [exchanged(): return lax.all_to_all(x, axis, split_axis=0, concat_axis=0, tiled=True)]
    all_to_all x7 -> x5, starting transfers between devices: 43.3 us -> 34.2 us  [exchanged(): return lax.all_to_all(x, axis, split_axis=0, concat_axis=0, tiled=True)]
    reshape x5 -> x1, local copies, waits for them, and re-layouts: 7.37 us -> 1.46 us  [layer(): arrived = exchanged(send, EP).reshape(128, D)]
    reduce_or x3 -> x0, other arithmetic: 4.92 us -> none  [the longest x1 4.13 us: layer(): jnp.any(local[:, :, None] == jnp.arange(1024)[None, None, :], axis=1)]
    unnamed x91 -> x66, local copies, waits for them, and re-layouts: 9.34 us -> 6.34 us
    reduce_sum x5 -> x0, other arithmetic: 2.74 us -> none  [the longest x1 1.09 us: slot_ranks(): return jnp.sum(chosen * earlier[:, None, :], axis=2).astype(jnp.int32)]
    pallas_call x3 -> x5, Pallas kernels: 10.7 us -> 13.4 us  [the longest x2 8.13 us: project(): pl.pallas_call(functools.partial(project_kernel, kept), grid=(NY,), out_s...]
    ppermute x7 -> x13, starting transfers between devices: 18.7 us -> 21.2 us  [the longest x3 11 us: gathered_z(): down = lax.ppermute(down, 'z', [(i, (i - 1) % NZ) for i in range(NZ)])]
  transfers between devices with their start and end apart: 28 -> 32, of which waited for: 15 -> 15; matrix products, arithmetic and copies ran while one was open for 12% -> 4% of each run, Pallas kernels for 6% -> 8%
where the time goes in v2:
time: 215 us; the launch traced here: 214 us
  waiting for transfers between devices  80 us (37%)
  starting transfers between devices  76 us (35%)
  Pallas kernels  36.9 us (17%)
  local copies, waits for them, and re-layouts  14.9 us (7%)
  other arithmetic  3.41 us (2%)
    all_to_all x5, waiting for transfers between devices, exchanged(): return lax.all_to_all(x, axis, split_axis=0, concat_axis=0, tiled=True)  52.9 us
    all_to_all x5, starting transfers between devices, exchanged(): return lax.all_to_all(x, axis, split_axis=0, concat_axis=0, tiled=True)  34.2 us
    ppermute x3, starting transfers between devices, gathered_z(): down = lax.ppermute(down, 'z', [(i, (i - 1) % NZ) for i in range(NZ)])  11 us
    ppermute x4, waiting for transfers between devices, gathered_z(): up = lax.ppermute(up, 'z', [(i, (i + 1) % NZ) for i in range(NZ)])  8.56 us
    pallas_call x2, Pallas kernels, project(): pl.pallas_call(functools.partial(project_kernel, kept), grid=(NY,), out_s...  8.13 us
    unnamed x66, local copies, waits for them, and re-layouts  6.34 us
    ppermute x3, waiting for transfers between devices, gathered_z(): down = lax.ppermute(down, 'z', [(i, (i - 1) % NZ) for i in range(NZ)])  5.85 us
    ppermute x3, starting transfers between devices, layer(): lax.ppermute(sums[s], 'y', [(i, (i - s) % NY) for i in range(NY)])  5.59 us
  transfers between devices with their start and end apart: 32, of which 15 were waited for; matrix products, arithmetic and copies ran while one was open for 4% of the time, Pallas kernels for 8%

profile of v2, /device:TPU:8, one launch (start us, length us, event | category | flops | bytes accessed | tf_op | source)
XLA Modules:
  0.0 213.9 jit_solution(18321811225197276009)
XLA Ops:
  1.3 3.5 %project_away.1 = bf16[4,128,1664]{2,1,0:T(8,128)(2,1)} custom-call(s32[4]{0:T(128)} %pad_add_fusion.c_ref, bf16[64,1024]{1,0:T(8,128)(2,1)} %bitcast.80, bf16[1,64]{1,0:T(2,128)(2,1)} %bitcast.91, bf16[64,256]{1,0:T(8,128)(2,1)} %q_ref.3, bf16[64,256]{1,0:T(8,128)(2,1)} %k_ref.3, bf16[64,512]{1,0:T(8,128)(2,1)} %v_ref.3, bf16[64,512]{1,0:T(8,128)(2,1)} %o_ref.3, ...), custom_call_target="tpu_custom_call" | custom-call | flops 436207616 | bytes 3145728 | tf_op jit(solution)/shard_map/project_away/pallas_call | solution.py:315
  7.9 4.0 %collective-permute-start.5 = (bf16[656,128]{1,0:T(8,128)(2,1)S(1)}, bf16[656,128]{1,0:T(8,128)(2,1)S(1)}, u32[]{:S(2)}, u32[]{:S(2)}) collective-permute-start(bf16[656,128]{1,0:T(8,128)(2,1)S(1)} %concatenate.20.refs_0_), channel_id=1, source_target_pairs={{0,224},{32,0},{64,32},{96,64},{128,96},{160,128},{192,160},{224,1... | collective-permute-start | bytes 503816 | tf_op jit(solution)/shard_map/ppermute | solution.py:43
  11.9 4.9 %collective-permute-done.1.refs_1_ = bf16[656,128]{1,0:T(8,128)(2,1)S(1)} collective-permute-done((bf16[656,128]{1,0:T(8,128)(2,1)S(1)}, bf16[656,128]{1,0:T(8,128)(2,1)S(1)}, u32[]{:S(2)}, u32[]{:S(2)}) %collective-permute-start.1) | collective-permute-done | bytes 167968 | tf_op jit(solution)/shard_map/ppermute | solution.py:40
  16.8 4.6 %project_kept.1 = bf16[4,128,1792]{2,1,0:T(8,128)(2,1)} custom-call(s32[4]{0:T(128)} %pad_add_fusion.c_ref, bf16[64,1024]{1,0:T(8,128)(2,1)} %bitcast.81, bf16[1,64]{1,0:T(2,128)(2,1)} %bitcast.92, bf16[64,256]{1,0:T(8,128)(2,1)} %q_ref.3, bf16[64,256]{1,0:T(8,128)(2,1)} %k_ref.3, bf16[64,512]{1,0:T(8,128)(2,1)} %v_ref.3, bf16[64,512]{1,0:T(8,128)(2,1)} %o_ref.3, ...), custom_call_target="tpu_custom_call" | custom-call | flops 436207616 | bytes 3145728 | tf_op jit(solution)/shard_map/project_kept/pallas_call | solution.py:315
  21.4 4.9 %all-to-all-start = ((bf16[4,128,1792]{2,1,0:T(8,128)(2,1)}), bf16[4,128,1792]{2,1,0:T(8,128)(2,1)}, u32[]{:S(2)}, u32[]{:S(2)}) async-start(bf16[4,128,1792]{2,1,0:T(8,128)(2,1)} %project_kept.1), calls=%async_computation | async-start | bytes 3670016 | tf_op jit(solution)/shard_map/all_to_all | solution.py:24
  26.3 3.3 %collective-permute-start.6 = (bf16[656,128]{1,0:T(8,128)(2,1)S(1)}, bf16[656,128]{1,0:T(8,128)(2,1)S(1)}, u32[]{:S(2)}, u32[]{:S(2)}) collective-permute-start(bf16[656,128]{1,0:T(8,128)(2,1)S(1)} %collective-permute-done.5.refs_7_), channel_id=1, source_target_pairs={{0,224},{32,0},{64,32},{96,64},{128,96},{160,128},{192,160},{224,1... | collective-permute-start | bytes 503816 | tf_op jit(solution)/shard_map/ppermute | solution.py:43
  29.6 3.0 %collective-permute-done.6.refs_6_ = bf16[656,128]{1,0:T(8,128)(2,1)S(1)} collective-permute-done((bf16[656,128]{1,0:T(8,128)(2,1)S(1)}, bf16[656,128]{1,0:T(8,128)(2,1)S(1)}, u32[]{:S(2)}, u32[]{:S(2)}) %collective-permute-start.6) | collective-permute-done | bytes 167968 | tf_op jit(solution)/shard_map/ppermute | solution.py:43
  32.5 3.7 %collective-permute-start.7 = (bf16[656,128]{1,0:T(8,128)(2,1)S(1)}, bf16[656,128]{1,0:T(8,128)(2,1)S(1)}, u32[]{:S(2)}, u32[]{:S(2)}) collective-permute-start(bf16[656,128]{1,0:T(8,128)(2,1)S(1)} %collective-permute-done.6.refs_6_), channel_id=1, source_target_pairs={{0,224},{32,0},{64,32},{96,64},{128,96},{160,128},{192,160},{224,1... | collective-permute-start | bytes 503816 | tf_op jit(solution)/shard_map/ppermute | solution.py:43
  36.3 2.9 %collective-permute-done.7.refs_5_ = bf16[656,128]{1,0:T(8,128)(2,1)S(1)} collective-permute-done((bf16[656,128]{1,0:T(8,128)(2,1)S(1)}, bf16[656,128]{1,0:T(8,128)(2,1)S(1)}, u32[]{:S(2)}, u32[]{:S(2)}) %collective-permute-start.7) | collective-permute-done | bytes 167968 | tf_op jit(solution)/shard_map/ppermute | solution.py:43
  39.1 3.7 %collective-permute-done.4.refs_4_ = bf16[656,128]{1,0:T(8,128)(2,1)S(1)} collective-permute-done((bf16[656,128]{1,0:T(8,128)(2,1)S(1)}, bf16[656,128]{1,0:T(8,128)(2,1)S(1)}, u32[]{:S(2)}, u32[]{:S(2)}) %collective-permute-start.4) | collective-permute-done | bytes 167968 | tf_op jit(solution)/shard_map/ppermute | solution.py:40
  51.3 5.7 %all-to-all-start.1 = ((bf16[8,16,2176]{2,1,0:T(8,128)(2,1)}), bf16[8,16,2176]{2,1,0:T(8,128)(2,1)}, u32[]{:S(2)}, u32[]{:S(2)}) async-start(bf16[8,16,2176]{2,1,0:T(8,128)(2,1)} %fold_y.1), calls=%async_computation.1 | async-start | bytes 1114112 | tf_op jit(solution)/shard_map/all_to_all | solution.py:24
  58.5 16.1 %all-to-all-done.1.in_ref = bf16[8,16,2176]{2,1,0:T(8,128)(2,1)} async-done(((bf16[8,16,2176]{2,1,0:T(8,128)(2,1)}), bf16[8,16,2176]{2,1,0:T(8,128)(2,1)}, u32[]{:S(2)}, u32[]{:S(2)}) %all-to-all-start.1) | async-done | bytes 557088 | tf_op jit(solution)/shard_map/all_to_all | solution.py:24
  74.6 5.6 %recur.1 = (bf16[16,512]{1,0:T(8,128)(2,1)}, bf16[16,4096]{1,0:T(8,128)(2,1)}, f32[16,4,64,128]{3,2,1,0:T(8,128)}, f32[16,4,64]{2,1,0:T(4,128)}, f32[16,4]{1,0:T(8,128)}) custom-call(bf16[8,16,2176]{2,1,0:T(8,128)(2,1)} %all-to-all-done.1.in_ref, f32[1,4]{1,0:T(1,128)} %bitcast.93, f32[1,4]{1,0:T(1,128)} %bitcast.94, ...), custom_call_target="tpu_custom_call" | custom-call | flops 8388608 | bytes 5242880 | tf_op jit(solution)/shard_map/recur/pallas_call | solution.py:432
  91.2 6.9 %all-to-all-start.2 = ((bf16[16,16,1024]{2,1,0:T(8,128)(2,1)}), bf16[16,16,1024]{2,1,0:T(8,128)(2,1)}, u32[]{:S(2)}, u32[]{:S(2)}) async-start(bf16[16,16,1024]{2,1,0:T(8,128)(2,1)} %bitcast.76), calls=%async_computation.2 | async-start | bytes 1048576 | tf_op jit(solution)/shard_map/all_to_all | solution.py:24
  99.6 7.0 %all-to-all-done.2 = bf16[16,16,1024]{2,1,0:T(8,128)(2,1)} async-done(((bf16[16,16,1024]{2,1,0:T(8,128)(2,1)}), bf16[16,16,1024]{2,1,0:T(8,128)(2,1)}, u32[]{:S(2)}, u32[]{:S(2)}) %all-to-all-start.2) | async-done | bytes 524320 | tf_op jit(solution)/shard_map/all_to_all | solution.py:24
  106.5 3.5 %settle.1 = (bf16[16,4096]{1,0:T(8,128)(2,1)}, f32[16,128]{1,0:T(8,128)}, bf16[64,2,4096]{2,1,0:T(2,128)(2,1)}, bf16[16,1024]{1,0:T(8,128)(2,1)}, bf16[16,1024]{...) custom-call(s32[4]{0:T(128)} %pad_add_fusion.c_ref, bf16[4,4,16,1024]{3,2,1,0:T(8,128)(2,1)} %bitcast.17.got_ref, ...), custom_call_target="tpu_custom_call" | custom-call | flops 134217728 | bytes 3145728 | tf_op jit(solution)/shard_map/settle/pallas_call | solution.py:144
  110.1 7.2 %all-to-all-start.3 = ((bf16[64,2,4096]{2,1,0:T(2,128)(2,1)}), bf16[64,2,4096]{2,1,0:T(2,128)(2,1)}, u32[]{:S(2)}, u32[]{:S(2)}) async-start(bf16[64,2,4096]{2,1,0:T(2,128)(2,1)} %get-tuple-element.30), calls=%async_computation.3 | async-start | bytes 2097152 | tf_op jit(solution)/shard_map/all_to_all | solution.py:24
  122.1 3.4 %collective-permute-done.13.x2 = bf16[16,1024]{1,0:T(8,128)(2,1)S(1)} collective-permute-done((bf16[16,1024]{1,0:T(8,128)(2,1)}, bf16[16,1024]{1,0:T(8,128)(2,1)S(1)}, u32[]{:S(2)}, u32[]{:S(2)}) %collective-permute-start.13) | collective-permute-done | bytes 32800 | tf_op jit(solution)/shard_map/ppermute | solution.py:640
  139.5 3.0 %collective-permute-done.19.x2 = bf16[16,256]{1,0:T(8,128)(2,1)S(1)} collective-permute-done((bf16[16,256]{1,0:T(8,128)(2,1)S(1)}, bf16[16,256]{1,0:T(8,128)(2,1)S(1)}, u32[]{:S(2)}, u32[]{:S(2)}) %collective-permute-start.19) | collective-permute-done | bytes 8224 | tf_op jit(solution)/shard_map/ppermute | solution.py:651
  148.0 2.6 %collective-permute-start.23 = (bf16[16,1024]{1,0:T(8,128)(2,1)S(1)}, bf16[16,1024]{1,0:T(8,128)(2,1)S(1)}, u32[]{:S(2)}, u32[]{:S(2)}) collective-permute-start(bf16[16,1024]{1,0:T(8,128)(2,1)S(1)} %get-tuple-element.45), channel_id=1, source_target_pairs={{0,8},{8,16},{16,24},{24,0},{1,9},{9,17},{17,25},{25,1},{2,10},{10... | collective-permute-start | bytes 98312 | tf_op jit(solution)/shard_map/ppermute | solution.py:656
  155.3 3.1 %down.1 = bf16[64,72,128]{2,1,0:T(8,128)(2,1)} custom-call(s32[4]{0:T(128)S(1)} %copy-done.7, bf16[128,256]{1,0:T(8,128)(2,1)S(1)} %fusion.15.h_ref, bf16[256,4096]{1,0:T(8,128)(2,1)S(1)} %bitcast.73, bf16[16,4096]{1,0:T(8,128)(2,1)S(1)} %copy-done.5, bf16[16,1024]{1,0:T(8,128)(2,1)S(1)} %get-tuple-element.42.d0, ...), custom_call_target="tpu_custom_call" | custom-call | flops 268435456 | bytes 4194304 | tf_op jit(solution)/shard_map/down/pallas_call | solution.py:248
  158.4 9.5 %all-to-all-start.4 = ((bf16[64,72,128]{2,1,0:T(8,128)(2,1)}), bf16[64,72,128]{2,1,0:T(8,128)(2,1)}, u32[]{:S(2)}, u32[]{:S(2)}) async-start(bf16[64,72,128]{2,1,0:T(8,128)(2,1)} %down.1), calls=%async_computation.4 | async-start | bytes 2359296 | tf_op jit(solution)/shard_map/all_to_all | solution.py:24
  170.9 28.5 %all-to-all-done.4 = bf16[64,72,128]{2,1,0:T(8,128)(2,1)} async-done(((bf16[64,72,128]{2,1,0:T(8,128)(2,1)}), bf16[64,72,128]{2,1,0:T(8,128)(2,1)}, u32[]{:S(2)}, u32[]{:S(2)}) %all-to-all-start.4) | async-done | bytes 1179680 | tf_op jit(solution)/shard_map/all_to_all | solution.py:24
  207.9 4.0 %collective-permute-done.24.b1 = bf16[512,128]{1,0:T(8,128)(2,1)S(1)} collective-permute-done((bf16[512,128]{1,0:T(8,128)(2,1)S(1)}, bf16[512,128]{1,0:T(8,128)(2,1)S(1)}, u32[]{:S(2)}, u32[]{:S(2)}) %collective-permute-start.24) | collective-permute-done | bytes 131104 | tf_op jit(solution)/shard_map/ppermute | solution.py:673
  (172 shorter events, 68.2 us)
Async XLA Ops:
  4.9 11.9 %collective-permute-start = (bf16[4,128,1664]{2,1,0:T(8,128)(2,1)}, bf16[4,128,1664]{2,1,0:T(8,128)(2,1)}, u32[]{:S(2)}, u32[]{:S(2)}) collective-permute-start(bf16[4,128,1664]{2,1,0:T(8,128)(2,1)} %project_away.1), channel_id=1, source_target_pairs={{0,4},{4,0},{1,5},{5,1},{2,6},{6,2},{3,7},{7,3},{8,12},{12,8},{9,1... | collective-permute-start | bytes 5111816 | tf_op jit(solution)/shard_map/ppermute | solution.py:28
  5.9 10.9 %collective-permute-start.1 = (bf16[656,128]{1,0:T(8,128)(2,1)S(1)}, bf16[656,128]{1,0:T(8,128)(2,1)S(1)}, u32[]{:S(2)}, u32[]{:S(2)}) collective-permute-start(bf16[656,128]{1,0:T(8,128)(2,1)S(1)} %concatenate.20.refs_0_), channel_id=1, source_target_pairs={{0,32},{32,64},{64,96},{96,128},{128,160},{160,192},{192,224},{224... | collective-permute-start | bytes 503816 | tf_op jit(solution)/shard_map/ppermute | solution.py:40
  7.9 18.4 %collective-permute-start.5 = (bf16[656,128]{1,0:T(8,128)(2,1)S(1)}, bf16[656,128]{1,0:T(8,128)(2,1)S(1)}, u32[]{:S(2)}, u32[]{:S(2)}) collective-permute-start(bf16[656,128]{1,0:T(8,128)(2,1)S(1)} %concatenate.20.refs_0_), channel_id=1, source_target_pairs={{0,224},{32,0},{64,32},{96,64},{128,96},{160,128},{192,160},{224,1... | collective-permute-start | bytes 503816 | tf_op jit(solution)/shard_map/ppermute | solution.py:43
  16.8 12.8 %collective-permute-start.2 = (bf16[656,128]{1,0:T(8,128)(2,1)S(1)}, bf16[656,128]{1,0:T(8,128)(2,1)S(1)}, u32[]{:S(2)}, u32[]{:S(2)}) collective-permute-start(bf16[656,128]{1,0:T(8,128)(2,1)S(1)} %collective-permute-done.1.refs_1_), channel_id=1, source_target_pairs={{0,32},{32,64},{64,96},{96,128},{128,160},{160,192},{192,224},{224... | collective-permute-start | bytes 503816 | tf_op jit(solution)/shard_map/ppermute | solution.py:40
  21.4 27.4 %all-to-all-start = ((bf16[4,128,1792]{2,1,0:T(8,128)(2,1)}), bf16[4,128,1792]{2,1,0:T(8,128)(2,1)}, u32[]{:S(2)}, u32[]{:S(2)}) async-start(bf16[4,128,1792]{2,1,0:T(8,128)(2,1)} %project_kept.1), calls=%async_computation | async-start | bytes 3670016 | tf_op jit(solution)/shard_map/all_to_all | solution.py:24
  26.3 6.2 %collective-permute-start.6 = (bf16[656,128]{1,0:T(8,128)(2,1)S(1)}, bf16[656,128]{1,0:T(8,128)(2,1)S(1)}, u32[]{:S(2)}, u32[]{:S(2)}) collective-permute-start(bf16[656,128]{1,0:T(8,128)(2,1)S(1)} %collective-permute-done.5.refs_7_), channel_id=1, source_target_pairs={{0,224},{32,0},{64,32},{96,64},{128,96},{160,128},{192,160},{224,1... | collective-permute-start | bytes 503816 | tf_op jit(solution)/shard_map/ppermute | solution.py:43
  29.6 6.7 %collective-permute-start.3 = (bf16[656,128]{1,0:T(8,128)(2,1)S(1)}, bf16[656,128]{1,0:T(8,128)(2,1)S(1)}, u32[]{:S(2)}, u32[]{:S(2)}) collective-permute-start(bf16[656,128]{1,0:T(8,128)(2,1)S(1)} %collective-permute-done.2.refs_2_), channel_id=1, source_target_pairs={{0,32},{32,64},{64,96},{96,128},{128,160},{160,192},{192,224},{224... | collective-permute-start | bytes 503816 | tf_op jit(solution)/shard_map/ppermute | solution.py:40
  32.5 6.6 %collective-permute-start.7 = (bf16[656,128]{1,0:T(8,128)(2,1)S(1)}, bf16[656,128]{1,0:T(8,128)(2,1)S(1)}, u32[]{:S(2)}, u32[]{:S(2)}) collective-permute-start(bf16[656,128]{1,0:T(8,128)(2,1)S(1)} %collective-permute-done.6.refs_6_), channel_id=1, source_target_pairs={{0,224},{32,0},{64,32},{96,64},{128,96},{160,128},{192,160},{224,1... | collective-permute-start | bytes 503816 | tf_op jit(solution)/shard_map/ppermute | solution.py:43
  36.2 6.6 %collective-permute-start.4 = (bf16[656,128]{1,0:T(8,128)(2,1)S(1)}, bf16[656,128]{1,0:T(8,128)(2,1)S(1)}, u32[]{:S(2)}, u32[]{:S(2)}) collective-permute-start(bf16[656,128]{1,0:T(8,128)(2,1)S(1)} %collective-permute-done.3.refs_3_), channel_id=1, source_target_pairs={{0,32},{32,64},{64,96},{96,128},{128,160},{160,192},{192,224},{224... | collective-permute-start | bytes 503816 | tf_op jit(solution)/shard_map/ppermute | solution.py:40
  46.1 10.9 %collective-permute-start.8 = (bf16[8,656,128]{2,1,0:T(8,128)(2,1)}, bf16[8,656,128]{2,1,0:T(8,128)(2,1)}, u32[]{:S(2)}, u32[]{:S(2)}) collective-permute-start(bf16[8,656,128]{2,1,0:T(8,128)(2,1)} %stacked.1.mine_ref), channel_id=1, source_target_pairs={{0,4},{4,0},{1,5},{5,1},{2,6},{6,2},{3,7},{7,3},{8,12},{12,8},{9,1... | collective-permute-start | bytes 4030472 | tf_op jit(solution)/shard_map/ppermute | solution.py:28
  51.3 23.3 %all-to-all-start.1 = ((bf16[8,16,2176]{2,1,0:T(8,128)(2,1)}), bf16[8,16,2176]{2,1,0:T(8,128)(2,1)}, u32[]{:S(2)}, u32[]{:S(2)}) async-start(bf16[8,16,2176]{2,1,0:T(8,128)(2,1)} %fold_y.1), calls=%async_computation.1 | async-start | bytes 1114112 | tf_op jit(solution)/shard_map/all_to_all | solution.py:24
  80.9 7.5 %collective-permute-start.11 = (bf16[24,512]{1,0:T(8,128)(2,1)S(1)}, bf16[24,512]{1,0:T(8,128)(2,1)S(1)}, u32[]{:S(2)}, u32[]{:S(2)}) collective-permute-start(bf16[24,512]{1,0:T(8,128)(2,1)S(1)} %maximum_maximum_fusion.x0), channel_id=1, source_target_pairs={{0,24},{8,0},{16,8},{24,16},{1,25},{9,1},{17,9},{25,17},{2,26},{10... | collective-permute-start | bytes 73736 | tf_op jit(solution)/shard_map/ppermute | solution.py:626
  81.7 6.8 %collective-permute-start.10 = (bf16[24,512]{1,0:T(8,128)(2,1)S(1)}, bf16[24,512]{1,0:T(8,128)(2,1)S(1)}, u32[]{:S(2)}, u32[]{:S(2)}) collective-permute-start(bf16[24,512]{1,0:T(8,128)(2,1)S(1)} %maximum_maximum_fusion.x0), channel_id=1, source_target_pairs={{0,16},{8,24},{16,0},{24,8},{1,17},{9,25},{17,1},{25,9},{2,18},{10... | collective-permute-start | bytes 73736 | tf_op jit(solution)/shard_map/ppermute | solution.py:626
  91.2 15.3 %all-to-all-start.2 = ((bf16[16,16,1024]{2,1,0:T(8,128)(2,1)}), bf16[16,16,1024]{2,1,0:T(8,128)(2,1)}, u32[]{:S(2)}, u32[]{:S(2)}) async-start(bf16[16,16,1024]{2,1,0:T(8,128)(2,1)} %bitcast.76), calls=%async_computation.2 | async-start | bytes 1048576 | tf_op jit(solution)/shard_map/all_to_all | solution.py:24
  110.1 40.6 %all-to-all-start.3 = ((bf16[64,2,4096]{2,1,0:T(2,128)(2,1)}), bf16[64,2,4096]{2,1,0:T(2,128)(2,1)}, u32[]{:S(2)}, u32[]{:S(2)}) async-start(bf16[64,2,4096]{2,1,0:T(2,128)(2,1)} %get-tuple-element.30), calls=%async_computation.3 | async-start | bytes 2097152 | tf_op jit(solution)/shard_map/all_to_all | solution.py:24
  118.9 6.6 %collective-permute-start.13 = (bf16[16,1024]{1,0:T(8,128)(2,1)}, bf16[16,1024]{1,0:T(8,128)(2,1)S(1)}, u32[]{:S(2)}, u32[]{:S(2)}) collective-permute-start(bf16[16,1024]{1,0:T(8,128)(2,1)} %get-tuple-element.35), channel_id=1, source_target_pairs={{0,16},{8,24},{16,0},{24,8},{1,17},{9,25},{17,1},{25,9},{2,18},{10... | collective-permute-start | bytes 98312 | tf_op jit(solution)/shard_map/ppermute | solution.py:640
  127.4 5.7 %collective-permute-start.15 = (bf16[16,512]{1,0:T(8,128)(2,1)S(1)}, bf16[16,512]{1,0:T(8,128)(2,1)S(1)}, u32[]{:S(2)}, u32[]{:S(2)}) collective-permute-start(bf16[16,512]{1,0:T(8,128)(2,1)S(1)} %get-tuple-element.38), channel_id=1, source_target_pairs={{0,24},{8,0},{16,8},{24,16},{1,25},{9,1},{17,9},{25,17},{2,26},{10... | collective-permute-start | bytes 49160 | tf_op jit(solution)/shard_map/ppermute | solution.py:644
  145.2 9.0 %collective-permute-start.21 = (bf16[16,1024]{1,0:T(8,128)(2,1)}, bf16[16,1024]{1,0:T(8,128)(2,1)S(1)}, u32[]{:S(2)}, u32[]{:S(2)}) collective-permute-start(bf16[16,1024]{1,0:T(8,128)(2,1)} %get-tuple-element.43), channel_id=1, source_target_pairs={{0,24},{8,0},{16,8},{24,16},{1,25},{9,1},{17,9},{25,17},{2,26},{10... | collective-permute-start | bytes 98312 | tf_op jit(solution)/shard_map/ppermute | solution.py:656
  145.7 8.5 %collective-permute-start.22 = (bf16[16,1024]{1,0:T(8,128)(2,1)S(1)}, bf16[16,1024]{1,0:T(8,128)(2,1)S(1)}, u32[]{:S(2)}, u32[]{:S(2)}) collective-permute-start(bf16[16,1024]{1,0:T(8,128)(2,1)S(1)} %get-tuple-element.44), channel_id=1, source_target_pairs={{0,16},{8,24},{16,0},{24,8},{1,17},{9,25},{17,1},{25,9},{2,18},{10... | collective-permute-start | bytes 98312 | tf_op jit(solution)/shard_map/ppermute | solution.py:656
  148.0 6.2 %collective-permute-start.23 = (bf16[16,1024]{1,0:T(8,128)(2,1)S(1)}, bf16[16,1024]{1,0:T(8,128)(2,1)S(1)}, u32[]{:S(2)}, u32[]{:S(2)}) collective-permute-start(bf16[16,1024]{1,0:T(8,128)(2,1)S(1)} %get-tuple-element.45), channel_id=1, source_target_pairs={{0,8},{8,16},{16,24},{24,0},{1,9},{9,17},{17,25},{25,1},{2,10},{10... | collective-permute-start | bytes 98312 | tf_op jit(solution)/shard_map/ppermute | solution.py:656
  158.4 41.0 %all-to-all-start.4 = ((bf16[64,72,128]{2,1,0:T(8,128)(2,1)}), bf16[64,72,128]{2,1,0:T(8,128)(2,1)}, u32[]{:S(2)}, u32[]{:S(2)}) async-start(bf16[64,72,128]{2,1,0:T(8,128)(2,1)} %down.1), calls=%async_computation.4 | async-start | bytes 2359296 | tf_op jit(solution)/shard_map/all_to_all | solution.py:24
  203.7 8.1 %collective-permute-start.24 = (bf16[512,128]{1,0:T(8,128)(2,1)S(1)}, bf16[512,128]{1,0:T(8,128)(2,1)S(1)}, u32[]{:S(2)}, u32[]{:S(2)}) collective-permute-start(bf16[512,128]{1,0:T(8,128)(2,1)S(1)} %pad_maximum_fusion.b0), channel_id=1, source_target_pairs={{0,1},{1,2},{2,3},{3,0},{4,5},{5,6},{6,7},{7,4},{8,9},{9,10},{10,1... | collective-permute-start | bytes 393224 | tf_op jit(solution)/shard_map/ppermute | solution.py:673
  204.4 7.5 %collective-permute-start.25 = (bf16[512,128]{1,0:T(8,128)(2,1)S(1)}, bf16[512,128]{1,0:T(8,128)(2,1)S(1)}, u32[]{:S(2)}, u32[]{:S(2)}) collective-permute-start(bf16[512,128]{1,0:T(8,128)(2,1)S(1)} %pad_maximum_fusion.b0), channel_id=1, source_target_pairs={{0,2},{1,3},{2,0},{3,1},{4,6},{5,7},{6,4},{7,5},{8,10},{9,11},{10,... | collective-permute-start | bytes 393224 | tf_op jit(solution)/shard_map/ppermute | solution.py:673
  205.7 6.8 %collective-permute-start.26 = (bf16[512,128]{1,0:T(8,128)(2,1)S(1)}, bf16[512,128]{1,0:T(8,128)(2,1)S(1)}, u32[]{:S(2)}, u32[]{:S(2)}) collective-permute-start(bf16[512,128]{1,0:T(8,128)(2,1)S(1)} %pad_maximum_fusion.b0), channel_id=1, source_target_pairs={{0,3},{1,0},{2,1},{3,2},{4,7},{5,4},{6,5},{7,6},{8,11},{9,8},{10,9... | collective-permute-start | bytes 393224 | tf_op jit(solution)/shard_map/ppermute | solution.py:673
  (38 other events, 503.7 us)

commit v3 on v2

--- a/solution.py
+++ b/solution.py
@@ -71,41 +71,43 @@
         res.append((top + pltpu.roll(low, 64, 1), pltpu.roll(top, 64, 1) + low))
     first = jnp.where(c == 0, res[0][0], res[1][0])
     second = jnp.where(c == 0, res[1][1], res[0][1])
-    return jnp.where(lane < 64, first, second).astype(BF16)
-
-
-def mix_kernel(c_ref, x0, x1, x2, x3, mine_ref, away_ref, out_ref):
+    return jnp.where(lane < 64, first, second)
+
+
+def mix_kernel(c_ref, x0, x1, x2, x3, tok_ref, mine_ref, away_ref, out_ref):
     c = c_ref[0]
     xs = (x0, x1, x2, x3)
     both = jnp.concatenate([r[:16, :256] for r in xs] + [r[:16, 256:] for r in xs], axis=0)
     for z in range(NZ):
         w = jnp.concatenate([mine_ref[z, :256, :], away_ref[z, :256, :]], axis=1)
         tile = both_kinds(c, jnp.dot(both, w, preferred_element_type=F32), 64)
+        tok = tok_ref[:, turned_z(c_ref, z)].astype(F32)
         for s in range(NY):
             to = lax.rem(c_ref[1] + (NY - s), NY)
-            out_ref[to, :, turned_z(c_ref, z)] = tile[s * 16 : (s + 1) * 16]
+            rows = tile[s * 16 : (s + 1) * 16] + jnp.where(to == c_ref[3], tok, 0.0)
+            out_ref[to, :, turned_z(c_ref, z)] = rows.astype(BF16)
 
 
 VMEM = pl.BlockSpec(memory_space=pltpu.VMEM)
 SMEM = pl.BlockSpec(memory_space=pltpu.SMEM)
 
 
-def mix(c, heads, mine, away):
+def mix(c, heads, tok, mine, away):
     return pl.pallas_call(
         mix_kernel,
         out_shape=jax.ShapeDtypeStruct((NY, 16, 1024), BF16),
-        in_specs=[SMEM] + [VMEM] * 6,
+        in_specs=[SMEM] + [VMEM] * 7,
         out_specs=VMEM,
         compiler_params=pltpu.CompilerParams(vmem_limit_bytes=LIMIT),
         cost_estimate=pl.CostEstimate(
             flops=2 * 128 * 256 * 128 * 16, bytes_accessed=2 << 20, transcendentals=0
         ),
         name="mix",
-    )(c, *heads, mine, away)
+    )(c, *heads, tok, mine, away)
 
 
 def settle_kernel(
-    c_ref, got_ref, tok_ref, gain_ref, mix_ref, spread_ref,
+    c_ref, got_ref, gain_ref, mix_ref, spread_ref,
     hid_ref, gate_ref, send_ref, n0_ref, n1_ref, n2_ref, n3_ref, norm_ref,
 ):
     square = jnp.zeros((16, 1), F32)
@@ -114,11 +116,10 @@
         total = got_ref[y, 0].astype(F32)
         for x in range(1, NX):
             total += got_ref[y, x].astype(F32)
-        total = total.astype(BF16).astype(F32)
         for z in range(NZ):
             at = (z * NY + y) * 128
             cols = slice(at, at + 128)
-            hid = (tok_ref[:, cols].astype(F32) + total[:, z * 128 : (z + 1) * 128]).astype(BF16)
+            hid = total[:, z * 128 : (z + 1) * 128].astype(BF16)
             hid_ref[:, cols] = hid
             wide = hid.astype(F32)
             square += jnp.sum(wide * wide, axis=1, keepdims=True)
@@ -139,7 +140,7 @@
             out[:, z * 128 : (z + 1) * 128] = norm_ref[:, pl.ds(at, 128)]
 
 
-def settle(c, got, tok, gain, mix_row, spread):
+def settle(c, got, gain, mix_row, spread):
     part = jax.ShapeDtypeStruct((16, 1024), BF16)
     return pl.pallas_call(
         settle_kernel,
@@ -149,17 +150,17 @@
             jax.ShapeDtypeStruct((64, 2, D), BF16),
             part, part, part, part,
         ),
-        in_specs=[SMEM] + [VMEM] * 5,
+        in_specs=[SMEM] + [VMEM] * 4,
         out_specs=(VMEM,) * 7,
         scratch_shapes=[pltpu.VMEM((16, D), BF16)],
         cost_estimate=pl.CostEstimate(
             flops=2 * 128 * 128 * 4096, bytes_accessed=3 << 20, transcendentals=0
         ),
         name="settle",
-    )(c, got, tok, gain, mix_row, spread)
-
-
-def dense_kernel(c_ref, x0, x1, x2, x3, mine_ref, away_ref, o0, o1, o2, o3):
+    )(c, got, gain, mix_row, spread)
+
+
+def dense_kernel(c_ref, x0, x1, x2, x3, mine_ref, away_ref, out_ref):
     c = c_ref[0]
     acc = jnp.zeros((64, 512), F32)
     for z in range(NZ):
@@ -172,17 +173,15 @@
                 [ref[z, 272 + j * 64 : 336 + j * 64, :] for j in range(4)], axis=1
             )
             acc += jnp.dot(part, w, preferred_element_type=F32)
-    for s, out in enumerate((o0, o1, o2, o3)):
-        out[...] = acc[s * 16 : (s + 1) * 16].astype(BF16)
+    out_ref[...] = acc.astype(BF16)
 
 
 def dense_products(c, xs, mine, away):
-    part = jax.ShapeDtypeStruct((16, 512), BF16)
     return pl.pallas_call(
         dense_kernel,
-        out_shape=(part,) * 4,
+        out_shape=jax.ShapeDtypeStruct((64, 512), BF16),
         in_specs=[SMEM] + [VMEM] * 6,
-        out_specs=(VMEM,) * 4,
+        out_specs=VMEM,
         compiler_params=pltpu.CompilerParams(vmem_limit_bytes=LIMIT),
         cost_estimate=pl.CostEstimate(
             flops=2 * 64 * 1024 * 512, bytes_accessed=2 << 20, transcendentals=0
@@ -194,12 +193,20 @@
 def dense_down_kernel(c_ref, x0, x1, x2, x3, mine_ref, away_ref, o0, o1, o2, o3):
     c = c_ref[0]
     xs = (x0, x1, x2, x3)
-    both = jnp.concatenate([r[:, :128] for r in xs] + [r[:, 128:] for r in xs], axis=0)
+    units = []
+    for s in range(NY):
+        total = jnp.zeros((16, 512), F32)
+        for k in range(NY):
+            j = (s - k) % NY
+            total += xs[k][j * 16 : (j + 1) * 16, :].astype(F32)
+        gate = total[:, :256]
+        units.append((gate / (1.0 + jnp.exp(-gate)) * total[:, 256:]).astype(BF16))
+    both = jnp.concatenate([u[:, :128] for u in units] + [u[:, 128:] for u in units], axis=0)
     for z in range(NZ):
         w = jnp.concatenate([mine_ref[z, 528:656, :], away_ref[z, 528:656, :]], axis=1)
         tile = both_kinds(c, jnp.dot(both, w, preferred_element_type=F32), 64)
         for s, out in enumerate((o0, o1, o2, o3)):
-            out[:, turned_z(c_ref, z)] = tile[s * 16 : (s + 1) * 16]
+            out[:, turned_z(c_ref, z)] = tile[s * 16 : (s + 1) * 16].astype(BF16)
 
 
 def dense_down(c, xs, mine, away):
@@ -226,7 +233,7 @@
     )
 
 
-def down_kernel(c_ref, h_ref, w_ref, hid_ref, d0, d1, d2, d3, out_ref):
+def down_kernel(c_ref, h_ref, w_ref, hid_ref, gate_ref, d0, d1, d2, d3, out_ref):
     res = jnp.dot(h_ref[...], w_ref[...], preferred_element_type=F32)
     lane = lax.broadcasted_iota(jnp.int32, (64, 128), 1)
     for p in range(8):
@@ -239,12 +246,13 @@
         for s, d in enumerate((d0, d1, d2, d3)):
             at = zl * NY + lax.rem(c_ref[1] + s, NY)
             hid = hid_ref[:, pl.ds(pl.multiple_of(at * 128, 128), 128)].astype(F32)
-            wide = d[:, zl * 128 : (zl + 1) * 128].astype(F32) + jnp.where(quarter, hid, 0.0)
+            dense = d[:, zl * 128 : (zl + 1) * 128].astype(F32) * gate_ref[...]
+            wide = dense + jnp.where(quarter, hid, 0.0)
             for k, half in enumerate(half_rows(wide)):
                 out_ref[2 * at + k, 64:] = half.astype(BF16)
 
 
-def down_for_all(c, expert_hidden, w, hidden, downs):
+def down_for_all(c, expert_hidden, w, hidden, gate, downs):
     return pl.pallas_call(
         down_kernel,
         grid=(4,),
@@ -254,6 +262,7 @@
             pl.BlockSpec((128, 256), lambda i: (0, 0)),
             pl.BlockSpec((256, 1024), lambda i: (0, i)),
             pl.BlockSpec((16, 1024), lambda i: (0, i)),
+            pl.BlockSpec((16, 128), lambda i: (0, 0)),
         ]
         + [pl.BlockSpec((16, 256), lambda i: (0, i))] * 4,
         out_specs=pl.BlockSpec((16, 72, 128), lambda i: (i, 0, 0)),
@@ -262,11 +271,11 @@
             flops=2 * 128 * 256 * 4096, bytes_accessed=4 << 20, transcendentals=0
         ),
         name="down",
-    )(c, expert_hidden, w, hidden, *downs)
+    )(c, expert_hidden, w, hidden, gate, *downs)
 
 
 def project_kernel(kept, c_ref, tok_ref, gain_ref, q_ref, k_ref, v_ref, o_ref, i_ref, f_ref, *refs):
-    got_ref, out, all_ref, x_ref = refs if kept else (None, *refs)
+    got_ref, out, tile_ref, all_ref, x_ref = refs if kept else (None, refs[0], None, *refs[1:])
     c = c_ref[0]
     core = c if kept else 1 - c
     y = pl.program_id(0)
@@ -304,22 +313,25 @@
     else:
         other = got_ref[:, 1536:].astype(F32)
         out[0, :, 1536:1664] = (last + other).astype(BF16)
-        first = jnp.where(c == 0, last, other)
-        second = jnp.where(c == 0, other, last)
-        out[0, :, 1664:] = jnp.where(lane < 64, first, pltpu.roll(second, 64, 1)).astype(BF16)
+
+        @pl.when(y == c_ref[3])
+        def _():
+            first = jnp.where(c == 0, last, other)
+            second = jnp.where(c == 0, other, last)
+            tile_ref[...] = jnp.where(lane < 64, first, pltpu.roll(second, 64, 1)).astype(BF16)
 
 
 def project(kept, *args):
     whole = lambda *shape: pl.BlockSpec(shape, lambda g: (0,) * len(shape))
-    wide = 1792 if kept else 1664
     return pl.pallas_call(
         functools.partial(project_kernel, kept),
         grid=(NY,),
-        out_shape=jax.ShapeDtypeStruct((NY, 128, wide), BF16),
+        out_shape=(jax.ShapeDtypeStruct((NY, 128, 1664), BF16),)
+        + (jax.ShapeDtypeStruct((128, 128), BF16),) * kept,
         in_specs=[SMEM]
         + [whole(*a.shape) for a in args[1:9]]
         + [pl.BlockSpec((None, 128, 1664), lambda g: (g, 0, 0))] * kept,
-        out_specs=pl.BlockSpec((1, 128, wide), lambda g: (g, 0, 0)),
+        out_specs=(pl.BlockSpec((1, 128, 1664), lambda g: (g, 0, 0)),) + (whole(128, 128),) * kept,
         scratch_shapes=[pltpu.VMEM((1024, 64), BF16), pltpu.VMEM((128, 64), BF16)],
         cost_estimate=pl.CostEstimate(
             flops=2 * 512 * 256 * 1664, bytes_accessed=3 << 20, transcendentals=0
@@ -328,29 +340,27 @@
     )(*args)
 
 
-def fold_y_kernel(in_ref, out_ref):
+def fold_y_kernel(in_ref, tile_ref, out_ref):
     for z in range(NZ):
         rows = slice(z * 16, (z + 1) * 16)
-        total = in_ref[0, rows, :1664].astype(F32)
+        total = in_ref[0, rows, :].astype(F32)
         for y in range(1, NY):
-            total += in_ref[y, rows, :1664].astype(F32)
+            total += in_ref[y, rows, :].astype(F32)
         out_ref[z, :, :1664] = total.astype(BF16)
-        for y in range(NY):
-            at = 1664 + y * 128
-            out_ref[z, :, at : at + 128] = in_ref[y, rows, 1664:]
-
-
-def fold_y(x):
+        out_ref[z, :, 1664:] = tile_ref[rows, :]
+
+
+def fold_y(x, tile):
     return pl.pallas_call(
         fold_y_kernel,
-        out_shape=jax.ShapeDtypeStruct((NZ, 16, 2176), BF16),
-        in_specs=[VMEM],
+        out_shape=jax.ShapeDtypeStruct((NZ, 16, 1792), BF16),
+        in_specs=[VMEM, VMEM],
         out_specs=VMEM,
         cost_estimate=pl.CostEstimate(
             flops=1 << 20, bytes_accessed=3 << 20, transcendentals=0
         ),
         name="fold_y",
-    )(x)
+    )(x, tile)
 
 
 def recur_kernel(
@@ -366,9 +376,7 @@
         for z in range(1, NZ):
             total += in_ref[z, :, :1664].astype(F32)
         for z in range(NZ):
-            for y in range(NY):
-                at, src = (z * NY + y) * 128, 1664 + y * 128
-                tok_ref[:, at : at + 128] = in_ref[z, :, src : src + 128]
+            tok_ref[:, z * 128 : (z + 1) * 128] = in_ref[z, :, 1664:]
         inverse = lax.rsqrt(total[:, 1608:1609] / D + EPSILON)
         total = total * inverse
         q = total[:, :256].astype(BF16).astype(F32) * 0.125
@@ -434,16 +442,16 @@
         grid=(4,),
         out_shape=(
             jax.ShapeDtypeStruct((16, 512), BF16),
-            jax.ShapeDtypeStruct((16, D), BF16),
+            jax.ShapeDtypeStruct((16, 1024), BF16),
             jax.ShapeDtypeStruct((16, 4, 64, 128), F32),
             jax.ShapeDtypeStruct((16, 4, 64), F32),
             jax.ShapeDtypeStruct((16, 4), F32),
         ),
         in_specs=[
-            whole(NZ, 16, 2176), whole(1, 4), whole(1, 4), whole(1, 512),
+            whole(NZ, 16, 1792), whole(1, 4), whole(1, 4), whole(1, 512),
             block, whole(16, 4, 64), whole(16, 4),
         ],
-        out_specs=(whole(16, 512), whole(16, D), block, whole(16, 4, 64), whole(16, 4)),
+        out_specs=(whole(16, 512), whole(16, 1024), block, whole(16, 4, 64), whole(16, 4)),
         scratch_shapes=[
             pltpu.VMEM((4, 256, 4), F32),
             pltpu.VMEM((4, 256, 4), F32),
@@ -532,6 +540,39 @@
         cost_estimate=pl.CostEstimate(flops=1 << 24, bytes_accessed=2 << 20, transcendentals=0),
         name="picks",
     )(target)
+
+
+def combine_kernel(got_ref, pick_ref, out_ref):
+    lane = lax.broadcasted_iota(jnp.int32, (128, 128), 1)
+    lane8 = lax.broadcasted_iota(jnp.int32, (8, 128), 1)
+    for g in range(4):
+        source = got_ref[:, g * 16 : (g + 1) * 16, :].reshape(1024, 128)
+        first, second = (
+            lax.dot_general(
+                pick_ref[h * 4 + g], source, (((0,), (0,)), ((), ())), preferred_element_type=F32
+            )
+            for h in range(2)
+        )
+        rows = []
+        for b in range(g * 8, g * 8 + 8):
+            left = got_ref[b, 64:, :].astype(F32)
+            right = got_ref[b + 32, 64:, :].astype(F32)
+            rows.append(jnp.where(lane8 < 64, left, pltpu.roll(right, 64, 1)))
+            rows.append(jnp.where(lane8 < 64, pltpu.roll(left, 64, 1), right))
+        routed = jnp.where(lane < 64, first, second)
+        out_ref[g * 128 : (g + 1) * 128, :] = (routed + jnp.concatenate(rows, axis=0)).astype(BF16)
+
+
+def combine(returned, pick):
+    return pl.pallas_call(
+        combine_kernel,
+        out_shape=jax.ShapeDtypeStruct((512, 128), BF16),
+        in_specs=[VMEM, VMEM],
+        out_specs=VMEM,
+        compiler_params=pltpu.CompilerParams(vmem_limit_bytes=LIMIT),
+        cost_estimate=pl.CostEstimate(flops=1 << 28, bytes_accessed=3 << 20, transcendentals=0),
+        name="combine",
+    )(returned, pick)
 
 
 def finish_kernel(c_ref, b0, b1, b2, b3, out_ref):
@@ -608,11 +649,11 @@
     operands = (
         c_ref, tokens.T, mix_gain[None], w_query, w_key, w_value, w_outgate, w_igate.T, w_fgate.T
     )
-    away = project(False, *operands)
+    (away,) = project(False, *operands)
     got = other_core(away)
-    folded = project(True, *operands, got)
+    folded, tile = project(True, *operands, got)
     folded = exchanged(folded, "y")
-    folded = fold_y(folded)
+    folded = fold_y(folded, tile)
     folded = exchanged(folded, "z")
     heads_out, tok, new_matrix, new_norm, new_max = recur(
         folded, igate_bias, fgate_bias, head_gain, state_matrix, state_norm, state_max
@@ -628,47 +669,31 @@
     vectors = jnp.stack([h[16:20] for h in heads])[(y - jnp.arange(NY)) % NY]
     vectors = vectors.reshape(NY, 2, NZ, 128).transpose(1, 2, 0, 3).reshape(2, 1, D)
     vectors = vectors.astype(F32)
-    partial = mix(c_ref, heads, mine, away)
+    partial = mix(c_ref, heads, tok, mine, away)
     copies = jnp.broadcast_to(partial[:, None], (NY, NX, 16, 1024)).reshape(16, 16, 1024)
     got = exchanged(copies, ("y", "x")).reshape(NY, NX, 16, 1024)
     target, spread, weight = rank_rows(
         jnp.full((1,), me, jnp.int32), routes.T, route_weights.T
     )
-    hidden, dense_gate, send, *sides = settle(c_ref, got, tok, vectors[0], vectors[1], spread)
+    hidden, dense_gate, send, *sides = settle(c_ref, got, vectors[0], vectors[1], spread)
     arrived = exchanged(send, EP).reshape(128, D)
     xs = [sides[0]] + [
         lax.ppermute(sides[s], "y", [(i, (i + s) % NY) for i in range(NY)]) for s in (1, 2, 3)
     ]
     sums = dense_products(c_ref, xs, mine, away)
-    parts = [sums[0]] + [
-        lax.ppermute(sums[s], "y", [(i, (i - s) % NY) for i in range(NY)]) for s in (1, 2, 3)
+    sums = [sums] + [
+        lax.ppermute(sums, "y", [(i, (i + s) % NY) for i in range(NY)]) for s in (1, 2, 3)
     ]
-    dense_sum = sum(p.astype(F32) for p in parts)
-    dense_hidden = (
-        jax.nn.silu(dense_sum[:, :256]) * dense_sum[:, 256:] * dense_gate[:, :1]
-    ).astype(BF16)
-    units = [dense_hidden] + [
-        lax.ppermute(dense_hidden, "y", [(i, (i + s) % NY) for i in range(NY)])
-        for s in (1, 2, 3)
-    ]
-    downs = dense_down(c_ref, units, mine, away)
+    downs = dense_down(c_ref, sums, mine, away)
     downs = [downs[0]] + [
         lax.ppermute(downs[s], "y", [(i, (i - s) % NY) for i in range(NY)]) for s in (1, 2, 3)
     ]
     gate_part = jnp.dot(arrived, w_exp_gate[0], preferred_element_type=F32)
     up_part = jnp.dot(arrived, w_exp_up[0], preferred_element_type=F32)
     expert_hidden = (jax.nn.silu(gate_part) * up_part * weight[:, :1]).astype(BF16)
-    returned = down_for_all(c_ref, expert_hidden, w_exp_down[0], hidden, downs)
+    returned = down_for_all(c_ref, expert_hidden, w_exp_down[0], hidden, dense_gate, downs)
     returned = exchanged(returned, EP)
-    dense_rows = returned[:, 64:].reshape(64, 8, 2, 64).transpose(0, 2, 1, 3).reshape(1024, 64)
-    returned = returned[:, :64]
-    source = returned.reshape(64, 4, 16, 128).transpose(1, 0, 2, 3).reshape(4, 1024, 128)
-    pick = picks(target).reshape(2, 4, 1024, 128)
-    halves = jnp.einsum("hgkm,gkn->hgmn", pick, source, preferred_element_type=F32)
-    routed = jnp.concatenate(
-        [halves[0, :, :, :64].reshape(512, 64), halves[1, :, :, 64:].reshape(512, 64)], axis=0
-    )
-    branch = packed((routed + dense_rows.astype(F32)).astype(BF16))
+    branch = combine(returned, picks(target))
     branches = [branch] + [
         lax.ppermute(branch, "x", [(i, (i + s) % NX) for i in range(NX)]) for s in (1, 2, 3)
     ]

time: 215 us -> 209 us (0.972)
  starting transfers between devices: 76 us -> 69.2 us
    ppermute x6 -> x3, starting transfers between devices: 10.4 us -> 5.6 us  [layer(): lax.ppermute(sums, 'y', [(i, (i + s) % NY) for i in range(NY)])]
    ppermute x4, waiting for transfers between devices: 8.56 us -> 12.6 us  [gathered_z(): up = lax.ppermute(up, 'z', [(i, (i + 1) % NZ) for i in range(NZ)])]
    unnamed x66 -> x70, local copies, waits for them, and re-layouts: 6.34 us -> 9.48 us
    ppermute x3, waiting for transfers between devices: 5.85 us -> 2.88 us  [gathered_z(): down = lax.ppermute(down, 'z', [(i, (i - 1) % NZ) for i in range(NZ)])]
    all_to_all x5, waiting for transfers between devices: 52.9 us -> 55.4 us  [exchanged(): return lax.all_to_all(x, axis, split_axis=0, concat_axis=0, tiled=True)]
    ppermute x6 -> x3, waiting for transfers between devices: 4.65 us -> 2.83 us  [layer(): lax.ppermute(sums, 'y', [(i, (i + s) % NY) for i in range(NY)])]
    pallas_call x2 -> x3, Pallas kernels: 4.43 us -> 5.09 us  [the longest x1 2.43 us: fold_y(): pl.pallas_call(fold_y_kernel, out_shape=jax.ShapeDtypeStruct((NZ, 16, 179...]
  transfers between devices with their start and end apart: 32 -> 29, of which waited for: 15 -> 14; matrix products, arithmetic and copies ran while one was open for 4% -> 4% of each run, Pallas kernels for 8% -> 8%
where the time goes in v3:
time: 209 us; the launch traced here: 207 us
  waiting for transfers between devices  81.8 us (39%)
  starting transfers between devices  69.2 us (33%)
  Pallas kernels  36.2 us (17%)
  local copies, waits for them, and re-layouts  15.7 us (8%)
  other arithmetic  2.24 us (1%)
    all_to_all x5, waiting for transfers between devices, exchanged(): return lax.all_to_all(x, axis, split_axis=0, concat_axis=0, tiled=True)  55.4 us
    all_to_all x5, starting transfers between devices, exchanged(): return lax.all_to_all(x, axis, split_axis=0, concat_axis=0, tiled=True)  33 us
    ppermute x4, waiting for transfers between devices, gathered_z(): up = lax.ppermute(up, 'z', [(i, (i + 1) % NZ) for i in range(NZ)])  12.6 us
    ppermute x3, starting transfers between devices, gathered_z(): down = lax.ppermute(down, 'z', [(i, (i - 1) % NZ) for i in range(NZ)])  10.4 us
    unnamed x70, local copies, waits for them, and re-layouts  9.48 us
    pallas_call x2, Pallas kernels, project(): pl.pallas_call(functools.partial(project_kernel, kept), grid=(NY,), out_s...  8.03 us
    ppermute x3, starting transfers between devices, layer(): lax.ppermute(downs[s], 'y', [(i, (i - s) % NY) for i in range(NY)])  5.81 us
    ppermute x3, starting transfers between devices, layer(): lax.ppermute(sums, 'y', [(i, (i + s) % NY) for i in range(NY)])  5.6 us
  transfers between devices with their start and end apart: 29, of which 14 were waited for; matrix products, arithmetic and copies ran while one was open for 4% of the time, Pallas kernels for 8%

profile of v3, /device:TPU:8, one launch (start us, length us, event | category | flops | bytes accessed | tf_op | source)
XLA Modules:
  0.0 207.2 jit_solution(15900901131958082638)
XLA Ops:
  1.3 3.5 %project_away.1 = bf16[4,128,1664]{2,1,0:T(8,128)(2,1)} custom-call(s32[4]{0:T(128)} %pad_add_fusion.c_ref, bf16[64,1024]{1,0:T(8,128)(2,1)} %bitcast.57, bf16[1,64]{1,0:T(2,128)(2,1)} %bitcast.68, bf16[64,256]{1,0:T(8,128)(2,1)} %q_ref.3, bf16[64,256]{1,0:T(8,128)(2,1)} %k_ref.3, bf16[64,512]{1,0:T(8,128)(2,1)} %v_ref.3, bf16[64,512]{1,0:T(8,128)(2,1)} %o_ref.3, ...), custom_call_target="tpu_custom_call" | custom-call | flops 436207616 | bytes 3145728 | tf_op jit(solution)/shard_map/project_away/pallas_call | solution.py:326
  7.9 4.0 %collective-permute-start.5 = (bf16[656,128]{1,0:T(8,128)(2,1)S(1)}, bf16[656,128]{1,0:T(8,128)(2,1)S(1)}, u32[]{:S(2)}, u32[]{:S(2)}) collective-permute-start(bf16[656,128]{1,0:T(8,128)(2,1)S(1)} %concatenate.14.refs_0_), channel_id=1, source_target_pairs={{0,224},{32,0},{64,32},{96,64},{128,96},{160,128},{192,160},{224,1... | collective-permute-start | bytes 503816 | tf_op jit(solution)/shard_map/ppermute | solution.py:43
  11.9 4.9 %collective-permute-done.1.refs_1_ = bf16[656,128]{1,0:T(8,128)(2,1)S(1)} collective-permute-done((bf16[656,128]{1,0:T(8,128)(2,1)S(1)}, bf16[656,128]{1,0:T(8,128)(2,1)S(1)}, u32[]{:S(2)}, u32[]{:S(2)}) %collective-permute-start.1) | collective-permute-done | bytes 167968 | tf_op jit(solution)/shard_map/ppermute | solution.py:40
  16.8 3.2 %collective-permute-start.6 = (bf16[656,128]{1,0:T(8,128)(2,1)S(1)}, bf16[656,128]{1,0:T(8,128)(2,1)S(1)}, u32[]{:S(2)}, u32[]{:S(2)}) collective-permute-start(bf16[656,128]{1,0:T(8,128)(2,1)S(1)} %collective-permute-done.5.refs_7_), channel_id=1, source_target_pairs={{0,224},{32,0},{64,32},{96,64},{128,96},{160,128},{192,160},{224,1... | collective-permute-start | bytes 503816 | tf_op jit(solution)/shard_map/ppermute | solution.py:43
  20.0 4.1 %collective-permute-done.2.refs_2_ = bf16[656,128]{1,0:T(8,128)(2,1)S(1)} collective-permute-done((bf16[656,128]{1,0:T(8,128)(2,1)S(1)}, bf16[656,128]{1,0:T(8,128)(2,1)S(1)}, u32[]{:S(2)}, u32[]{:S(2)}) %collective-permute-start.2) | collective-permute-done | bytes 167968 | tf_op jit(solution)/shard_map/ppermute | solution.py:40
  24.1 4.5 %project_kept.1 = (bf16[4,128,1664]{2,1,0:T(8,128)(2,1)}, bf16[128,128]{1,0:T(8,128)(2,1)}) custom-call(s32[4]{0:T(128)} %pad_add_fusion.c_ref, bf16[64,1024]{1,0:T(8,128)(2,1)} %bitcast.58, bf16[1,64]{1,0:T(2,128)(2,1)} %bitcast.69, bf16[64,256]{1,0:T(8,128)(2,1)} %q_ref.3, bf16[64,256]{1,0:T(8,128)(2,1)} %k_ref.3, bf16[64,512]{1,0:T(8,128)(2,1)} %v_ref.3, ...), custom_call_target="tpu_custom_call" | custom-call | flops 436207616 | bytes 3145728 | tf_op jit(solution)/shard_map/project_kept/pallas_call | solution.py:326
  28.6 4.9 %all-to-all-start = ((bf16[4,128,1664]{2,1,0:T(8,128)(2,1)}), bf16[4,128,1664]{2,1,0:T(8,128)(2,1)}, u32[]{:S(2)}, u32[]{:S(2)}) async-start(bf16[4,128,1664]{2,1,0:T(8,128)(2,1)} %get-tuple-element.25), calls=%async_computation | async-start | bytes 3407872 | tf_op jit(solution)/shard_map/all_to_all | solution.py:24
  33.5 3.2 %collective-permute-start.7 = (bf16[656,128]{1,0:T(8,128)(2,1)S(1)}, bf16[656,128]{1,0:T(8,128)(2,1)S(1)}, u32[]{:S(2)}, u32[]{:S(2)}) collective-permute-start(bf16[656,128]{1,0:T(8,128)(2,1)S(1)} %collective-permute-done.6.refs_6_), channel_id=1, source_target_pairs={{0,224},{32,0},{64,32},{96,64},{128,96},{160,128},{192,160},{224,1... | collective-permute-start | bytes 503816 | tf_op jit(solution)/shard_map/ppermute | solution.py:43
  36.7 2.9 %collective-permute-done.7.refs_5_ = bf16[656,128]{1,0:T(8,128)(2,1)S(1)} collective-permute-done((bf16[656,128]{1,0:T(8,128)(2,1)S(1)}, bf16[656,128]{1,0:T(8,128)(2,1)S(1)}, u32[]{:S(2)}, u32[]{:S(2)}) %collective-permute-start.7) | collective-permute-done | bytes 167968 | tf_op jit(solution)/shard_map/ppermute | solution.py:43
  39.6 3.7 %collective-permute-done.4.refs_4_ = bf16[656,128]{1,0:T(8,128)(2,1)S(1)} collective-permute-done((bf16[656,128]{1,0:T(8,128)(2,1)S(1)}, bf16[656,128]{1,0:T(8,128)(2,1)S(1)}, u32[]{:S(2)}, u32[]{:S(2)}) %collective-permute-start.4) | collective-permute-done | bytes 167968 | tf_op jit(solution)/shard_map/ppermute | solution.py:40
  44.0 2.5 %stacked.1.mine_ref = bf16[8,656,128]{2,1,0:T(8,128)(2,1)} custom-call(bf16[656,128]{1,0:T(8,128)(2,1)} %copy-done.13, bf16[656,128]{1,0:T(8,128)(2,1)} %copy-done.14, bf16[656,128]{1,0:T(8,128)(2,1)} %copy-done.16, bf16[656,128]{1,0:T(8,128)(2,1)} %copy-done.18, bf16[656,128]{1,0:T(8,128)(2,1)} %copy-done.20, bf16[656,128]{1,0:T(8,128)(2,1)} %copy-done.19, ...), custom_call_target="tpu_custom_call" | custom-call | flops 1048576 | bytes 2097152 | tf_op jit(solution)/shard_map/stacked/pallas_call | solution.py:45
  46.7 7.1 %all-to-all-done.in_ref = bf16[4,128,1664]{2,1,0:T(8,128)(2,1)} async-done(((bf16[4,128,1664]{2,1,0:T(8,128)(2,1)}), bf16[4,128,1664]{2,1,0:T(8,128)(2,1)}, u32[]{:S(2)}, u32[]{:S(2)}) %all-to-all-start) | async-done | bytes 1703968 | tf_op jit(solution)/shard_map/all_to_all | solution.py:24
  56.2 5.4 %all-to-all-start.1 = ((bf16[8,16,1792]{2,1,0:T(8,128)(2,1)}), bf16[8,16,1792]{2,1,0:T(8,128)(2,1)}, u32[]{:S(2)}, u32[]{:S(2)}) async-start(bf16[8,16,1792]{2,1,0:T(8,128)(2,1)} %fold_y.1), calls=%async_computation.1 | async-start | bytes 917504 | tf_op jit(solution)/shard_map/all_to_all | solution.py:24
  64.4 11.2 %all-to-all-done.1.in_ref = bf16[8,16,1792]{2,1,0:T(8,128)(2,1)} async-done(((bf16[8,16,1792]{2,1,0:T(8,128)(2,1)}), bf16[8,16,1792]{2,1,0:T(8,128)(2,1)}, u32[]{:S(2)}, u32[]{:S(2)}) %all-to-all-start.1) | async-done | bytes 458784 | tf_op jit(solution)/shard_map/all_to_all | solution.py:24
  75.6 5.5 %recur.1 = (bf16[16,512]{1,0:T(8,128)(2,1)}, bf16[16,1024]{1,0:T(8,128)(2,1)}, f32[16,4,64,128]{3,2,1,0:T(8,128)}, f32[16,4,64]{2,1,0:T(4,128)}, f32[16,4]{1,0:T(8,128)}) custom-call(bf16[8,16,1792]{2,1,0:T(8,128)(2,1)} %all-to-all-done.1.in_ref, f32[1,4]{1,0:T(1,128)} %bitcast.70, f32[1,4]{1,0:T(1,128)} %bitcast.71, ...), custom_call_target="tpu_custom_call" | custom-call | flops 8388608 | bytes 5242880 | tf_op jit(solution)/shard_map/recur/pallas_call | solution.py:440
  92.2 7.3 %all-to-all-start.2 = ((bf16[16,16,1024]{2,1,0:T(8,128)(2,1)}), bf16[16,16,1024]{2,1,0:T(8,128)(2,1)}, u32[]{:S(2)}, u32[]{:S(2)}) async-start(bf16[16,16,1024]{2,1,0:T(8,128)(2,1)} %bitcast.56), calls=%async_computation.2 | async-start | bytes 1048576 | tf_op jit(solution)/shard_map/all_to_all | solution.py:24
  101.0 6.7 %all-to-all-done.2 = bf16[16,16,1024]{2,1,0:T(8,128)(2,1)} async-done(((bf16[16,16,1024]{2,1,0:T(8,128)(2,1)}), bf16[16,16,1024]{2,1,0:T(8,128)(2,1)}, u32[]{:S(2)}, u32[]{:S(2)}) %all-to-all-start.2) | async-done | bytes 524320 | tf_op jit(solution)/shard_map/all_to_all | solution.py:24
  107.7 3.4 %settle.1 = (bf16[16,4096]{1,0:T(8,128)(2,1)}, f32[16,128]{1,0:T(8,128)}, bf16[64,2,4096]{2,1,0:T(2,128)(2,1)}, bf16[16,1024]{1,0:T(8,128)(2,1)}, bf16[16,1024]{...) custom-call(s32[4]{0:T(128)} %pad_add_fusion.c_ref, bf16[4,4,16,1024]{3,2,1,0:T(8,128)(2,1)} %bitcast.17.got_ref, ...), custom_call_target="tpu_custom_call" | custom-call | flops 134217728 | bytes 3145728 | tf_op jit(solution)/shard_map/settle/pallas_call | solution.py:145
  111.1 7.3 %all-to-all-start.3 = ((bf16[64,2,4096]{2,1,0:T(2,128)(2,1)}), bf16[64,2,4096]{2,1,0:T(2,128)(2,1)}, u32[]{:S(2)}, u32[]{:S(2)}) async-start(bf16[64,2,4096]{2,1,0:T(2,128)(2,1)} %get-tuple-element.30), calls=%async_computation.3 | async-start | bytes 2097152 | tf_op jit(solution)/shard_map/all_to_all | solution.py:24
  123.1 3.4 %collective-permute-done.13.x2 = bf16[16,1024]{1,0:T(8,128)(2,1)S(1)} collective-permute-done((bf16[16,1024]{1,0:T(8,128)(2,1)}, bf16[16,1024]{1,0:T(8,128)(2,1)S(1)}, u32[]{:S(2)}, u32[]{:S(2)}) %collective-permute-start.13) | collective-permute-done | bytes 32800 | tf_op jit(solution)/shard_map/ppermute | solution.py:681
  142.6 2.6 %collective-permute-start.20 = (bf16[16,1024]{1,0:T(8,128)(2,1)S(1)}, bf16[16,1024]{1,0:T(8,128)(2,1)S(1)}, u32[]{:S(2)}, u32[]{:S(2)}) collective-permute-start(bf16[16,1024]{1,0:T(8,128)(2,1)S(1)} %get-tuple-element.41), channel_id=1, source_target_pairs={{0,8},{8,16},{16,24},{24,0},{1,9},{9,17},{17,25},{25,1},{2,10},{10... | collective-permute-start | bytes 98312 | tf_op jit(solution)/shard_map/ppermute | solution.py:689
  154.9 8.1 %all-to-all-start.4 = ((bf16[64,72,128]{2,1,0:T(8,128)(2,1)}), bf16[64,72,128]{2,1,0:T(8,128)(2,1)S(1)}, u32[]{:S(2)}, u32[]{:S(2)}) async-start(bf16[64,72,128]{2,1,0:T(8,128)(2,1)} %copy-done.4), calls=%async_computation.4 | async-start | bytes 2359296 | tf_op jit(solution)/shard_map/all_to_all | solution.py:24
  166.0 28.6 %all-to-all-done.4.got_ref = bf16[64,72,128]{2,1,0:T(8,128)(2,1)S(1)} async-done(((bf16[64,72,128]{2,1,0:T(8,128)(2,1)}), bf16[64,72,128]{2,1,0:T(8,128)(2,1)S(1)}, u32[]{:S(2)}, u32[]{:S(2)}) %all-to-all-start.4) | async-done | bytes 1179680 | tf_op jit(solution)/shard_map/all_to_all | solution.py:24
  201.1 3.9 %collective-permute-done.21.b1 = bf16[512,128]{1,0:T(8,128)(2,1)S(1)} collective-permute-done((bf16[512,128]{1,0:T(8,128)(2,1)S(1)}, bf16[512,128]{1,0:T(8,128)(2,1)S(1)}, u32[]{:S(2)}, u32[]{:S(2)}) %collective-permute-start.21) | collective-permute-done | bytes 131104 | tf_op jit(solution)/shard_map/ppermute | solution.py:698
  (156 shorter events, 64.1 us)
Async XLA Ops:
  4.9 19.2 %collective-permute-start = (bf16[4,128,1664]{2,1,0:T(8,128)(2,1)}, bf16[4,128,1664]{2,1,0:T(8,128)(2,1)}, u32[]{:S(2)}, u32[]{:S(2)}) collective-permute-start(bf16[4,128,1664]{2,1,0:T(8,128)(2,1)} %project_away.1), channel_id=1, source_target_pairs={{0,4},{4,0},{1,5},{5,1},{2,6},{6,2},{3,7},{7,3},{8,12},{12,8},{9,1... | collective-permute-start | bytes 5111816 | tf_op jit(solution)/shard_map/ppermute | solution.py:28
  5.9 10.9 %collective-permute-start.1 = (bf16[656,128]{1,0:T(8,128)(2,1)S(1)}, bf16[656,128]{1,0:T(8,128)(2,1)S(1)}, u32[]{:S(2)}, u32[]{:S(2)}) collective-permute-start(bf16[656,128]{1,0:T(8,128)(2,1)S(1)} %concatenate.14.refs_0_), channel_id=1, source_target_pairs={{0,32},{32,64},{64,96},{96,128},{128,160},{160,192},{192,224},{224... | collective-permute-start | bytes 503816 | tf_op jit(solution)/shard_map/ppermute | solution.py:40
  7.9 8.9 %collective-permute-start.5 = (bf16[656,128]{1,0:T(8,128)(2,1)S(1)}, bf16[656,128]{1,0:T(8,128)(2,1)S(1)}, u32[]{:S(2)}, u32[]{:S(2)}) collective-permute-start(bf16[656,128]{1,0:T(8,128)(2,1)S(1)} %concatenate.14.refs_0_), channel_id=1, source_target_pairs={{0,224},{32,0},{64,32},{96,64},{128,96},{160,128},{192,160},{224,1... | collective-permute-start | bytes 503816 | tf_op jit(solution)/shard_map/ppermute | solution.py:43
  16.8 7.3 %collective-permute-start.2 = (bf16[656,128]{1,0:T(8,128)(2,1)S(1)}, bf16[656,128]{1,0:T(8,128)(2,1)S(1)}, u32[]{:S(2)}, u32[]{:S(2)}) collective-permute-start(bf16[656,128]{1,0:T(8,128)(2,1)S(1)} %collective-permute-done.1.refs_1_), channel_id=1, source_target_pairs={{0,32},{32,64},{64,96},{96,128},{128,160},{160,192},{192,224},{224... | collective-permute-start | bytes 503816 | tf_op jit(solution)/shard_map/ppermute | solution.py:40
  16.8 16.8 %collective-permute-start.6 = (bf16[656,128]{1,0:T(8,128)(2,1)S(1)}, bf16[656,128]{1,0:T(8,128)(2,1)S(1)}, u32[]{:S(2)}, u32[]{:S(2)}) collective-permute-start(bf16[656,128]{1,0:T(8,128)(2,1)S(1)} %collective-permute-done.5.refs_7_), channel_id=1, source_target_pairs={{0,224},{32,0},{64,32},{96,64},{128,96},{160,128},{192,160},{224,1... | collective-permute-start | bytes 503816 | tf_op jit(solution)/shard_map/ppermute | solution.py:43
  24.1 12.6 %collective-permute-start.3 = (bf16[656,128]{1,0:T(8,128)(2,1)S(1)}, bf16[656,128]{1,0:T(8,128)(2,1)S(1)}, u32[]{:S(2)}, u32[]{:S(2)}) collective-permute-start(bf16[656,128]{1,0:T(8,128)(2,1)S(1)} %collective-permute-done.2.refs_2_), channel_id=1, source_target_pairs={{0,32},{32,64},{64,96},{96,128},{128,160},{160,192},{192,224},{224... | collective-permute-start | bytes 503816 | tf_op jit(solution)/shard_map/ppermute | solution.py:40
  28.6 25.1 %all-to-all-start = ((bf16[4,128,1664]{2,1,0:T(8,128)(2,1)}), bf16[4,128,1664]{2,1,0:T(8,128)(2,1)}, u32[]{:S(2)}, u32[]{:S(2)}) async-start(bf16[4,128,1664]{2,1,0:T(8,128)(2,1)} %get-tuple-element.25), calls=%async_computation | async-start | bytes 3407872 | tf_op jit(solution)/shard_map/all_to_all | solution.py:24
  33.5 6.1 %collective-permute-start.7 = (bf16[656,128]{1,0:T(8,128)(2,1)S(1)}, bf16[656,128]{1,0:T(8,128)(2,1)S(1)}, u32[]{:S(2)}, u32[]{:S(2)}) collective-permute-start(bf16[656,128]{1,0:T(8,128)(2,1)S(1)} %collective-permute-done.6.refs_6_), channel_id=1, source_target_pairs={{0,224},{32,0},{64,32},{96,64},{128,96},{160,128},{192,160},{224,1... | collective-permute-start | bytes 503816 | tf_op jit(solution)/shard_map/ppermute | solution.py:43
  36.7 6.6 %collective-permute-start.4 = (bf16[656,128]{1,0:T(8,128)(2,1)S(1)}, bf16[656,128]{1,0:T(8,128)(2,1)S(1)}, u32[]{:S(2)}, u32[]{:S(2)}) collective-permute-start(bf16[656,128]{1,0:T(8,128)(2,1)S(1)} %collective-permute-done.3.refs_3_), channel_id=1, source_target_pairs={{0,32},{32,64},{64,96},{96,128},{128,160},{160,192},{192,224},{224... | collective-permute-start | bytes 503816 | tf_op jit(solution)/shard_map/ppermute | solution.py:40
  46.5 16.4 %collective-permute-start.8 = (bf16[8,656,128]{2,1,0:T(8,128)(2,1)}, bf16[8,656,128]{2,1,0:T(8,128)(2,1)}, u32[]{:S(2)}, u32[]{:S(2)}) collective-permute-start(bf16[8,656,128]{2,1,0:T(8,128)(2,1)} %stacked.1.mine_ref), channel_id=1, source_target_pairs={{0,4},{4,0},{1,5},{5,1},{2,6},{6,2},{3,7},{7,3},{8,12},{12,8},{9,1... | collective-permute-start | bytes 4030472 | tf_op jit(solution)/shard_map/ppermute | solution.py:28
  56.2 19.4 %all-to-all-start.1 = ((bf16[8,16,1792]{2,1,0:T(8,128)(2,1)}), bf16[8,16,1792]{2,1,0:T(8,128)(2,1)}, u32[]{:S(2)}, u32[]{:S(2)}) async-start(bf16[8,16,1792]{2,1,0:T(8,128)(2,1)} %fold_y.1), calls=%async_computation.1 | async-start | bytes 917504 | tf_op jit(solution)/shard_map/all_to_all | solution.py:24
  81.9 6.8 %collective-permute-start.11 = (bf16[24,512]{1,0:T(8,128)(2,1)S(1)}, bf16[24,512]{1,0:T(8,128)(2,1)S(1)}, u32[]{:S(2)}, u32[]{:S(2)}) collective-permute-start(bf16[24,512]{1,0:T(8,128)(2,1)S(1)} %maximum_maximum_fusion.x0), channel_id=1, source_target_pairs={{0,24},{8,0},{16,8},{24,16},{1,25},{9,1},{17,9},{25,17},{2,26},{10... | collective-permute-start | bytes 73736 | tf_op jit(solution)/shard_map/ppermute | solution.py:667
  92.2 15.5 %all-to-all-start.2 = ((bf16[16,16,1024]{2,1,0:T(8,128)(2,1)}), bf16[16,16,1024]{2,1,0:T(8,128)(2,1)}, u32[]{:S(2)}, u32[]{:S(2)}) async-start(bf16[16,16,1024]{2,1,0:T(8,128)(2,1)} %bitcast.56), calls=%async_computation.2 | async-start | bytes 1048576 | tf_op jit(solution)/shard_map/all_to_all | solution.py:24
  111.1 36.0 %all-to-all-start.3 = ((bf16[64,2,4096]{2,1,0:T(2,128)(2,1)}), bf16[64,2,4096]{2,1,0:T(2,128)(2,1)}, u32[]{:S(2)}, u32[]{:S(2)}) async-start(bf16[64,2,4096]{2,1,0:T(2,128)(2,1)} %get-tuple-element.30), calls=%async_computation.3 | async-start | bytes 2097152 | tf_op jit(solution)/shard_map/all_to_all | solution.py:24
  119.9 6.6 %collective-permute-start.13 = (bf16[16,1024]{1,0:T(8,128)(2,1)}, bf16[16,1024]{1,0:T(8,128)(2,1)S(1)}, u32[]{:S(2)}, u32[]{:S(2)}) collective-permute-start(bf16[16,1024]{1,0:T(8,128)(2,1)} %get-tuple-element.36), channel_id=1, source_target_pairs={{0,16},{8,24},{16,0},{24,8},{1,17},{9,25},{17,1},{25,9},{2,18},{10... | collective-permute-start | bytes 98312 | tf_op jit(solution)/shard_map/ppermute | solution.py:681
  128.5 5.7 %collective-permute-start.15 = (bf16[64,512]{1,0:T(8,128)(2,1)S(1)}, bf16[64,512]{1,0:T(8,128)(2,1)S(1)}, u32[]{:S(2)}, u32[]{:S(2)}) collective-permute-start(bf16[64,512]{1,0:T(8,128)(2,1)S(1)} %dense_products.1.x0), channel_id=1, source_target_pairs={{0,8},{8,16},{16,24},{24,0},{1,9},{9,17},{17,25},{25,1},{2,10},{10... | collective-permute-start | bytes 196616 | tf_op jit(solution)/shard_map/ppermute | solution.py:685
  129.5 6.6 %collective-permute-start.16 = (bf16[64,512]{1,0:T(8,128)(2,1)S(1)}, bf16[64,512]{1,0:T(8,128)(2,1)S(1)}, u32[]{:S(2)}, u32[]{:S(2)}) collective-permute-start(bf16[64,512]{1,0:T(8,128)(2,1)S(1)} %dense_products.1.x0), channel_id=1, source_target_pairs={{0,16},{8,24},{16,0},{24,8},{1,17},{9,25},{17,1},{25,9},{2,18},{10... | collective-permute-start | bytes 196616 | tf_op jit(solution)/shard_map/ppermute | solution.py:685
  139.4 11.2 %collective-permute-start.18 = (bf16[16,1024]{1,0:T(8,128)(2,1)}, bf16[16,1024]{1,0:T(8,128)(2,1)S(1)}, u32[]{:S(2)}, u32[]{:S(2)}) collective-permute-start(bf16[16,1024]{1,0:T(8,128)(2,1)} %get-tuple-element.39), channel_id=1, source_target_pairs={{0,24},{8,0},{16,8},{24,16},{1,25},{9,1},{17,9},{25,17},{2,26},{10... | collective-permute-start | bytes 98312 | tf_op jit(solution)/shard_map/ppermute | solution.py:689
  141.3 9.4 %collective-permute-start.19 = (bf16[16,1024]{1,0:T(8,128)(2,1)S(1)}, bf16[16,1024]{1,0:T(8,128)(2,1)S(1)}, u32[]{:S(2)}, u32[]{:S(2)}) collective-permute-start(bf16[16,1024]{1,0:T(8,128)(2,1)S(1)} %get-tuple-element.40), channel_id=1, source_target_pairs={{0,16},{8,24},{16,0},{24,8},{1,17},{9,25},{17,1},{25,9},{2,18},{10... | collective-permute-start | bytes 98312 | tf_op jit(solution)/shard_map/ppermute | solution.py:689
  142.6 8.1 %collective-permute-start.20 = (bf16[16,1024]{1,0:T(8,128)(2,1)S(1)}, bf16[16,1024]{1,0:T(8,128)(2,1)S(1)}, u32[]{:S(2)}, u32[]{:S(2)}) collective-permute-start(bf16[16,1024]{1,0:T(8,128)(2,1)S(1)} %get-tuple-element.41), channel_id=1, source_target_pairs={{0,8},{8,16},{16,24},{24,0},{1,9},{9,17},{17,25},{25,1},{2,10},{10... | collective-permute-start | bytes 98312 | tf_op jit(solution)/shard_map/ppermute | solution.py:689
  154.9 39.7 %all-to-all-start.4 = ((bf16[64,72,128]{2,1,0:T(8,128)(2,1)}), bf16[64,72,128]{2,1,0:T(8,128)(2,1)S(1)}, u32[]{:S(2)}, u32[]{:S(2)}) async-start(bf16[64,72,128]{2,1,0:T(8,128)(2,1)} %copy-done.4), calls=%async_computation.4 | async-start | bytes 2359296 | tf_op jit(solution)/shard_map/all_to_all | solution.py:24
  196.9 8.1 %collective-permute-start.21 = (bf16[512,128]{1,0:T(8,128)(2,1)S(1)}, bf16[512,128]{1,0:T(8,128)(2,1)S(1)}, u32[]{:S(2)}, u32[]{:S(2)}) collective-permute-start(bf16[512,128]{1,0:T(8,128)(2,1)S(1)} %combine.1.b0), channel_id=1, source_target_pairs={{0,1},{1,2},{2,3},{3,0},{4,5},{5,6},{6,7},{7,4},{8,9},{9,10},{10,1... | collective-permute-start | bytes 393224 | tf_op jit(solution)/shard_map/ppermute | solution.py:698
  197.6 7.4 %collective-permute-start.22 = (bf16[512,128]{1,0:T(8,128)(2,1)S(1)}, bf16[512,128]{1,0:T(8,128)(2,1)S(1)}, u32[]{:S(2)}, u32[]{:S(2)}) collective-permute-start(bf16[512,128]{1,0:T(8,128)(2,1)S(1)} %combine.1.b0), channel_id=1, source_target_pairs={{0,2},{1,3},{2,0},{3,1},{4,6},{5,7},{6,4},{7,5},{8,10},{9,11},{10,... | collective-permute-start | bytes 393224 | tf_op jit(solution)/shard_map/ppermute | solution.py:698
  199.0 6.7 %collective-permute-start.23 = (bf16[512,128]{1,0:T(8,128)(2,1)S(1)}, bf16[512,128]{1,0:T(8,128)(2,1)S(1)}, u32[]{:S(2)}, u32[]{:S(2)}) collective-permute-start(bf16[512,128]{1,0:T(8,128)(2,1)S(1)} %combine.1.b0), channel_id=1, source_target_pairs={{0,3},{1,0},{2,1},{3,2},{4,7},{5,4},{6,5},{7,6},{8,11},{9,8},{10,9... | collective-permute-start | bytes 393224 | tf_op jit(solution)/shard_map/ppermute | solution.py:698
  (37 other events, 452.9 us)

commit v4 on v3

--- a/solution.py
+++ b/solution.py
@@ -85,7 +85,8 @@
         for s in range(NY):
             to = lax.rem(c_ref[1] + (NY - s), NY)
             rows = tile[s * 16 : (s + 1) * 16] + jnp.where(to == c_ref[3], tok, 0.0)
-            out_ref[to, :, turned_z(c_ref, z)] = rows.astype(BF16)
+            for x in range(NX):
+                out_ref[to * NX + x, :, turned_z(c_ref, z)] = rows.astype(BF16)
 
 
 VMEM = pl.BlockSpec(memory_space=pltpu.VMEM)
@@ -95,7 +96,7 @@
 def mix(c, heads, tok, mine, away):
     return pl.pallas_call(
         mix_kernel,
-        out_shape=jax.ShapeDtypeStruct((NY, 16, 1024), BF16),
+        out_shape=jax.ShapeDtypeStruct((NY * NX, 16, 1024), BF16),
         in_specs=[SMEM] + [VMEM] * 7,
         out_specs=VMEM,
         compiler_params=pltpu.CompilerParams(vmem_limit_bytes=LIMIT),
@@ -364,7 +365,7 @@
 
 
 def recur_kernel(
-    in_ref, ib_ref, fb_ref, hg_ref, sm_ref, sn_ref, mx_ref,
+    in_ref, ib_ref, fb_ref, hg_ref, sm_ref, sn_ref, mx_ref, ex_ref,
     heads_ref, tok_ref, nm_ref, nn_ref, nx_ref,
     kt_ref, qt_ref, car_ref, flo_ref, val_ref, out_ref, num_ref,
 ):
@@ -425,23 +426,24 @@
 
     @pl.when(g == 3)
     def _():
+        heads_ref[16:, :] = ex_ref[...]
         for h in range(4):
             cols = slice(h * 128, (h + 1) * 128)
             read = num_ref[h] / flo_ref[h]
             mean = jnp.mean(read * read, axis=1, keepdims=True)
             gate = 1.0 / (1.0 + jnp.exp(-out_ref[:, cols]))
             scaled = read * lax.rsqrt(mean + EPSILON) * hg_ref[:, cols].astype(F32)
-            heads_ref[:, cols] = (scaled * gate).astype(BF16)
-
-
-def recur(x, igate_bias, fgate_bias, head_gain, state_matrix, state_norm, state_max):
+            heads_ref[:16, cols] = (scaled * gate).astype(BF16)
+
+
+def recur(x, igate_bias, fgate_bias, head_gain, state_matrix, state_norm, state_max, extra):
     whole = lambda *shape: pl.BlockSpec(shape, lambda g: (0,) * len(shape))
     block = pl.BlockSpec((4, 4, 64, 128), lambda g: (g, 0, 0, 0))
     return pl.pallas_call(
         recur_kernel,
         grid=(4,),
         out_shape=(
-            jax.ShapeDtypeStruct((16, 512), BF16),
+            jax.ShapeDtypeStruct((24, 512), BF16),
             jax.ShapeDtypeStruct((16, 1024), BF16),
             jax.ShapeDtypeStruct((16, 4, 64, 128), F32),
             jax.ShapeDtypeStruct((16, 4, 64), F32),
@@ -449,9 +451,9 @@
         ),
         in_specs=[
             whole(NZ, 16, 1792), whole(1, 4), whole(1, 4), whole(1, 512),
-            block, whole(16, 4, 64), whole(16, 4),
+            block, whole(16, 4, 64), whole(16, 4), whole(8, 512),
         ],
-        out_specs=(whole(16, 512), whole(16, 1024), block, whole(16, 4, 64), whole(16, 4)),
+        out_specs=(whole(24, 512), whole(16, 1024), block, whole(16, 4, 64), whole(16, 4)),
         scratch_shapes=[
             pltpu.VMEM((4, 256, 4), F32),
             pltpu.VMEM((4, 256, 4), F32),
@@ -465,7 +467,7 @@
             flops=8 << 20, bytes_accessed=5 << 20, transcendentals=1 << 14
         ),
         name="recur",
-    )(x, igate_bias[None], fgate_bias[None], head_gain[None], state_matrix, state_norm, state_max)
+    )(x, igate_bias[None], fgate_bias[None], head_gain[None], state_matrix, state_norm, state_max, extra)
 
 
 def rank_kernel(me_ref, routes_ref, weights_ref, target_ref, spread_ref, weight_ref):
@@ -655,14 +657,13 @@
     folded = exchanged(folded, "y")
     folded = fold_y(folded, tile)
     folded = exchanged(folded, "z")
-    heads_out, tok, new_matrix, new_norm, new_max = recur(
-        folded, igate_bias, fgate_bias, head_gain, state_matrix, state_norm, state_max
-    )
     mine, away = gathered_z(piece)
     extra = jnp.stack([mine[:, 256:258, :64], away[:, 256:258, :64]])
     extra = jnp.where(c == 0, extra, extra[::-1])[:, (z - jnp.arange(NZ)) % NZ]
-    extra = extra.transpose(2, 1, 0, 3).reshape(4, 512)
-    heads = jnp.concatenate([heads_out, extra, jnp.zeros((4, 512), BF16)], axis=0)
+    extra = jnp.pad(extra.transpose(2, 1, 0, 3).reshape(4, 512), ((0, 4), (0, 0)))
+    heads, tok, new_matrix, new_norm, new_max = recur(
+        folded, igate_bias, fgate_bias, head_gain, state_matrix, state_norm, state_max, extra
+    )
     heads = [heads] + [
         lax.ppermute(heads, "y", [(i, (i + s) % NY) for i in range(NY)]) for s in (1, 2, 3)
     ]
@@ -670,8 +671,7 @@
     vectors = vectors.reshape(NY, 2, NZ, 128).transpose(1, 2, 0, 3).reshape(2, 1, D)
     vectors = vectors.astype(F32)
     partial = mix(c_ref, heads, tok, mine, away)
-    copies = jnp.broadcast_to(partial[:, None], (NY, NX, 16, 1024)).reshape(16, 16, 1024)
-    got = exchanged(copies, ("y", "x")).reshape(NY, NX, 16, 1024)
+    got = exchanged(partial, ("y", "x")).reshape(NY, NX, 16, 1024)
     target, spread, weight = rank_rows(
         jnp.full((1,), me, jnp.int32), routes.T, route_weights.T
     )

time: 209 us -> 208 us (level)
    all_to_all x5, waiting for transfers between devices: 55.4 us -> 52.8 us  [exchanged(): return lax.all_to_all(x, axis, split_axis=0, concat_axis=0, tiled=True)]
    ppermute x3, waiting for transfers between devices: 0.01 us -> 2.18 us  [layer(): lax.ppermute(heads, 'y', [(i, (i + s) % NY) for i in range(NY)])]
    unnamed x70 -> x74, local copies, waits for them, and re-layouts: 9.48 us -> 11 us
  transfers between devices with their start and end apart: 29 -> 29, of which waited for: 14 -> 15; matrix products, arithmetic and copies ran while one was open for 4% -> 5% of each run, Pallas kernels for 8% -> 9%
where the time goes in v4:
time: 208 us; the launch traced here: 207 us
  waiting for transfers between devices  81.4 us (39%)
  starting transfers between devices  68.9 us (33%)
  Pallas kernels  36.2 us (17%)
  local copies, waits for them, and re-layouts  17.4 us (8%)
    all_to_all x5, waiting for transfers between devices, exchanged(): return lax.all_to_all(x, axis, split_axis=0, concat_axis=0, tiled=True)  52.8 us
    all_to_all x5, starting transfers between devices, exchanged(): return lax.all_to_all(x, axis, split_axis=0, concat_axis=0, tiled=True)  32.6 us
    ppermute x4, waiting for transfers between devices, gathered_z(): up = lax.ppermute(up, 'z', [(i, (i + 1) % NZ) for i in range(NZ)])  12.6 us
    unnamed x74, local copies, waits for them, and re-layouts  11 us
    ppermute x3, starting transfers between devices, gathered_z(): down = lax.ppermute(down, 'z', [(i, (i - 1) % NZ) for i in range(NZ)])  10.4 us
    pallas_call x2, Pallas kernels, project(): pl.pallas_call(functools.partial(project_kernel, kept), grid=(NY,), out_s...  8.02 us
    ppermute x3, starting transfers between devices, layer(): lax.ppermute(downs[s], 'y', [(i, (i - s) % NY) for i in range(NY)])  5.8 us
    ppermute x3, starting transfers between devices, layer(): lax.ppermute(sums, 'y', [(i, (i + s) % NY) for i in range(NY)])  5.6 us
  transfers between devices with their start and end apart: 29, of which 15 were waited for; matrix products, arithmetic and copies ran while one was open for 5% of the time, Pallas kernels for 9%

profile of v4, /device:TPU:8, one launch (start us, length us, event | category | flops | bytes accessed | tf_op | source)
XLA Modules:
  0.0 206.8 jit_solution(6573563120821925289)
XLA Ops:
  1.3 3.5 %project_away.1 = bf16[4,128,1664]{2,1,0:T(8,128)(2,1)} custom-call(s32[4]{0:T(128)} %pad_add_fusion.c_ref, bf16[64,1024]{1,0:T(8,128)(2,1)} %bitcast.57, bf16[1,64]{1,0:T(2,128)(2,1)} %bitcast.68, bf16[64,256]{1,0:T(8,128)(2,1)} %q_ref.3, bf16[64,256]{1,0:T(8,128)(2,1)} %k_ref.3, bf16[64,512]{1,0:T(8,128)(2,1)} %v_ref.3, bf16[64,512]{1,0:T(8,128)(2,1)} %o_ref.3, ...), custom_call_target="tpu_custom_call" | custom-call | flops 436207616 | bytes 3145728 | tf_op jit(solution)/shard_map/project_away/pallas_call | solution.py:327
  7.8 4.0 %collective-permute-start.5 = (bf16[656,128]{1,0:T(8,128)(2,1)S(1)}, bf16[656,128]{1,0:T(8,128)(2,1)S(1)}, u32[]{:S(2)}, u32[]{:S(2)}) collective-permute-start(bf16[656,128]{1,0:T(8,128)(2,1)S(1)} %concatenate.11.refs_0_), channel_id=1, source_target_pairs={{0,224},{32,0},{64,32},{96,64},{128,96},{160,128},{192,160},{224,1... | collective-permute-start | bytes 503816 | tf_op jit(solution)/shard_map/ppermute | solution.py:43
  11.9 4.9 %collective-permute-done.1.refs_1_ = bf16[656,128]{1,0:T(8,128)(2,1)S(1)} collective-permute-done((bf16[656,128]{1,0:T(8,128)(2,1)S(1)}, bf16[656,128]{1,0:T(8,128)(2,1)S(1)}, u32[]{:S(2)}, u32[]{:S(2)}) %collective-permute-start.1) | collective-permute-done | bytes 167968 | tf_op jit(solution)/shard_map/ppermute | solution.py:40
  16.8 3.2 %collective-permute-start.6 = (bf16[656,128]{1,0:T(8,128)(2,1)S(1)}, bf16[656,128]{1,0:T(8,128)(2,1)S(1)}, u32[]{:S(2)}, u32[]{:S(2)}) collective-permute-start(bf16[656,128]{1,0:T(8,128)(2,1)S(1)} %collective-permute-done.5.refs_7_), channel_id=1, source_target_pairs={{0,224},{32,0},{64,32},{96,64},{128,96},{160,128},{192,160},{224,1... | collective-permute-start | bytes 503816 | tf_op jit(solution)/shard_map/ppermute | solution.py:43
  20.0 4.1 %collective-permute-done.2.refs_2_ = bf16[656,128]{1,0:T(8,128)(2,1)S(1)} collective-permute-done((bf16[656,128]{1,0:T(8,128)(2,1)S(1)}, bf16[656,128]{1,0:T(8,128)(2,1)S(1)}, u32[]{:S(2)}, u32[]{:S(2)}) %collective-permute-start.2) | collective-permute-done | bytes 167968 | tf_op jit(solution)/shard_map/ppermute | solution.py:40
  24.1 4.5 %project_kept.1 = (bf16[4,128,1664]{2,1,0:T(8,128)(2,1)}, bf16[128,128]{1,0:T(8,128)(2,1)}) custom-call(s32[4]{0:T(128)} %pad_add_fusion.c_ref, bf16[64,1024]{1,0:T(8,128)(2,1)} %bitcast.58, bf16[1,64]{1,0:T(2,128)(2,1)} %bitcast.69, bf16[64,256]{1,0:T(8,128)(2,1)} %q_ref.3, bf16[64,256]{1,0:T(8,128)(2,1)} %k_ref.3, bf16[64,512]{1,0:T(8,128)(2,1)} %v_ref.3, ...), custom_call_target="tpu_custom_call" | custom-call | flops 436207616 | bytes 3145728 | tf_op jit(solution)/shard_map/project_kept/pallas_call | solution.py:327
  28.6 4.9 %all-to-all-start = ((bf16[4,128,1664]{2,1,0:T(8,128)(2,1)}), bf16[4,128,1664]{2,1,0:T(8,128)(2,1)}, u32[]{:S(2)}, u32[]{:S(2)}) async-start(bf16[4,128,1664]{2,1,0:T(8,128)(2,1)} %get-tuple-element.25), calls=%async_computation | async-start | bytes 3407872 | tf_op jit(solution)/shard_map/all_to_all | solution.py:24
  33.5 3.2 %collective-permute-start.7 = (bf16[656,128]{1,0:T(8,128)(2,1)S(1)}, bf16[656,128]{1,0:T(8,128)(2,1)S(1)}, u32[]{:S(2)}, u32[]{:S(2)}) collective-permute-start(bf16[656,128]{1,0:T(8,128)(2,1)S(1)} %collective-permute-done.6.refs_6_), channel_id=1, source_target_pairs={{0,224},{32,0},{64,32},{96,64},{128,96},{160,128},{192,160},{224,1... | collective-permute-start | bytes 503816 | tf_op jit(solution)/shard_map/ppermute | solution.py:43
  36.7 2.9 %collective-permute-done.7.refs_5_ = bf16[656,128]{1,0:T(8,128)(2,1)S(1)} collective-permute-done((bf16[656,128]{1,0:T(8,128)(2,1)S(1)}, bf16[656,128]{1,0:T(8,128)(2,1)S(1)}, u32[]{:S(2)}, u32[]{:S(2)}) %collective-permute-start.7) | collective-permute-done | bytes 167968 | tf_op jit(solution)/shard_map/ppermute | solution.py:43
  39.6 3.7 %collective-permute-done.4.refs_4_ = bf16[656,128]{1,0:T(8,128)(2,1)S(1)} collective-permute-done((bf16[656,128]{1,0:T(8,128)(2,1)S(1)}, bf16[656,128]{1,0:T(8,128)(2,1)S(1)}, u32[]{:S(2)}, u32[]{:S(2)}) %collective-permute-start.4) | collective-permute-done | bytes 167968 | tf_op jit(solution)/shard_map/ppermute | solution.py:40
  44.0 2.6 %stacked.1.mine_ref = bf16[8,656,128]{2,1,0:T(8,128)(2,1)} custom-call(bf16[656,128]{1,0:T(8,128)(2,1)} %copy-done.15, bf16[656,128]{1,0:T(8,128)(2,1)} %copy-done.16, bf16[656,128]{1,0:T(8,128)(2,1)} %copy-done.18, bf16[656,128]{1,0:T(8,128)(2,1)} %copy-done.20, bf16[656,128]{1,0:T(8,128)(2,1)} %copy-done.22, bf16[656,128]{1,0:T(8,128)(2,1)} %copy-done.21, ...), custom_call_target="tpu_custom_call" | custom-call | flops 1048576 | bytes 2097152 | tf_op jit(solution)/shard_map/stacked/pallas_call | solution.py:45
  46.7 7.1 %all-to-all-done.in_ref = bf16[4,128,1664]{2,1,0:T(8,128)(2,1)} async-done(((bf16[4,128,1664]{2,1,0:T(8,128)(2,1)}), bf16[4,128,1664]{2,1,0:T(8,128)(2,1)}, u32[]{:S(2)}, u32[]{:S(2)}) %all-to-all-start) | async-done | bytes 1703968 | tf_op jit(solution)/shard_map/all_to_all | solution.py:24
  56.2 5.4 %all-to-all-start.1 = ((bf16[8,16,1792]{2,1,0:T(8,128)(2,1)}), bf16[8,16,1792]{2,1,0:T(8,128)(2,1)}, u32[]{:S(2)}, u32[]{:S(2)}) async-start(bf16[8,16,1792]{2,1,0:T(8,128)(2,1)} %fold_y.1), calls=%async_computation.1 | async-start | bytes 917504 | tf_op jit(solution)/shard_map/all_to_all | solution.py:24
  67.1 8.5 %all-to-all-done.1.in_ref = bf16[8,16,1792]{2,1,0:T(8,128)(2,1)} async-done(((bf16[8,16,1792]{2,1,0:T(8,128)(2,1)}), bf16[8,16,1792]{2,1,0:T(8,128)(2,1)}, u32[]{:S(2)}, u32[]{:S(2)}) %all-to-all-start.1) | async-done | bytes 458784 | tf_op jit(solution)/shard_map/all_to_all | solution.py:24
  75.5 5.5 %recur.1 = (bf16[24,512]{1,0:T(8,128)(2,1)}, bf16[16,1024]{1,0:T(8,128)(2,1)}, f32[16,4,64,128]{3,2,1,0:T(8,128)}, f32[16,4,64]{2,1,0:T(4,128)}, f32[16,4]{1,0:T(8,128)}) custom-call(bf16[8,16,1792]{2,1,0:T(8,128)(2,1)} %all-to-all-done.1.in_ref, f32[1,4]{1,0:T(1,128)} %bitcast.70, f32[1,4]{1,0:T(1,128)} %bitcast.71, ...), custom_call_target="tpu_custom_call" | custom-call | flops 8388608 | bytes 5242880 | tf_op jit(solution)/shard_map/recur/pallas_call | solution.py:442
  92.2 7.0 %all-to-all-start.2 = ((bf16[16,16,1024]{2,1,0:T(8,128)(2,1)}), bf16[16,16,1024]{2,1,0:T(8,128)(2,1)}, u32[]{:S(2)}, u32[]{:S(2)}) async-start(bf16[16,16,1024]{2,1,0:T(8,128)(2,1)} %copy-done.6), calls=%async_computation.2 | async-start | bytes 1048576 | tf_op jit(solution)/shard_map/all_to_all | solution.py:24
  100.5 6.8 %all-to-all-done.2 = bf16[16,16,1024]{2,1,0:T(8,128)(2,1)} async-done(((bf16[16,16,1024]{2,1,0:T(8,128)(2,1)}), bf16[16,16,1024]{2,1,0:T(8,128)(2,1)}, u32[]{:S(2)}, u32[]{:S(2)}) %all-to-all-start.2) | async-done | bytes 524320 | tf_op jit(solution)/shard_map/all_to_all | solution.py:24
  107.3 3.4 %settle.1 = (bf16[16,4096]{1,0:T(8,128)(2,1)}, f32[16,128]{1,0:T(8,128)}, bf16[64,2,4096]{2,1,0:T(2,128)(2,1)}, bf16[16,1024]{1,0:T(8,128)(2,1)}, bf16[16,1024]{...) custom-call(s32[4]{0:T(128)} %pad_add_fusion.c_ref, bf16[4,4,16,1024]{3,2,1,0:T(8,128)(2,1)} %bitcast.16.got_ref, ...), custom_call_target="tpu_custom_call" | custom-call | flops 134217728 | bytes 3145728 | tf_op jit(solution)/shard_map/settle/pallas_call | solution.py:146
  110.7 7.2 %all-to-all-start.3 = ((bf16[64,2,4096]{2,1,0:T(2,128)(2,1)}), bf16[64,2,4096]{2,1,0:T(2,128)(2,1)}, u32[]{:S(2)}, u32[]{:S(2)}) async-start(bf16[64,2,4096]{2,1,0:T(2,128)(2,1)} %get-tuple-element.30), calls=%async_computation.3 | async-start | bytes 2097152 | tf_op jit(solution)/shard_map/all_to_all | solution.py:24
  122.8 3.4 %collective-permute-done.13.x2 = bf16[16,1024]{1,0:T(8,128)(2,1)S(1)} collective-permute-done((bf16[16,1024]{1,0:T(8,128)(2,1)}, bf16[16,1024]{1,0:T(8,128)(2,1)S(1)}, u32[]{:S(2)}, u32[]{:S(2)}) %collective-permute-start.13) | collective-permute-done | bytes 32800 | tf_op jit(solution)/shard_map/ppermute | solution.py:681
  142.3 2.6 %collective-permute-start.20 = (bf16[16,1024]{1,0:T(8,128)(2,1)S(1)}, bf16[16,1024]{1,0:T(8,128)(2,1)S(1)}, u32[]{:S(2)}, u32[]{:S(2)}) collective-permute-start(bf16[16,1024]{1,0:T(8,128)(2,1)S(1)} %get-tuple-element.41), channel_id=1, source_target_pairs={{0,8},{8,16},{16,24},{24,0},{1,9},{9,17},{17,25},{25,1},{2,10},{10... | collective-permute-start | bytes 98312 | tf_op jit(solution)/shard_map/ppermute | solution.py:689
  154.6 8.1 %all-to-all-start.4 = ((bf16[64,72,128]{2,1,0:T(8,128)(2,1)}), bf16[64,72,128]{2,1,0:T(8,128)(2,1)S(1)}, u32[]{:S(2)}, u32[]{:S(2)}) async-start(bf16[64,72,128]{2,1,0:T(8,128)(2,1)} %copy-done.4), calls=%async_computation.4 | async-start | bytes 2359296 | tf_op jit(solution)/shard_map/all_to_all | solution.py:24
  165.6 28.6 %all-to-all-done.4.got_ref = bf16[64,72,128]{2,1,0:T(8,128)(2,1)S(1)} async-done(((bf16[64,72,128]{2,1,0:T(8,128)(2,1)}), bf16[64,72,128]{2,1,0:T(8,128)(2,1)S(1)}, u32[]{:S(2)}, u32[]{:S(2)}) %all-to-all-start.4) | async-done | bytes 1179680 | tf_op jit(solution)/shard_map/all_to_all | solution.py:24
  200.7 3.9 %collective-permute-done.21.b1 = bf16[512,128]{1,0:T(8,128)(2,1)S(1)} collective-permute-done((bf16[512,128]{1,0:T(8,128)(2,1)S(1)}, bf16[512,128]{1,0:T(8,128)(2,1)S(1)}, u32[]{:S(2)}, u32[]{:S(2)}) %collective-permute-start.21) | collective-permute-done | bytes 131104 | tf_op jit(solution)/shard_map/ppermute | solution.py:698
  (157 shorter events, 66.7 us)
Async XLA Ops:
  4.8 19.2 %collective-permute-start = (bf16[4,128,1664]{2,1,0:T(8,128)(2,1)}, bf16[4,128,1664]{2,1,0:T(8,128)(2,1)}, u32[]{:S(2)}, u32[]{:S(2)}) collective-permute-start(bf16[4,128,1664]{2,1,0:T(8,128)(2,1)} %project_away.1), channel_id=1, source_target_pairs={{0,4},{4,0},{1,5},{5,1},{2,6},{6,2},{3,7},{7,3},{8,12},{12,8},{9,1... | collective-permute-start | bytes 5111816 | tf_op jit(solution)/shard_map/ppermute | solution.py:28
  5.9 10.9 %collective-permute-start.1 = (bf16[656,128]{1,0:T(8,128)(2,1)S(1)}, bf16[656,128]{1,0:T(8,128)(2,1)S(1)}, u32[]{:S(2)}, u32[]{:S(2)}) collective-permute-start(bf16[656,128]{1,0:T(8,128)(2,1)S(1)} %concatenate.11.refs_0_), channel_id=1, source_target_pairs={{0,32},{32,64},{64,96},{96,128},{128,160},{160,192},{192,224},{224... | collective-permute-start | bytes 503816 | tf_op jit(solution)/shard_map/ppermute | solution.py:40
  7.8 8.9 %collective-permute-start.5 = (bf16[656,128]{1,0:T(8,128)(2,1)S(1)}, bf16[656,128]{1,0:T(8,128)(2,1)S(1)}, u32[]{:S(2)}, u32[]{:S(2)}) collective-permute-start(bf16[656,128]{1,0:T(8,128)(2,1)S(1)} %concatenate.11.refs_0_), channel_id=1, source_target_pairs={{0,224},{32,0},{64,32},{96,64},{128,96},{160,128},{192,160},{224,1... | collective-permute-start | bytes 503816 | tf_op jit(solution)/shard_map/ppermute | solution.py:43
  16.7 7.3 %collective-permute-start.2 = (bf16[656,128]{1,0:T(8,128)(2,1)S(1)}, bf16[656,128]{1,0:T(8,128)(2,1)S(1)}, u32[]{:S(2)}, u32[]{:S(2)}) collective-permute-start(bf16[656,128]{1,0:T(8,128)(2,1)S(1)} %collective-permute-done.1.refs_1_), channel_id=1, source_target_pairs={{0,32},{32,64},{64,96},{96,128},{128,160},{160,192},{192,224},{224... | collective-permute-start | bytes 503816 | tf_op jit(solution)/shard_map/ppermute | solution.py:40
  16.8 16.8 %collective-permute-start.6 = (bf16[656,128]{1,0:T(8,128)(2,1)S(1)}, bf16[656,128]{1,0:T(8,128)(2,1)S(1)}, u32[]{:S(2)}, u32[]{:S(2)}) collective-permute-start(bf16[656,128]{1,0:T(8,128)(2,1)S(1)} %collective-permute-done.5.refs_7_), channel_id=1, source_target_pairs={{0,224},{32,0},{64,32},{96,64},{128,96},{160,128},{192,160},{224,1... | collective-permute-start | bytes 503816 | tf_op jit(solution)/shard_map/ppermute | solution.py:43
  24.1 12.6 %collective-permute-start.3 = (bf16[656,128]{1,0:T(8,128)(2,1)S(1)}, bf16[656,128]{1,0:T(8,128)(2,1)S(1)}, u32[]{:S(2)}, u32[]{:S(2)}) collective-permute-start(bf16[656,128]{1,0:T(8,128)(2,1)S(1)} %collective-permute-done.2.refs_2_), channel_id=1, source_target_pairs={{0,32},{32,64},{64,96},{96,128},{128,160},{160,192},{192,224},{224... | collective-permute-start | bytes 503816 | tf_op jit(solution)/shard_map/ppermute | solution.py:40
  28.6 25.1 %all-to-all-start = ((bf16[4,128,1664]{2,1,0:T(8,128)(2,1)}), bf16[4,128,1664]{2,1,0:T(8,128)(2,1)}, u32[]{:S(2)}, u32[]{:S(2)}) async-start(bf16[4,128,1664]{2,1,0:T(8,128)(2,1)} %get-tuple-element.25), calls=%async_computation | async-start | bytes 3407872 | tf_op jit(solution)/shard_map/all_to_all | solution.py:24
  33.5 6.1 %collective-permute-start.7 = (bf16[656,128]{1,0:T(8,128)(2,1)S(1)}, bf16[656,128]{1,0:T(8,128)(2,1)S(1)}, u32[]{:S(2)}, u32[]{:S(2)}) collective-permute-start(bf16[656,128]{1,0:T(8,128)(2,1)S(1)} %collective-permute-done.6.refs_6_), channel_id=1, source_target_pairs={{0,224},{32,0},{64,32},{96,64},{128,96},{160,128},{192,160},{224,1... | collective-permute-start | bytes 503816 | tf_op jit(solution)/shard_map/ppermute | solution.py:43
  36.7 6.6 %collective-permute-start.4 = (bf16[656,128]{1,0:T(8,128)(2,1)S(1)}, bf16[656,128]{1,0:T(8,128)(2,1)S(1)}, u32[]{:S(2)}, u32[]{:S(2)}) collective-permute-start(bf16[656,128]{1,0:T(8,128)(2,1)S(1)} %collective-permute-done.3.refs_3_), channel_id=1, source_target_pairs={{0,32},{32,64},{64,96},{96,128},{128,160},{160,192},{192,224},{224... | collective-permute-start | bytes 503816 | tf_op jit(solution)/shard_map/ppermute | solution.py:40
  46.5 18.5 %collective-permute-start.8 = (bf16[8,656,128]{2,1,0:T(8,128)(2,1)}, bf16[8,656,128]{2,1,0:T(8,128)(2,1)}, u32[]{:S(2)}, u32[]{:S(2)}) collective-permute-start(bf16[8,656,128]{2,1,0:T(8,128)(2,1)} %stacked.1.mine_ref), channel_id=1, source_target_pairs={{0,4},{4,0},{1,5},{5,1},{2,6},{6,2},{3,7},{7,3},{8,12},{12,8},{9,1... | collective-permute-start | bytes 4030472 | tf_op jit(solution)/shard_map/ppermute | solution.py:28
  56.2 19.4 %all-to-all-start.1 = ((bf16[8,16,1792]{2,1,0:T(8,128)(2,1)}), bf16[8,16,1792]{2,1,0:T(8,128)(2,1)}, u32[]{:S(2)}, u32[]{:S(2)}) async-start(bf16[8,16,1792]{2,1,0:T(8,128)(2,1)} %fold_y.1), calls=%async_computation.1 | async-start | bytes 917504 | tf_op jit(solution)/shard_map/all_to_all | solution.py:24
  82.5 5.5 %collective-permute-start.10 = (bf16[24,512]{1,0:T(8,128)(2,1)}, bf16[24,512]{1,0:T(8,128)(2,1)S(1)}, u32[]{:S(2)}, u32[]{:S(2)}) collective-permute-start(bf16[24,512]{1,0:T(8,128)(2,1)} %get-tuple-element.27.x0), channel_id=1, source_target_pairs={{0,16},{8,24},{16,0},{24,8},{1,17},{9,25},{17,1},{25,9},{2,18},{10... | collective-permute-start | bytes 73736 | tf_op jit(solution)/shard_map/ppermute | solution.py:668
  92.2 15.1 %all-to-all-start.2 = ((bf16[16,16,1024]{2,1,0:T(8,128)(2,1)}), bf16[16,16,1024]{2,1,0:T(8,128)(2,1)}, u32[]{:S(2)}, u32[]{:S(2)}) async-start(bf16[16,16,1024]{2,1,0:T(8,128)(2,1)} %copy-done.6), calls=%async_computation.2 | async-start | bytes 1048576 | tf_op jit(solution)/shard_map/all_to_all | solution.py:24
  110.7 36.0 %all-to-all-start.3 = ((bf16[64,2,4096]{2,1,0:T(2,128)(2,1)}), bf16[64,2,4096]{2,1,0:T(2,128)(2,1)}, u32[]{:S(2)}, u32[]{:S(2)}) async-start(bf16[64,2,4096]{2,1,0:T(2,128)(2,1)} %get-tuple-element.30), calls=%async_computation.3 | async-start | bytes 2097152 | tf_op jit(solution)/shard_map/all_to_all | solution.py:24
  119.5 6.6 %collective-permute-start.13 = (bf16[16,1024]{1,0:T(8,128)(2,1)}, bf16[16,1024]{1,0:T(8,128)(2,1)S(1)}, u32[]{:S(2)}, u32[]{:S(2)}) collective-permute-start(bf16[16,1024]{1,0:T(8,128)(2,1)} %get-tuple-element.36), channel_id=1, source_target_pairs={{0,16},{8,24},{16,0},{24,8},{1,17},{9,25},{17,1},{25,9},{2,18},{10... | collective-permute-start | bytes 98312 | tf_op jit(solution)/shard_map/ppermute | solution.py:681
  128.1 5.7 %collective-permute-start.15 = (bf16[64,512]{1,0:T(8,128)(2,1)S(1)}, bf16[64,512]{1,0:T(8,128)(2,1)S(1)}, u32[]{:S(2)}, u32[]{:S(2)}) collective-permute-start(bf16[64,512]{1,0:T(8,128)(2,1)S(1)} %dense_products.1.x0), channel_id=1, source_target_pairs={{0,8},{8,16},{16,24},{24,0},{1,9},{9,17},{17,25},{25,1},{2,10},{10... | collective-permute-start | bytes 196616 | tf_op jit(solution)/shard_map/ppermute | solution.py:685
  129.1 6.6 %collective-permute-start.16 = (bf16[64,512]{1,0:T(8,128)(2,1)S(1)}, bf16[64,512]{1,0:T(8,128)(2,1)S(1)}, u32[]{:S(2)}, u32[]{:S(2)}) collective-permute-start(bf16[64,512]{1,0:T(8,128)(2,1)S(1)} %dense_products.1.x0), channel_id=1, source_target_pairs={{0,16},{8,24},{16,0},{24,8},{1,17},{9,25},{17,1},{25,9},{2,18},{10... | collective-permute-start | bytes 196616 | tf_op jit(solution)/shard_map/ppermute | solution.py:685
  139.1 11.2 %collective-permute-start.18 = (bf16[16,1024]{1,0:T(8,128)(2,1)}, bf16[16,1024]{1,0:T(8,128)(2,1)S(1)}, u32[]{:S(2)}, u32[]{:S(2)}) collective-permute-start(bf16[16,1024]{1,0:T(8,128)(2,1)} %get-tuple-element.39), channel_id=1, source_target_pairs={{0,24},{8,0},{16,8},{24,16},{1,25},{9,1},{17,9},{25,17},{2,26},{10... | collective-permute-start | bytes 98312 | tf_op jit(solution)/shard_map/ppermute | solution.py:689
  140.9 9.4 %collective-permute-start.19 = (bf16[16,1024]{1,0:T(8,128)(2,1)S(1)}, bf16[16,1024]{1,0:T(8,128)(2,1)S(1)}, u32[]{:S(2)}, u32[]{:S(2)}) collective-permute-start(bf16[16,1024]{1,0:T(8,128)(2,1)S(1)} %get-tuple-element.40), channel_id=1, source_target_pairs={{0,16},{8,24},{16,0},{24,8},{1,17},{9,25},{17,1},{25,9},{2,18},{10... | collective-permute-start | bytes 98312 | tf_op jit(solution)/shard_map/ppermute | solution.py:689
  142.3 8.1 %collective-permute-start.20 = (bf16[16,1024]{1,0:T(8,128)(2,1)S(1)}, bf16[16,1024]{1,0:T(8,128)(2,1)S(1)}, u32[]{:S(2)}, u32[]{:S(2)}) collective-permute-start(bf16[16,1024]{1,0:T(8,128)(2,1)S(1)} %get-tuple-element.41), channel_id=1, source_target_pairs={{0,8},{8,16},{16,24},{24,0},{1,9},{9,17},{17,25},{25,1},{2,10},{10... | collective-permute-start | bytes 98312 | tf_op jit(solution)/shard_map/ppermute | solution.py:689
  154.6 39.7 %all-to-all-start.4 = ((bf16[64,72,128]{2,1,0:T(8,128)(2,1)}), bf16[64,72,128]{2,1,0:T(8,128)(2,1)S(1)}, u32[]{:S(2)}, u32[]{:S(2)}) async-start(bf16[64,72,128]{2,1,0:T(8,128)(2,1)} %copy-done.4), calls=%async_computation.4 | async-start | bytes 2359296 | tf_op jit(solution)/shard_map/all_to_all | solution.py:24
  196.6 8.1 %collective-permute-start.21 = (bf16[512,128]{1,0:T(8,128)(2,1)S(1)}, bf16[512,128]{1,0:T(8,128)(2,1)S(1)}, u32[]{:S(2)}, u32[]{:S(2)}) collective-permute-start(bf16[512,128]{1,0:T(8,128)(2,1)S(1)} %combine.1.b0), channel_id=1, source_target_pairs={{0,1},{1,2},{2,3},{3,0},{4,5},{5,6},{6,7},{7,4},{8,9},{9,10},{10,1... | collective-permute-start | bytes 393224 | tf_op jit(solution)/shard_map/ppermute | solution.py:698
  197.2 7.5 %collective-permute-start.22 = (bf16[512,128]{1,0:T(8,128)(2,1)S(1)}, bf16[512,128]{1,0:T(8,128)(2,1)S(1)}, u32[]{:S(2)}, u32[]{:S(2)}) collective-permute-start(bf16[512,128]{1,0:T(8,128)(2,1)S(1)} %combine.1.b0), channel_id=1, source_target_pairs={{0,2},{1,3},{2,0},{3,1},{4,6},{5,7},{6,4},{7,5},{8,10},{9,11},{10,... | collective-permute-start | bytes 393224 | tf_op jit(solution)/shard_map/ppermute | solution.py:698
  198.6 6.7 %collective-permute-start.23 = (bf16[512,128]{1,0:T(8,128)(2,1)S(1)}, bf16[512,128]{1,0:T(8,128)(2,1)S(1)}, u32[]{:S(2)}, u32[]{:S(2)}) collective-permute-start(bf16[512,128]{1,0:T(8,128)(2,1)S(1)} %combine.1.b0), channel_id=1, source_target_pairs={{0,3},{1,0},{2,1},{3,2},{4,7},{5,4},{6,5},{7,6},{8,11},{9,8},{10,9... | collective-permute-start | bytes 393224 | tf_op jit(solution)/shard_map/ppermute | solution.py:698
  (39 other events, 454.4 us)
